TPU v7x, 256 devices: a whole 4x4x8 slice. The times are simulated.
256 devices in a mesh: ep: 64 (over z, y, core), tp: 4 (over x).
Axes of the slice: x: 4, y: 4, z: 8, core: 2. Of those that a mesh axis runs over, the one named last changes fastest.
Arguments:
- tokens: bfloat16 [3072, 2048], P('ep'), may hold values from -6 to 6
- out_grad: bfloat16 [3072, 2048], P('ep'), may hold values from -4 to 4
- expert_ids: int32 [3072, 4], P('ep'), may hold values from 0 to 63, all different within a row; in each aligned block of 48 rows (0 to 47, 48 to 95, ...) at most 8 rows name the same one
- router_weight: bfloat16 [2048, 64], replicated, may hold values from -0.125 to 0.125
- w_gate: bfloat16 [64, 2048, 1536], P('ep', None, 'tp'), may hold values from -0.125 to 0.125
- w_up: bfloat16 [64, 2048, 1536], P('ep', None, 'tp'), may hold values from -0.125 to 0.125
- w_down: bfloat16 [64, 1536, 2048], P('ep', 'tp'), may hold values from -0.15625 to 0.15625
Outputs:
- token_grad: bfloat16 [3072, 2048], P('ep', 'tp')
- router_grad: float32 [2048, 64], P('tp', 'ep')
- w_gate_grad: bfloat16 [64, 2048, 1536], P('ep', None, 'tp')
- w_up_grad: bfloat16 [64, 2048, 1536], P('ep', None, 'tp')
- w_down_grad: bfloat16 [64, 1536, 2048], P('ep', 'tp')
Inputs may be any that keep to these rules, and one draw needn't show every extreme that they name: `expert_ids`: each row names 4 different experts; among the rows of one device no expert is named more than 8 times, and in some devices' rows one expert is named exactly 8 times.
All inputs are finite; a program needn't handle non-finite values.
Results may differ from a plain program's by a relative error of at most 0.0058.
Values may be sent and summed in bfloat16 or wider, within the bound.
No kernel may reach another device: no remote copies, remote signals or barrier semaphores. Data moves between devices by JAX's collectives and lax.ppermute only.
A program may use at most 128 MiB of HBM per device.

v0:
```python
import jax
import jax.numpy as jnp
from jax import lax
from jax.sharding import PartitionSpec as P


def side_by_side(arrays, axis, split_dim, concat_dim, along):
    both = jnp.concatenate(arrays, axis=along)
    out, at, gathered = (
        lax.all_to_all(both, axis, split_axis=split_dim, concat_axis=concat_dim, tiled=True),
        0,
        [],
    )
    for a in arrays:
        gathered.append(lax.slice_in_dim(out, at, at + a.shape[along], axis=along))
        at += a.shape[along]
    return tuple(gathered)


def side_by_side_2(arrays, axis, dim, along):
    both = jnp.concatenate(arrays, axis=along)
    out, at, gathered = (lax.all_gather(both, axis, axis=dim, tiled=True), 0, [])
    for a in arrays:
        gathered.append(lax.slice_in_dim(out, at, at + a.shape[along], axis=along))
        at += a.shape[along]
    return tuple(gathered)


def laid_out(blocks, dim):
    dims = list(blocks.shape[1:])
    dims[dim] *= blocks.shape[0]
    return jnp.moveaxis(blocks, 0, dim).reshape(dims)


def from_everyone(value, axis):
    copies = jnp.broadcast_to(value, (lax.axis_size(axis), *value.shape))
    return lax.all_to_all(copies, axis, split_axis=0, concat_axis=0, tiled=True)


def collect(value, axis, dim):
    return laid_out(from_everyone(value, axis), dim)


def split_up(value, dim, devices):
    before, after = (value.shape[:dim], value.shape[dim + 1 :])
    return jnp.moveaxis(value.reshape(*before, devices, -1, *after), dim, 0)


def summed_on_arrival(value, axis, dim):
    devices = lax.axis_size(axis)
    blocks = lax.all_to_all(split_up(value, dim, devices), axis, 0, 0, tiled=True)
    return jnp.sum(blocks.astype(jnp.float32), axis=0)


def side_by_side_3(arrays, axis, split_dim, concat_dim, along):
    columns = [a.reshape(*a.shape[:along], -1) for a in arrays]
    both = jnp.concatenate(columns, axis=along)
    out, at, gathered = (
        lax.all_to_all(both, axis, split_axis=split_dim, concat_axis=concat_dim, tiled=True),
        0,
        [],
    )
    for a, column in zip(arrays, columns):
        piece = out[..., at : at + column.shape[along]]
        gathered.append(piece.reshape(*piece.shape[:along], *a.shape[along:]))
        at += column.shape[along]
    return tuple(gathered)


def taken_together(value, axis):
    return from_everyone(value, axis).sum(axis=0)


def sum_at_owner(value, axis, dim):
    blocks = split_up(value, dim, lax.axis_size(axis))
    arrived = lax.all_to_all(blocks, axis, split_axis=0, concat_axis=0, tiled=True)
    return arrived.sum(axis=0)


def activation_parts(gate_pre, up_pre):
    glu = jnp.minimum(gate_pre, 7.0)
    linear = jnp.clip(up_pre, -7.0, 7.0)
    sigma = jax.nn.sigmoid(1.702 * glu)
    act_value = glu * sigma
    hidden = (linear + 1.0) * act_value
    slope = (linear + 1.0) * (sigma + 1.702 * glu * sigma * (1.0 - sigma))
    slope = jnp.where(gate_pre < 7.0, slope, 0.0)
    up_slope = jnp.where((up_pre > -7.0) & (up_pre < 7.0), act_value, 0.0)
    return (hidden, slope, up_slope)


def contract_last(left, right):
    return lax.dot_general(
        left, right, (((1,), (1,)), ((), ())), preferred_element_type=jnp.float32
    )


def contract_first(left, right):
    return lax.dot_general(
        left, right, (((0,), (0,)), ((), ())), preferred_element_type=jnp.float32
    )


def per_device(tokens, out_grad, expert_ids, router_weight, w_gate, w_up, w_down):
    tok_dev, model_width = tokens.shape
    top_count = expert_ids.shape[1]
    expert_count = router_weight.shape[1]
    peer_count = lax.axis_size("ep")
    tp_count = lax.axis_size("tp")
    capacity = min(
        tok_dev,
        tp_count * max(1, (2 * tok_dev * top_count // expert_count + tp_count - 1) // tp_count),
    )
    feature_part = model_width // tp_count
    logits = jnp.dot(tokens, router_weight, preferred_element_type=jnp.float32)
    chosen = jnp.take_along_axis(logits, expert_ids, axis=1)
    gate_values = jax.nn.softmax(chosen, axis=-1)
    flat_ids = expert_ids.reshape(-1)
    one_hot = (flat_ids[:, None] == jnp.arange(expert_count, dtype=jnp.int32)[None, :]).astype(
        jnp.int32
    )
    slot_rank = jnp.sum((jnp.cumsum(one_hot, axis=0) - one_hot) * one_hot, axis=1)
    slot_index = flat_ids * capacity + slot_rank
    flat_tok = jnp.arange(tok_dev * top_count, dtype=jnp.int32) // top_count
    buffer_rows = expert_count * capacity
    sent_tokens = (
        jnp.zeros((buffer_rows, model_width), jnp.bfloat16).at[slot_index].set(tokens[flat_tok])
    )
    sent_grads = (
        jnp.zeros((buffer_rows, model_width), jnp.bfloat16).at[slot_index].set(out_grad[flat_tok])
    )
    sent_gates = jnp.zeros((buffer_rows,), jnp.float32).at[slot_index].set(gate_values.reshape(-1))
    slot_tokens = sent_tokens.reshape(expert_count, capacity, model_width)
    slot_grads = sent_grads.reshape(expert_count, capacity, model_width)
    slot_gates = sent_gates.reshape(expert_count, capacity)
    slot_share = capacity // tp_count
    share_start = lax.axis_index("tp") * slot_share
    part_tokens = lax.dynamic_slice_in_dim(slot_tokens, share_start, slot_share, 1)
    part_grads = lax.dynamic_slice_in_dim(slot_grads, share_start, slot_share, 1)
    part_gates = lax.dynamic_slice_in_dim(slot_gates, share_start, slot_share, 1)
    got_tokens, got_grads = side_by_side((part_tokens, part_grads), "ep", 0, 0, 1)
    got_gates = lax.all_to_all(part_gates, "ep", split_axis=0, concat_axis=0, tiled=True)
    recv_tokens, recv_grads = side_by_side_2((got_tokens, got_grads), "tp", 1, 0)
    recv_gates = collect(got_gates, "tp", 1)
    slot_count = peer_count * capacity
    inputs_rows = recv_tokens.reshape(slot_count, model_width)
    grad_rows = recv_grads.reshape(slot_count, model_width)
    weight_rows = recv_gates.reshape(slot_count)
    gate_mat = w_gate[0]
    up_mat = w_up[0]
    down_mat = w_down[0]
    gate_pre = jnp.dot(inputs_rows, gate_mat, preferred_element_type=jnp.float32)
    up_pre = jnp.dot(inputs_rows, up_mat, preferred_element_type=jnp.float32)
    hidden, slope, up_slope = activation_parts(gate_pre, up_pre)
    back_proj = contract_last(grad_rows, down_mat)
    gate_score = jnp.sum(hidden * back_proj, axis=1)
    d_hidden = weight_rows[:, None] * back_proj
    d_gate_pre = (d_hidden * slope).astype(jnp.bfloat16)
    d_up_pre = (d_hidden * up_slope).astype(jnp.bfloat16)
    weighted = (weight_rows[:, None] * hidden).astype(jnp.bfloat16)
    w_down_grad = contract_first(weighted, grad_rows).astype(jnp.bfloat16)[None]
    w_gate_grad = contract_first(inputs_rows, d_gate_pre).astype(jnp.bfloat16)[None]
    w_up_grad = contract_first(inputs_rows, d_up_pre).astype(jnp.bfloat16)[None]
    summed_part = summed_on_arrival(
        (contract_last(gate_mat, d_gate_pre) + contract_last(up_mat, d_up_pre)).astype(
            jnp.bfloat16
        ),
        "tp",
        0,
    )
    returned = summed_part.T.reshape(peer_count, capacity, feature_part)
    home_grads, home_scores = side_by_side_3(
        (returned, gate_score.reshape(peer_count, capacity)), "ep", 0, 0, 2
    )
    picked = home_grads.reshape(buffer_rows, feature_part)[slot_index]
    expert_part = jnp.sum(picked.reshape(tok_dev, top_count, feature_part), axis=1)
    local_scores = home_scores.reshape(buffer_rows)[slot_index].reshape(tok_dev, top_count)
    total_scores = taken_together(local_scores, "tp")
    d_chosen = gate_values * (
        total_scores - jnp.sum(gate_values * total_scores, axis=-1, keepdims=True)
    )
    expert_hot = (
        expert_ids[:, :, None] == jnp.arange(expert_count, dtype=jnp.int32)[None, None, :]
    ).astype(jnp.float32)
    d_logits = jnp.sum(d_chosen[:, :, None] * expert_hot, axis=1)
    column = lax.axis_index("tp") * feature_part
    local_tokens = lax.dynamic_slice_in_dim(tokens, column, feature_part, 1).astype(jnp.float32)
    router_term = jnp.dot(local_tokens.T, d_logits, precision=lax.Precision.HIGHEST)
    router_grad = sum_at_owner(router_term, "ep", 1)
    router_rows = lax.dynamic_slice_in_dim(router_weight, column, feature_part, 0).astype(
        jnp.float32
    )
    router_part = jnp.dot(d_logits, router_rows.T, precision=lax.Precision.HIGHEST)
    token_grad = (expert_part + router_part).astype(jnp.bfloat16)
    return (token_grad, router_grad, w_gate_grad, w_up_grad, w_down_grad)


def solution(mesh):
    in_specs = (
        P("ep", None),
        P("ep", None),
        P("ep", None),
        P(),
        P("ep", None, "tp"),
        P("ep", None, "tp"),
        P("ep", "tp", None),
    )
    out_specs = (
        P("ep", "tp"),
        P("tp", "ep"),
        P("ep", None, "tp"),
        P("ep", None, "tp"),
        P("ep", "tp", None),
    )
    return jax.shard_map(
        per_device, mesh=mesh, in_specs=in_specs, out_specs=out_specs, check_vma=False
    )
```

profile of v0, /device:TPU:1, one launch (start us, length us, event | category | flops | bytes accessed | tf_op | source)
XLA Modules:
  0.0 254.1 jit_solution(215335838511083896)
XLA Ops:
  10.1 6.4 %scatter_custom_fusion.1 = bf16[512,2048]{1,0:T(8,128)(2,1)} fusion(s32[192]{0:T(256)S(1)} %bitcast.99, bf16[]{:T(256)} %constant.65.clone.1, bf16[48,2048]{1,0:T(8,128)(2,1)} %param.7, s32[1024]{0:T(1024)S(1)} %pad_clamp_fusion.1), kind=kCustom, calls=%fused_computation.37 | custom fusion | bytes 2097664 | tf_op jit(solution)/shard_map/scatter | solution.py:127
  16.6 6.5 %scatter_custom_fusion.2 = bf16[512,2048]{1,0:T(8,128)(2,1)} fusion(s32[192]{0:T(256)S(1)} %bitcast.100, bf16[]{:T(256)} %constant.65.clone.1, bf16[48,2048]{1,0:T(8,128)(2,1)} %param.8, s32[1024]{0:T(1024)S(1)} %pad_clamp_fusion.1), kind=kCustom, calls=%fused_computation.35 | custom fusion | bytes 2097664 | tf_op jit(solution)/shard_map/scatter | solution.py:130
  23.0 2.1 constant_dynamic-slice_fusion.1
  25.2 2.1 constant_dynamic-slice_fusion
  28.4 41.1 %all_to_all.42 = bf16[64,4,2048]{2,1,0:T(4,128)(2,1)S(1)} all-to-all(bf16[64,4,2048]{2,1,0:T(4,128)(2,1)S(1)} %pad_maximum_fusion.1), channel_id=1, replica_groups=mesh['ep'=64,'tp'=4] {'ep'}, dimensions={0} | all-to-all | bytes 2097152 | tf_op jit(solution)/shard_map/all_to_all | solution.py:10
  77.3 15.5 %all_to_all.43 = f32[64,1,2]{2,1,0:T(1,128)S(1)} all-to-all(f32[64,1,2]{2,1,0:T(1,128)S(1)} %bitcast.96), channel_id=1, replica_groups=mesh['ep'=64,'tp'=4] {'ep'}, dimensions={0} | all-to-all | bytes 1024 | tf_op jit(solution)/shard_map/all_to_all | solution.py:142
  92.9 8.2 %all_to_all.44 = f32[4,1,128]{2,1,0:T(1,128)S(1)} all-to-all(f32[4,1,128]{2,1,0:T(1,128)S(1)} %reshape.278), channel_id=1, replica_groups=mesh['ep'=64,'tp'=4] {'tp'}, dimensions={0} | all-to-all | bytes 4096 | tf_op jit(solution)/shard_map/all_to_all | solution.py:37
  102.7 17.9 %all-gather.2.cloned.1.call-done = bf16[128,8,2048]{2,0,1:T(8,128)(2,1)} async-done(((bf16[128,2,2048]{2,0,1:T(8,128)(2,1)}), bf16[128,8,2048]{2,0,1:T(8,128)(2,1)}) %all-gather.2.cloned.1.call-update) | async-done | bytes 4194320 | tf_op jit(solution)/shard_map/all_gather | solution.py:22
  120.7 2.7 %fusion.36 = (bf16[64,8,2048]{2,0,1:T(8,128)(2,1)S(1)}, bf16[64,8,2048]{2,0,1:T(8,128)(2,1)S(1)}) fusion(bf16[128,8,2048]{2,0,1:T(8,128)(2,1)} %all-gather.2.cloned.1.call-done), kind=kLoop, calls=%fused_computation.93 | loop fusion | bytes 8388608 | tf_op jit(solution)/shard_map/slice | solution.py:24
  123.4 1.6 fusion.9
  127.6 3.6 %multiply_convert_fusion.1 = (bf16[512,384]{0,1:T(8,128)(2,1)S(1)}, bf16[512,384]{0,1:T(8,128)(2,1)S(1)}, f32[512]{0:T(512)}, f32[512,384]{0,1:T(8,128)}) fusion(f32[512,384]{0,1:T(8,128)S(1)} %fusion.3, f32[512]{0:T(512)S(1)} %mul.90, f32[512,384]{0,1:T(8,128)S(1)} %fusion.9, bf16[1,2048,384]{2,1,0:T(8,128)(2,1)S(1)} %copy-done, ...), kind=kOutput, calls=%fused_computation.43 | convolution fusion | flops 810614272 | bytes 6819840 | tf_op jit(solution)/shard_map/dot_general | solution.py:153
  135.3 4.6 %all-to-all-start.3 = ((bf16[4,512,512]{1,2,0:T(8,128)(2,1)}), bf16[4,512,512]{1,2,0:T(8,128)(2,1)}, u32[]{:S(2)}, u32[]{:S(2)}) async-start(bf16[4,512,512]{1,2,0:T(8,128)(2,1)} %bitcast.91), calls=%async_computation.3 | async-start | bytes 4194304 | tf_op jit(solution)/shard_map/all_to_all | solution.py:51
  140.1 25.4 %all-to-all-done.3 = bf16[4,512,512]{1,2,0:T(8,128)(2,1)} async-done(((bf16[4,512,512]{1,2,0:T(8,128)(2,1)}), bf16[4,512,512]{1,2,0:T(8,128)(2,1)}, u32[]{:S(2)}, u32[]{:S(2)}) %all-to-all-start.3) | async-done | bytes 2097184 | tf_op jit(solution)/shard_map/all_to_all | solution.py:51
  165.6 2.0 convert_reduce_fusion
  168.8 11.7 %all-to-all-start.4 = ((f32[64,8,513]{2,1,0:T(8,128)}), f32[64,8,513]{2,1,0:T(8,128)S(1)}, u32[]{:S(2)}, u32[]{:S(2)}) async-start(f32[64,8,513]{2,1,0:T(8,128)} %pad_maximum_fusion), calls=%async_computation.4 | async-start | bytes 2621440 | tf_op jit(solution)/shard_map/all_to_all | solution.py:59
  180.6 4.6 %fusion.1 = bf16[1,2048,384]{2,1,0:T(8,128)(2,1)} fusion(bf16[512,384]{0,1:T(8,128)(2,1)} %copy-done.7, bf16[64,8,2048]{2,0,1:T(8,128)(2,1)} %copy-done.2), kind=kOutput, calls=%fused_computation.14 | convolution fusion | flops 806092800 | bytes 4063232 | tf_op jit(solution)/shard_map/dot_general | solution.py:99
  185.1 3.0 %fusion.2 = bf16[1,384,2048]{2,1,0:T(8,128)(2,1)} fusion(bf16[64,8,2048]{2,0,1:T(8,128)(2,1)S(1)} %copy-done.4, f32[512]{0:T(512)S(1)} %copy-done.15, f32[512,384]{0,1:T(8,128)S(1)} %copy-done.20, f32[512,384]{0,1:T(8,128)S(1)} %copy-done.19), kind=kOutput, calls=%fused_computation.15 | convolution fusion | flops 808255488 | bytes 5244928 | tf_op jit(solution)/shard_map/dot_general | solution.py:99
  188.1 26.0 %all-to-all-done.4 = f32[64,8,513]{2,1,0:T(8,128)S(1)} async-done(((f32[64,8,513]{2,1,0:T(8,128)}), f32[64,8,513]{2,1,0:T(8,128)S(1)}, u32[]{:S(2)}, u32[]{:S(2)}) %all-to-all-start.4) | async-done | bytes 1050656 | tf_op jit(solution)/shard_map/all_to_all | solution.py:59
  215.4 1.6 gather_fusion.1
  217.9 3.2 %all-to-all-start.5 = ((f32[4,1,192]{2,1,0:T(1,128)}), f32[4,1,192]{2,1,0:T(1,128)S(1)}, u32[]{:S(2)}, u32[]{:S(2)}) async-start(f32[4,1,192]{2,1,0:T(1,128)} %reshape.280), calls=%async_computation.5 | async-start | bytes 8192 | tf_op jit(solution)/shard_map/all_to_all | solution.py:37
  221.2 4.4 %fusion = bf16[1,2048,384]{2,1,0:T(8,128)(2,1)} fusion(bf16[512,384]{0,1:T(8,128)(2,1)S(1)} %get-tuple-element.10, bf16[64,8,2048]{2,0,1:T(8,128)(2,1)} %copy-done.2), kind=kOutput, calls=%fused_computation.13 | convolution fusion | flops 806092800 | bytes 4063232 | tf_op jit(solution)/shard_map/dot_general | solution.py:99
  228.3 7.2 %all-to-all-start.6 = ((f32[64,512,1]{1,2,0:T(1,128)}), f32[64,512,1]{1,2,0:T(1,128)S(1)}, u32[]{:S(2)}, u32[]{:S(2)}) async-start(f32[64,512,1]{1,2,0:T(1,128)} %copy.117), calls=%async_computation.6 | async-start | bytes 262144 | tf_op jit(solution)/shard_map/all_to_all | solution.py:76
  238.0 1.6 fusion.12
  239.7 6.9 %all-to-all-done.6 = f32[64,512,1]{1,2,0:T(1,128)S(1)} async-done(((f32[64,512,1]{1,2,0:T(1,128)}), f32[64,512,1]{1,2,0:T(1,128)S(1)}, u32[]{:S(2)}, u32[]{:S(2)}) %all-to-all-start.6) | async-done | bytes 131104 | tf_op jit(solution)/shard_map/all_to_all | solution.py:76
  (114 shorter events, 29.5 us)
Async XLA Ops:
  7.2 120.4 %copy-start = (bf16[1,2048,384]{2,1,0:T(8,128)(2,1)S(1)}, bf16[1,2048,384]{2,1,0:T(8,128)(2,1)}, u32[]{:S(2)}) copy-start(bf16[1,2048,384]{2,1,0:T(8,128)(2,1)} %param.12) | copy-start | bytes 4718596
  7.2 113.5 %all-gather.2.cloned.1.call-start = ((), (), s32[]{:S(2)}) async-start(), calls=%async_computation.7 | async-start | bytes 5242880 | tf_op jit(solution)/shard_map/all_gather | solution.py:22
  10.1 65.4 %copy-start.12 = (s32[192,1]{0,1:T(1,128)}, s32[192,1]{0,1:T(1,128)S(1)}, u32[]{:S(2)}) copy-start(s32[192,1]{0,1:T(1,128)S(1)} %get-tuple-element.16) | copy-start | bytes 2308
  71.6 1.4 copy-start.9
  71.6 1.6 copy-start.6
  71.7 1.6 copy-start.8
  102.7 24.8 %copy-start.14 = (f32[512]{0:T(512)}, f32[512]{0:T(512)S(1)}, u32[]{:S(2)}) copy-start(f32[512]{0:T(512)S(1)} %mul.90) | copy-start | bytes 6148
  102.7 20.7 %copy-start.5 = (bf16[1,2048,384]{2,1,0:T(8,128)(2,1)S(1)}, bf16[1,2048,384]{2,1,0:T(8,128)(2,1)}, u32[]{:S(2)}) copy-start(bf16[1,2048,384]{2,1,0:T(8,128)(2,1)} %param.11) | copy-start | bytes 4718596
  123.4 1.7 copy-start.3
  123.4 4.1 %copy-start.2 = (bf16[64,8,2048]{2,0,1:T(8,128)(2,1)}, bf16[64,8,2048]{2,0,1:T(8,128)(2,1)S(1)}, u32[]{:S(2)}) copy-start(bf16[64,8,2048]{2,0,1:T(8,128)(2,1)S(1)} %get-tuple-element.7) | copy-start | bytes 6291460
  123.4 2.6 %copy-start.17 = (bf16[1,384,2048]{2,1,0:T(8,128)(2,1)S(1)}, bf16[1,384,2048]{2,1,0:T(8,128)(2,1)}, u32[]{:S(2)}) copy-start(bf16[1,384,2048]{2,1,0:T(8,128)(2,1)} %param.13) | copy-start | bytes 4718596
  125.1 2.5 copy-start.18
  131.2 1.3 copy-start.7
  135.3 4.6 %copy-start.16 = (f32[512]{0:T(512)S(1)}, f32[512]{0:T(512)}, u32[]{:S(2)}) copy-start(f32[512]{0:T(512)} %get-tuple-element.11) | copy-start | bytes 6148
  135.3 30.2 %all-to-all-start.3 = ((bf16[4,512,512]{1,2,0:T(8,128)(2,1)}), bf16[4,512,512]{1,2,0:T(8,128)(2,1)}, u32[]{:S(2)}, u32[]{:S(2)}) async-start(bf16[4,512,512]{1,2,0:T(8,128)(2,1)} %bitcast.91), calls=%async_computation.3 | async-start | bytes 4194304 | tf_op jit(solution)/shard_map/all_to_all | solution.py:51
  167.6 12.9 %copy-start.13 = (s32[192,1]{0,1:T(1,128)S(1)}, s32[192,1]{0,1:T(1,128)}, u32[]{:S(2)}) copy-start(s32[192,1]{0,1:T(1,128)} %copy-done.12) | copy-start | bytes 2308
  168.8 45.3 %all-to-all-start.4 = ((f32[64,8,513]{2,1,0:T(8,128)}), f32[64,8,513]{2,1,0:T(8,128)S(1)}, u32[]{:S(2)}, u32[]{:S(2)}) async-start(f32[64,8,513]{2,1,0:T(8,128)} %pad_maximum_fusion), calls=%async_computation.4 | async-start | bytes 2621440 | tf_op jit(solution)/shard_map/all_to_all | solution.py:59
  180.5 4.6 %copy-start.4 = (bf16[64,8,2048]{2,0,1:T(8,128)(2,1)S(1)}, bf16[64,8,2048]{2,0,1:T(8,128)(2,1)}, u32[]{:S(2)}) copy-start(bf16[64,8,2048]{2,0,1:T(8,128)(2,1)} %copy-done.3) | copy-start | bytes 6291460
  180.5 4.6 %copy-start.15 = (f32[512]{0:T(512)S(1)}, f32[512]{0:T(512)}, u32[]{:S(2)}) copy-start(f32[512]{0:T(512)} %copy-done.14) | copy-start | bytes 6148
  180.5 4.6 %copy-start.19 = (f32[512,384]{0,1:T(8,128)S(1)}, f32[512,384]{0,1:T(8,128)}, u32[]{:S(2)}) copy-start(f32[512,384]{0,1:T(8,128)} %copy-done.18) | copy-start | bytes 2359300
  180.5 4.6 %copy-start.20 = (f32[512,384]{0,1:T(8,128)S(1)}, f32[512,384]{0,1:T(8,128)}, u32[]{:S(2)}) copy-start(f32[512,384]{0,1:T(8,128)} %get-tuple-element.14) | copy-start | bytes 2359300
  217.9 7.6 %all-to-all-start.5 = ((f32[4,1,192]{2,1,0:T(1,128)}), f32[4,1,192]{2,1,0:T(1,128)S(1)}, u32[]{:S(2)}, u32[]{:S(2)}) async-start(f32[4,1,192]{2,1,0:T(1,128)} %reshape.280), calls=%async_computation.5 | async-start | bytes 8192 | tf_op jit(solution)/shard_map/all_to_all | solution.py:37
  221.2 5.1 %copy-start.11 = (f32[48]{0:T(128)S(1)}, f32[48]{0:T(128)}, u32[]{:S(2)}) copy-start(f32[48]{0:T(128)} %copy-done.10) | copy-start | bytes 580
  228.3 18.3 %all-to-all-start.6 = ((f32[64,512,1]{1,2,0:T(1,128)}), f32[64,512,1]{1,2,0:T(1,128)S(1)}, u32[]{:S(2)}, u32[]{:S(2)}) async-start(f32[64,512,1]{1,2,0:T(1,128)} %copy.117), calls=%async_computation.6 | async-start | bytes 262144 | tf_op jit(solution)/shard_map/all_to_all | solution.py:76
  (2 other events, 1.7 us)
Sparse Core Ops, SparseCore 0:
  73.1 47.4 all-gather.1
where the time goes:
time: 255 us; the launch traced here: 254 us
  waiting for transfers between devices  76.3 us (30%)
  blocking collectives  64.8 us (25%)
  local copies, waits for them, and re-layouts  38 us (15%)
  starting transfers between devices  26.8 us (11%)
  matrix products  24.2 us (9%)
  between operations  14.6 us (6%)
  other arithmetic  9.56 us (4%)
    all_to_all x1, blocking collectives, side_by_side(): lax.all_to_all(both, axis, split_axis=split_dim, concat_axis=concat_dim,...  41.1 us
    all_to_all x1, waiting for transfers between devices, side_by_side_3(): lax.all_to_all(both, axis, split_axis=split_dim, concat_axis=concat_dim,...  26 us
    all_to_all x1, waiting for transfers between devices, summed_on_arrival(): lax.all_to_all(split_up(value, dim, devices), axis, 0, 0, tiled=True)  25.4 us
    all_gather x1, waiting for transfers between devices, side_by_side_2(): lax.all_gather(both, axis, axis=dim, tiled=True)  17.9 us
    all_to_all x1, blocking collectives, per_device(): lax.all_to_all(part_gates, 'ep', split_axis=0, concat_axis=0, tiled=True)  15.5 us
    scatter x2, local copies, waits for them, and re-layouts, per_device(): jnp.zeros((buffer_rows, model_width), jnp.bfloat16).at[slot_index]  12.9 us
    dot_general x3, matrix products, contract_first(): lax.dot_general(left, right, (((0,), (0,)), ((), ())), preferred_element_...  11.9 us
    all_to_all x1, starting transfers between devices, side_by_side_3(): lax.all_to_all(both, axis, split_axis=split_dim, concat_axis=concat_dim,...  11.7 us
  transfers between devices with their start and end apart: 5, of which 4 were waited for; matrix products, arithmetic and copies ran while one was open for 9% of the time, Pallas kernels for 0%

commit v1 on v0

v1 whole, which is shorter than its diff:
```python
import functools

import jax
import jax.numpy as jnp
from jax import lax
from jax.experimental import pallas as pl
from jax.experimental.pallas import tpu as pltpu
from jax.sharding import PartitionSpec as P

F32 = jnp.float32
BF16 = jnp.bfloat16
HI = lax.Precision.HIGHEST
VMEM = pl.BlockSpec(memory_space=pltpu.VMEM)
SMEM = pl.BlockSpec(memory_space=pltpu.SMEM)


def mm(a, b, dims, precision=None):
    return lax.dot_general(a, b, (dims, ((), ())), precision=precision, preferred_element_type=F32)


NN = ((1,), (0,))
NT = ((1,), (1,))
TN = ((0,), (0,))


def iota(shape, dim):
    return lax.broadcasted_iota(jnp.int32, shape, dim)


def spread(experts, cap):
    rows = experts * cap
    return (iota((rows, experts), 0) // cap == iota((rows, experts), 1)).astype(F32)


def dispatch_kernel(cap, tp_ref, tok_ref, og_ref, ids_ref, rw_ref, send_ref, code_ref, gate_ref):
    n_tok, width = tok_ref.shape
    experts = rw_ref.shape[1]
    share = send_ref.shape[1] // 2
    start = pl.multiple_of(tp_ref[0] * share, share)
    logits = mm(tok_ref[...], rw_ref[...], NN)
    ids = ids_ref[...]
    lane = iota((n_tok, experts), 1)
    hit = lane == ids[:, 0:1]
    for k in range(1, ids.shape[1]):
        hit = hit | (lane == ids[:, k : k + 1])
    mask = hit.astype(F32)
    top = jnp.max(jnp.where(hit, logits, -jnp.inf), axis=1, keepdims=True)
    weight = jnp.where(hit, jnp.exp(jnp.where(hit, logits - top, 0.0)), 0.0)
    gate = weight / jnp.sum(weight, axis=1, keepdims=True)
    earlier = (iota((n_tok, n_tok), 1) < iota((n_tok, n_tok), 0)).astype(BF16)
    rank = mm(earlier, mask.astype(BF16), NN)
    code = mask * (rank + 1.0)
    code_ref[...] = code
    gate_ref[...] = gate
    expand = spread(experts, cap)
    rows = experts * cap
    code_of = mm(expand.astype(BF16), code.astype(BF16), NT)
    pick = code_of == (iota((rows, n_tok), 0) % cap + 1).astype(F32)
    gate_of = jnp.where(pick, mm(expand, gate, NT, HI), 0.0)
    send_ref[:, :share] = mm(pick.astype(F32).astype(BF16), tok_ref[:, pl.ds(start, share)], NN).astype(BF16)
    cot = og_ref[:, pl.ds(start, share)].astype(F32)
    send_ref[:, share:] = mm(gate_of, cot, NN, HI).astype(BF16)


def expert_kernel(cap, tp_ref, own_ref, prev_ref, next_ref, far0_ref, far1_ref, wg_ref, wu_ref, wd_ref,
                  hid_ref, dg_ref, du_ref, score_ref):
    share = own_ref.shape[1] // 2
    rows = own_ref.shape[0]
    half = rows // 2
    me = tp_ref[0]

    def terms(x, at, off):
        start = pl.multiple_of(lax.rem(me + off, 4) * share, share)
        wg = wg_ref[pl.ds(start, share), :]
        wu = wu_ref[pl.ds(start, share), :]
        wd = wd_ref[:, pl.ds(start, share)]
        t = x[at, :share]
        return (mm(t, wg, NN), mm(t, wu, NN), mm(x[at, share:], wd, NT))

    for h in range(2):
        at = pl.ds(h * half, half)
        far = far0_ref if h == 0 else far1_ref
        parts = [terms(own_ref, at, 0), terms(prev_ref, at, 3), terms(next_ref, at, 1),
                 terms(far, pl.ds(0, half), 2)]
        gate_pre = sum(p[0] for p in parts)
        up_pre = sum(p[1] for p in parts)
        back = sum(p[2] for p in parts)
        glu = jnp.minimum(gate_pre, 7.0)
        linear = jnp.clip(up_pre, -7.0, 7.0)
        sig = jax.nn.sigmoid(1.702 * glu)
        act = glu * sig
        hidden = (linear + 1.0) * act
        slope = (linear + 1.0) * (sig + 1.702 * glu * sig * (1.0 - sig))
        slope = jnp.where(gate_pre < 7.0, slope, 0.0)
        up_slope = jnp.where((up_pre > -7.0) & (up_pre < 7.0), act, 0.0)
        hid_ref[at, :] = hidden.astype(BF16)
        dg_ref[at, :] = (back * slope).astype(BF16)
        du_ref[at, :] = (back * up_slope).astype(BF16)
        score = jnp.sum(hidden * back, axis=1, keepdims=True)
        peers = half // cap
        spot = (iota((half, 128), 0) % cap == iota((half, 128), 1)).astype(F32) * score
        group = (iota((peers, half), 1) // cap == iota((peers, half), 0)).astype(F32)
        score_ref[h * peers : (h + 1) * peers, :] = mm(group, spot, NN, HI)


def token_kernel(tp_ref, dg_ref, du_ref, wg_ref, wu_ref, b0_ref, b1_ref, b2_ref, b3_ref):
    share = b0_ref.shape[1]
    me = tp_ref[0]
    dg, du = dg_ref[...], du_ref[...]
    for off, out in ((2, b2_ref), (1, b1_ref), (3, b3_ref), (0, b0_ref)):
        start = pl.multiple_of(lax.rem(me + off, 4) * share, share)
        part = mm(dg, wg_ref[pl.ds(start, share), :], NT) + mm(du, wu_ref[pl.ds(start, share), :], NT)
        out[...] = part.astype(out.dtype)


def weight_kernel(tp_ref, own_ref, prev_ref, next_ref, far0_ref, far1_ref, hid_ref, dg_ref, du_ref,
                  gwg_ref, gwu_ref, gwd_ref):
    share = own_ref.shape[1] // 2
    half = own_ref.shape[0] // 2
    me = tp_ref[0]
    dg, du, hid = dg_ref[...], du_ref[...], hid_ref[...]
    for off, x in ((0, own_ref), (3, prev_ref), (1, next_ref), (2, None)):
        start = pl.multiple_of(lax.rem(me + off, 4) * share, share)
        if x is None:
            t = jnp.concatenate([far0_ref[:, :share], far1_ref[:, :share]], axis=0)
            g = jnp.concatenate([far0_ref[:, share:], far1_ref[:, share:]], axis=0)
        else:
            t = x[:, :share]
            g = x[:, share:]
        gwg_ref[pl.ds(start, share), :] = mm(t, dg, TN).astype(BF16)
        gwu_ref[pl.ds(start, share), :] = mm(t, du, TN).astype(BF16)
        gwd_ref[:, pl.ds(start, share)] = mm(hid, g, TN).astype(BF16)


def router_kernel(cap, tp_ref, q_ref, code_ref, gate_ref, tok_ref, rw_ref, part_ref, term_ref):
    share = part_ref.shape[1]
    start = pl.multiple_of(tp_ref[0] * share, share)
    code, gate = code_ref[...], gate_ref[...]
    q = q_ref[...].T
    score = jnp.zeros_like(code)
    for r in range(cap):
        score = score + jnp.where(code == r + 1.0, q[r : r + 1, :], 0.0)
    d_logits = score - gate * jnp.sum(score, axis=1, keepdims=True)
    part_ref[...] = mm(d_logits, rw_ref[pl.ds(start, share), :].astype(F32), NT, HI)
    term = mm(d_logits, tok_ref[:, pl.ds(start, share)].astype(F32), TN, HI)
    high = term.astype(BF16)
    low = (term - high.astype(F32)).astype(BF16)
    pieces = share // 128
    for j in range(pieces):
        term_ref[:, j, :] = high[:, j * 128 : (j + 1) * 128]
        term_ref[:, pieces + j, :] = low[:, j * 128 : (j + 1) * 128]


def home_kernel(cap, home_ref, code_ref, part_ref, tok_out_ref, router_ref):
    share = part_ref.shape[1]
    code = code_ref[...]
    n_tok, experts = code.shape
    rows = experts * cap
    code_of = mm(code.astype(BF16), spread(experts, cap).astype(BF16), NT)
    pick = code_of == (iota((n_tok, rows), 1) % cap + 1).astype(F32)
    flat = home_ref[...].reshape(rows, home_ref.shape[2])
    tok_out_ref[...] = (
        mm(pick.astype(F32).astype(BF16), flat[:, :share], NN) + part_ref[...]
    ).astype(BF16)
    both = jnp.sum(home_ref[:, :, share:].astype(F32), axis=0)
    pieces = share // 128
    router_ref[...] = both[:pieces] + both[pieces:]


def call(body, outs, n_in, scalar=True):
    return pl.pallas_call(
        body,
        out_shape=outs,
        in_specs=([SMEM] if scalar else []) + [VMEM] * n_in,
        out_specs=[VMEM] * len(outs),
    )


def shape(dims, dtype):
    return jax.ShapeDtypeStruct(dims, dtype)


def per_device(tokens, out_grad, expert_ids, router_weight, w_gate, w_up, w_down):
    n_tok, width = tokens.shape
    experts = router_weight.shape[1]
    peers = lax.axis_size("ep")
    tp = lax.axis_size("tp")
    cap = 8
    share = width // tp
    ff = w_gate.shape[2]
    rows = peers * cap
    half = rows // 2
    me = jnp.full((1,), lax.axis_index("tp"), jnp.int32)

    def hop(value, by):
        return lax.ppermute(value, "tp", [(i, (i + by) % tp) for i in range(tp)])

    def exchange(value):
        return lax.all_to_all(value, "ep", split_axis=0, concat_axis=0, tiled=True)

    send, code, gate = call(
        functools.partial(dispatch_kernel, cap),
        [shape((rows, 2 * share), BF16), shape((n_tok, experts), F32), shape((n_tok, experts), F32)],
        4,
    )(me, tokens, out_grad, expert_ids, router_weight)
    own = exchange(send.reshape(peers, cap, 2 * share)).reshape(rows, 2 * share)
    prev, nxt = hop(own, 1), hop(own, -1)
    far0, far1 = hop(prev[:half], 1), hop(nxt[half:], -1)
    wg, wu, wd = w_gate[0], w_up[0], w_down[0]
    hid, dg, du, score = call(
        functools.partial(expert_kernel, cap),
        [shape((rows, ff), BF16)] * 3 + [shape((peers, 128), F32)],
        8,
    )(me, own, prev, nxt, far0, far1, wg, wu, wd)
    b0, b1, b2, b3 = call(
        token_kernel,
        [shape((rows, share), F32), shape((rows, share), F32), shape((rows, share), BF16),
         shape((rows, share), F32)],
        4,
    )(me, dg, du, wg, wu)
    score = score + hop(score, 1) + hop(score, -1) + hop(score, 2)
    s1, s2 = hop(b2[:half], 1), hop(b2[half:], -1)
    up = jnp.concatenate([b1[:half] + s1.astype(F32), b1[half:]], axis=0).astype(BF16)
    down = jnp.concatenate([b3[:half], b3[half:] + s2.astype(F32)], axis=0).astype(BF16)
    r1, r2 = hop(up, 1), hop(down, -1)
    summed = (b0 + r1.astype(F32) + r2.astype(F32)).astype(BF16)
    gwg, gwu, gwd = call(
        weight_kernel,
        [shape((width, ff), BF16), shape((width, ff), BF16), shape((ff, width), BF16)],
        8,
    )(me, own, prev, nxt, far0, far1, hid, dg, du)
    q = exchange(score.reshape(peers, 1, 128)).reshape(peers, 128)
    part, term = call(
        functools.partial(router_kernel, cap),
        [shape((n_tok, share), F32), shape((peers, cap, 128), BF16)],
        5,
    )(me, q, code, gate, tokens, router_weight)
    payload = jnp.concatenate([summed.reshape(peers, cap, share), term], axis=2)
    home = exchange(payload)
    token_grad, router = call(
        functools.partial(home_kernel, cap),
        [shape((n_tok, share), BF16), shape((share // 128, 128), F32)],
        3,
        scalar=False,
    )(home, code, part)
    return (token_grad, router.reshape(share, 1), gwg[None], gwu[None], gwd[None])


def solution(mesh):
    in_specs = (
        P("ep", None),
        P("ep", None),
        P("ep", None),
        P(),
        P("ep", None, "tp"),
        P("ep", None, "tp"),
        P("ep", "tp", None),
    )
    out_specs = (
        P("ep", "tp"),
        P("tp", "ep"),
        P("ep", None, "tp"),
        P("ep", None, "tp"),
        P("ep", "tp", None),
    )
    return jax.shard_map(
        per_device, mesh=mesh, in_specs=in_specs, out_specs=out_specs, check_vma=False
    )
```

time: 255 us -> 180 us (0.71)
  local copies, waits for them, and re-layouts: 38 us -> 7.27 us
  Pallas kernels: 0 us -> 30.5 us
  matrix products: 24.2 us -> 0 us
  waiting for transfers between devices: 76.3 us -> 56.3 us
  between operations: 14.6 us -> 0.82 us
  other arithmetic: 9.56 us -> 1.33 us
  starting transfers between devices: 26.8 us -> 19.4 us
    all_to_all x4 -> x1, waiting for transfers between devices: 58.3 us -> 13.1 us  [exchange(): return lax.all_to_all(value, 'ep', split_axis=0, concat_axis=0, tiled=True)]
    ppermute x0 -> x11, waiting for transfers between devices: none -> 43.2 us  [hop(): return lax.ppermute(value, 'tp', [(i, (i + by) % tp) for i in range(tp)])]
    pallas_call x0 -> x6, Pallas kernels: none -> 30.5 us  [the longest x1 8.7 us: per_device(): call(functools.partial(expert_kernel, cap), [shape((rows, ff), BF16)] * 3...]
    dot_general x11 -> x0, matrix products: 24.2 us -> none  [the longest x3 11.9 us: contract_first(): lax.dot_general(left, right, (((0,), (0,)), ((), ())), preferred_element_...]
    all_to_all x4 -> x1, starting transfers between devices: 26.7 us -> 4.55 us  [exchange(): return lax.all_to_all(value, 'ep', split_axis=0, concat_axis=0, tiled=True)]
    all_gather x1 -> x0, waiting for transfers between devices: 17.9 us -> none  [side_by_side_2(): lax.all_gather(both, axis, axis=dim, tiled=True)]
    ppermute x0 -> x11, starting transfers between devices: none -> 14.8 us  [hop(): return lax.ppermute(value, 'tp', [(i, (i + by) % tp) for i in range(tp)])]
    scatter x3 -> x0, local copies, waits for them, and re-layouts: 14.1 us -> none  [the longest x2 12.9 us: per_device(): jnp.zeros((buffer_rows, model_width), jnp.bfloat16).at[slot_index]]
  transfers between devices with their start and end apart: 5 -> 12, of which waited for: 4 -> 7; matrix products, arithmetic and copies ran while one was open for 9% -> 1% of each run, Pallas kernels for 0% -> 6%
where the time goes in v1:
time: 180 us
  blocking collectives  64.2 us (36%)
  waiting for transfers between devices  56.3 us (31%)
  Pallas kernels  30.5 us (17%)
  starting transfers between devices  19.4 us (11%)
  local copies, waits for them, and re-layouts  7.27 us (4%)
    all_to_all x2, blocking collectives, exchange(): return lax.all_to_all(value, 'ep', split_axis=0, concat_axis=0, tiled=True)  64.2 us
    ppermute x11, waiting for transfers between devices, hop(): return lax.ppermute(value, 'tp', [(i, (i + by) % tp) for i in range(tp)])  43.2 us
    ppermute x11, starting transfers between devices, hop(): return lax.ppermute(value, 'tp', [(i, (i + by) % tp) for i in range(tp)])  14.8 us
    all_to_all x1, waiting for transfers between devices, exchange(): return lax.all_to_all(value, 'ep', split_axis=0, concat_axis=0, tiled=True)  13.1 us
    pallas_call x1, Pallas kernels, per_device(): call(functools.partial(expert_kernel, cap), [shape((rows, ff), BF16)] * 3...  8.7 us
    pallas_call x1, Pallas kernels, per_device(): call(weight_kernel, [shape((width, ff), BF16), shape((width, ff), BF16),...  7.4 us
    pallas_call x1, Pallas kernels, per_device(): call(token_kernel, [shape((rows, share), F32), shape((rows, share), F32),...  5.47 us
    unnamed x20, local copies, waits for them, and re-layouts  4.88 us
  transfers between devices with their start and end apart: 12, of which 7 were waited for; matrix products, arithmetic and copies ran while one was open for 1% of the time, Pallas kernels for 6%

profile of v1, /device:TPU:1, one launch (start us, length us, event | category | flops | bytes accessed | tf_op | source)
XLA Modules:
  0.0 179.7 jit_solution(8792324903190826039)
XLA Ops:
  0.6 1.4 copy.15.ids_ref
  2.0 2.0 %copy.16.rw_ref = bf16[2048,64]{1,0:T(8,128)(2,1)} copy(bf16[2048,64]{0,1:T(8,128)(2,1)} %param.10) | data formatting | bytes 524288 | tf_op args[3]
  4.0 4.0 %shard_map.110 = (bf16[512,1024]{1,0:T(8,128)(2,1)}, f32[48,64]{1,0:T(8,128)}, f32[48,64]{1,0:T(8,128)}) custom-call(s32[1]{0:T(128)} %bitcast.tp_ref, bf16[48,2048]{1,0:T(8,128)(2,1)} %tok_ref.3, bf16[48,2048]{1,0:T(8,128)(2,1)} %og_ref.1, s32[48,4]{1,0:T(8,128)} %copy.15.ids_ref, bf16[2048,64]{1,0:T(8,128)(2,1)} %copy.16.rw_ref), custom_call_target="tpu_custom_call" | custom-call | tf_op jit(solution)/shard_map/pallas_call | solution.py:201
  8.0 41.3 %all_to_all.15 = bf16[64,8,1024]{2,1,0:T(8,128)(2,1)S(1)} all-to-all(bf16[64,8,1024]{2,1,0:T(8,128)(2,1)} %bitcast.25), channel_id=1, replica_groups=mesh['ep'=64,'tp'=4] {'ep'}, dimensions={0} | all-to-all | bytes 2097152 | tf_op jit(solution)/shard_map/all_to_all | solution.py:199
  49.3 1.2 collective-permute-start
  50.5 1.5 collective-permute-start.1
  52.0 22.1 %collective-permute-done.prev_ref = bf16[512,1024]{1,0:T(8,128)(2,1)S(1)} collective-permute-done((bf16[512,1024]{1,0:T(8,128)(2,1)S(1)}, bf16[512,1024]{1,0:T(8,128)(2,1)S(1)}, u32[]{:S(2)}, u32[]{:S(2)}) %collective-permute-start) | collective-permute-done | bytes 1048608 | tf_op jit(solution)/shard_map/ppermute | solution.py:196
  74.3 2.7 %collective-permute-start.3 = (bf16[256,1024]{1,0:T(8,128)(2,1)S(1)}, bf16[256,1024]{1,0:T(8,128)(2,1)}, u32[]{:S(2)}, u32[]{:S(2)}) collective-permute-start(bf16[256,1024]{1,0:T(8,128)(2,1)S(1)} %slice.35), channel_id=1, source_target_pairs={{0,3},{1,0},{2,1},{3,2},{4,7},{5,4},{6,5},{7,6},{8,11},{9,8},{10,9... | collective-permute-start | bytes 1572872 | tf_op jit(solution)/shard_map/ppermute | solution.py:196
  77.0 10.0 %collective-permute-done.2.far0_ref = bf16[256,1024]{1,0:T(8,128)(2,1)} collective-permute-done((bf16[256,1024]{1,0:T(8,128)(2,1)S(1)}, bf16[256,1024]{1,0:T(8,128)(2,1)}, u32[]{:S(2)}, u32[]{:S(2)}) %collective-permute-start.2) | collective-permute-done | bytes 524320 | tf_op jit(solution)/shard_map/ppermute | solution.py:196
  87.0 8.7 %shard_map.111 = (bf16[512,384]{1,0:T(8,128)(2,1)}, bf16[512,384]{1,0:T(8,128)(2,1)}, bf16[512,384]{1,0:T(8,128)(2,1)}, f32[64,128]{1,0:T(8,128)}) custom-call(s32[1]{0:T(128)} %bitcast.tp_ref, bf16[512,1024]{1,0:T(8,128)(2,1)} %bitcast.18, bf16[512,1024]{1,0:T(8,128)(2,1)} %copy-done.1, bf16[512,1024]{1,0:T(8,128)(2,1)} %copy-done.2, ...), custom_call_target="tpu_custom_call" | custom-call | tf_op jit(solution)/shard_map/pallas_call | solution.py:210
  95.7 5.5 %shard_map.112 = (f32[512,512]{1,0:T(8,128)}, f32[512,512]{1,0:T(8,128)}, bf16[512,512]{1,0:T(8,128)(2,1)}, f32[512,512]{1,0:T(8,128)}) custom-call(s32[1]{0:T(128)} %bitcast.tp_ref, bf16[512,384]{1,0:T(8,128)(2,1)} %get-tuple-element.24.dg_ref, bf16[512,384]{1,0:T(8,128)(2,1)} %get-tuple-element.25.du_ref, bf16[2048,384]{1,0:T(8,128)(2,1)} %bitcast.21, ...), custom_call_target="tpu_custom_call" | custom-call | tf_op jit(solution)/shard_map/pallas_call | solution.py:215
  101.2 1.2 fusion.1
  102.4 2.6 %collective-permute-start.6 = (bf16[256,512]{1,0:T(8,128)(2,1)S(1)}, bf16[256,512]{1,0:T(8,128)(2,1)S(1)}, u32[]{:S(2)}, u32[]{:S(2)}) collective-permute-start(bf16[256,512]{1,0:T(8,128)(2,1)S(1)} %get-tuple-element.42), channel_id=1, source_target_pairs={{0,3},{1,0},{2,1},{3,2},{4,7},{5,4},{6,5},{7,6},{8,11},{9,8},{10,9... | collective-permute-start | bytes 786440 | tf_op jit(solution)/shard_map/ppermute | solution.py:196
  106.4 1.9 %collective-permute-done.6 = bf16[256,512]{1,0:T(8,128)(2,1)S(1)} collective-permute-done((bf16[256,512]{1,0:T(8,128)(2,1)S(1)}, bf16[256,512]{1,0:T(8,128)(2,1)S(1)}, u32[]{:S(2)}, u32[]{:S(2)}) %collective-permute-start.6) | collective-permute-done | bytes 262176 | tf_op jit(solution)/shard_map/ppermute | solution.py:196
  108.5 3.2 %collective-permute-start.7 = (bf16[512,512]{1,0:T(8,128)(2,1)S(1)}, bf16[512,512]{1,0:T(8,128)(2,1)S(1)}, u32[]{:S(2)}, u32[]{:S(2)}) collective-permute-start(bf16[512,512]{1,0:T(8,128)(2,1)S(1)} %pad_maximum_fusion.2), channel_id=1, source_target_pairs={{0,3},{1,0},{2,1},{3,2},{4,7},{5,4},{6,5},{7,6},{8,11},{9,8},{10,9... | collective-permute-start | bytes 1572872 | tf_op jit(solution)/shard_map/ppermute | solution.py:196
  113.8 1.9 %collective-permute-start.9 = (f32[64,128]{1,0:T(8,128)S(1)}, f32[64,128]{1,0:T(8,128)S(1)}, u32[]{:S(2)}, u32[]{:S(2)}) collective-permute-start(f32[64,128]{1,0:T(8,128)S(1)} %copy-done.8), channel_id=1, source_target_pairs={{0,3},{1,0},{2,1},{3,2},{4,7},{5,4},{6,5},{7,6},{8,11},{9,8},{10,9... | collective-permute-start | bytes 98312 | tf_op jit(solution)/shard_map/ppermute | solution.py:196
  116.3 6.1 %collective-permute-done.10 = f32[64,128]{1,0:T(8,128)S(1)} collective-permute-done((f32[64,128]{1,0:T(8,128)S(1)}, f32[64,128]{1,0:T(8,128)S(1)}, u32[]{:S(2)}, u32[]{:S(2)}) %collective-permute-start.10) | collective-permute-done | bytes 32800 | tf_op jit(solution)/shard_map/ppermute | solution.py:196
  122.4 1.9 %collective-permute-done.8 = f32[64,128]{1,0:T(8,128)S(1)} collective-permute-done((f32[64,128]{1,0:T(8,128)S(1)}, f32[64,128]{1,0:T(8,128)S(1)}, u32[]{:S(2)}, u32[]{:S(2)}) %collective-permute-start.8) | collective-permute-done | bytes 32800 | tf_op jit(solution)/shard_map/ppermute | solution.py:196
  124.3 22.9 %all_to_all.16 = f32[64,1,128]{2,1,0:T(1,128)} all-to-all(f32[64,1,128]{2,1,0:T(1,128)S(1)} %bitcast.27), channel_id=1, replica_groups=mesh['ep'=64,'tp'=4] {'ep'}, dimensions={0} | all-to-all | bytes 65536 | tf_op jit(solution)/shard_map/all_to_all | solution.py:199
  147.2 2.8 %shard_map.113 = (f32[48,512]{1,0:T(8,128)}, bf16[64,8,128]{2,1,0:T(8,128)(2,1)}) custom-call(s32[1]{0:T(128)} %bitcast.tp_ref, f32[64,128]{1,0:T(8,128)} %bitcast.26, f32[48,64]{1,0:T(8,128)} %get-tuple-element.31.code_ref, f32[48,64]{1,0:T(8,128)} %get-tuple-element.32.gate_ref, bf16[48,2048]{1,0:T(8,128)(2,1)} %tok_ref.3, bf16[2048,64]{1,0:T(8,128)(2,1)} %copy.16.rw_ref), custom_call_target="tpu_custom_call" | custom-call | tf_op jit(solution)/shard_map/pallas_call | solution.py:233
  151.8 4.5 %all-to-all-start.2 = ((bf16[64,8,640]{2,1,0:T(8,128)(2,1)}), bf16[64,8,640]{2,1,0:T(8,128)(2,1)S(1)}, u32[]{:S(2)}, u32[]{:S(2)}) async-start(bf16[64,8,640]{2,1,0:T(8,128)(2,1)} %pad_maximum_fusion), calls=%async_computation.2 | async-start | bytes 1310720 | tf_op jit(solution)/shard_map/all_to_all | solution.py:199
  156.3 7.4 %shard_map.115 = (bf16[2048,384]{1,0:T(8,128)(2,1)}, bf16[2048,384]{1,0:T(8,128)(2,1)}, bf16[384,2048]{1,0:T(8,128)(2,1)}) custom-call(s32[1]{0:T(128)} %bitcast.tp_ref, bf16[512,1024]{1,0:T(8,128)(2,1)} %bitcast.19, bf16[512,1024]{1,0:T(8,128)(2,1)} %copy-done.1, bf16[512,1024]{1,0:T(8,128)(2,1)} %copy-done.2, ...), custom_call_target="tpu_custom_call" | custom-call | tf_op jit(solution)/shard_map/pallas_call | solution.py:227
  163.7 13.1 %all-to-all-done.2.home_ref = bf16[64,8,640]{2,1,0:T(8,128)(2,1)S(1)} async-done(((bf16[64,8,640]{2,1,0:T(8,128)(2,1)}), bf16[64,8,640]{2,1,0:T(8,128)(2,1)S(1)}, u32[]{:S(2)}, u32[]{:S(2)}) %all-to-all-start.2) | async-done | bytes 655392 | tf_op jit(solution)/shard_map/all_to_all | solution.py:199
  177.7 2.1 %shard_map.114 = (bf16[48,512]{1,0:T(8,128)(2,1)}, f32[4,128]{1,0:T(4,128)}) custom-call(bf16[64,8,640]{2,1,0:T(8,128)(2,1)} %copy-done.3, f32[48,64]{1,0:T(8,128)} %get-tuple-element.31.code_ref, f32[48,512]{1,0:T(8,128)} %get-tuple-element.34.part_ref), custom_call_target="tpu_custom_call" | custom-call | tf_op jit(solution)/shard_map/pallas_call | solution.py:240
  (40 shorter events, 7.0 us)
Async XLA Ops:
  49.3 37.7 %copy-start = (bf16[64,8,1024]{2,1,0:T(8,128)(2,1)}, bf16[64,8,1024]{2,1,0:T(8,128)(2,1)S(1)}, u32[]{:S(2)}) copy-start(bf16[64,8,1024]{2,1,0:T(8,128)(2,1)S(1)} %all_to_all.15) | copy-start | bytes 3145732
  49.3 24.8 %collective-permute-start = (bf16[512,1024]{1,0:T(8,128)(2,1)S(1)}, bf16[512,1024]{1,0:T(8,128)(2,1)S(1)}, u32[]{:S(2)}, u32[]{:S(2)}) collective-permute-start(bf16[512,1024]{1,0:T(8,128)(2,1)S(1)} %bitcast.16), channel_id=1, source_target_pairs={{0,1},{1,2},{2,3},{3,0},{4,5},{5,6},{6,7},{7,4},{8,9},{9,10},{10,1... | collective-permute-start | bytes 3145736 | tf_op jit(solution)/shard_map/ppermute | solution.py:196
  50.5 23.7 %collective-permute-start.1 = (bf16[512,1024]{1,0:T(8,128)(2,1)S(1)}, bf16[512,1024]{1,0:T(8,128)(2,1)S(1)}, u32[]{:S(2)}, u32[]{:S(2)}) collective-permute-start(bf16[512,1024]{1,0:T(8,128)(2,1)S(1)} %bitcast.17), channel_id=1, source_target_pairs={{0,3},{1,0},{2,1},{3,2},{4,7},{5,4},{6,5},{7,6},{8,11},{9,8},{10,9... | collective-permute-start | bytes 3145736 | tf_op jit(solution)/shard_map/ppermute | solution.py:196
  74.1 12.9 %copy-start.1 = (bf16[512,1024]{1,0:T(8,128)(2,1)}, bf16[512,1024]{1,0:T(8,128)(2,1)S(1)}, u32[]{:S(2)}) copy-start(bf16[512,1024]{1,0:T(8,128)(2,1)S(1)} %collective-permute-done.prev_ref) | copy-start | bytes 3145732
  74.1 12.9 %collective-permute-start.2 = (bf16[256,1024]{1,0:T(8,128)(2,1)S(1)}, bf16[256,1024]{1,0:T(8,128)(2,1)}, u32[]{:S(2)}, u32[]{:S(2)}) collective-permute-start(bf16[256,1024]{1,0:T(8,128)(2,1)S(1)} %slice.34), channel_id=1, source_target_pairs={{0,1},{1,2},{2,3},{3,0},{4,5},{5,6},{6,7},{7,4},{8,9},{9,10},{10,1... | collective-permute-start | bytes 1572872 | tf_op jit(solution)/shard_map/ppermute | solution.py:196
  74.2 12.8 %copy-start.2 = (bf16[512,1024]{1,0:T(8,128)(2,1)}, bf16[512,1024]{1,0:T(8,128)(2,1)S(1)}, u32[]{:S(2)}) copy-start(bf16[512,1024]{1,0:T(8,128)(2,1)S(1)} %collective-permute-done.1.next_ref) | copy-start | bytes 3145732
  74.3 12.7 %collective-permute-start.3 = (bf16[256,1024]{1,0:T(8,128)(2,1)S(1)}, bf16[256,1024]{1,0:T(8,128)(2,1)}, u32[]{:S(2)}, u32[]{:S(2)}) collective-permute-start(bf16[256,1024]{1,0:T(8,128)(2,1)S(1)} %slice.35), channel_id=1, source_target_pairs={{0,3},{1,0},{2,1},{3,2},{4,7},{5,4},{6,5},{7,6},{8,11},{9,8},{10,9... | collective-permute-start | bytes 1572872 | tf_op jit(solution)/shard_map/ppermute | solution.py:196
  101.2 4.9 %copy-start.5 = (f32[512,512]{1,0:T(8,128)S(1)}, f32[512,512]{1,0:T(8,128)}, u32[]{:S(2)}) copy-start(f32[512,512]{1,0:T(8,128)} %get-tuple-element.27) | copy-start | bytes 3145732
  101.2 7.1 %copy-start.6 = (f32[512,512]{1,0:T(8,128)S(1)}, f32[512,512]{1,0:T(8,128)}, u32[]{:S(2)}) copy-start(f32[512,512]{1,0:T(8,128)} %get-tuple-element.29) | copy-start | bytes 3145732
  102.4 5.9 %collective-permute-start.6 = (bf16[256,512]{1,0:T(8,128)(2,1)S(1)}, bf16[256,512]{1,0:T(8,128)(2,1)S(1)}, u32[]{:S(2)}, u32[]{:S(2)}) collective-permute-start(bf16[256,512]{1,0:T(8,128)(2,1)S(1)} %get-tuple-element.42), channel_id=1, source_target_pairs={{0,3},{1,0},{2,1},{3,2},{4,7},{5,4},{6,5},{7,6},{8,11},{9,8},{10,9... | collective-permute-start | bytes 786440 | tf_op jit(solution)/shard_map/ppermute | solution.py:196
  106.1 6.7 %collective-permute-start.4 = (bf16[256,512]{1,0:T(8,128)(2,1)S(1)}, bf16[256,512]{1,0:T(8,128)(2,1)S(1)}, u32[]{:S(2)}, u32[]{:S(2)}) collective-permute-start(bf16[256,512]{1,0:T(8,128)(2,1)S(1)} %get-tuple-element.41), channel_id=1, source_target_pairs={{0,1},{1,2},{2,3},{3,0},{4,5},{5,6},{6,7},{7,4},{8,9},{9,10},{10,1... | collective-permute-start | bytes 786440 | tf_op jit(solution)/shard_map/ppermute | solution.py:196
  108.4 4.6 %copy-start.8 = (f32[64,128]{1,0:T(8,128)S(1)}, f32[64,128]{1,0:T(8,128)}, u32[]{:S(2)}) copy-start(f32[64,128]{1,0:T(8,128)} %get-tuple-element.30) | copy-start | bytes 98308
  108.5 41.5 %copy-start.4 = (f32[512,512]{1,0:T(8,128)S(1)}, f32[512,512]{1,0:T(8,128)}, u32[]{:S(2)}) copy-start(f32[512,512]{1,0:T(8,128)} %get-tuple-element.26) | copy-start | bytes 3145732
  108.5 41.5 %collective-permute-start.7 = (bf16[512,512]{1,0:T(8,128)(2,1)S(1)}, bf16[512,512]{1,0:T(8,128)(2,1)S(1)}, u32[]{:S(2)}, u32[]{:S(2)}) collective-permute-start(bf16[512,512]{1,0:T(8,128)(2,1)S(1)} %pad_maximum_fusion.2), channel_id=1, source_target_pairs={{0,3},{1,0},{2,1},{3,2},{4,7},{5,4},{6,5},{7,6},{8,11},{9,8},{10,9... | collective-permute-start | bytes 1572872 | tf_op jit(solution)/shard_map/ppermute | solution.py:196
  113.0 37.0 %collective-permute-start.5 = (bf16[512,512]{1,0:T(8,128)(2,1)S(1)}, bf16[512,512]{1,0:T(8,128)(2,1)S(1)}, u32[]{:S(2)}, u32[]{:S(2)}) collective-permute-start(bf16[512,512]{1,0:T(8,128)(2,1)S(1)} %pad_maximum_fusion.1), channel_id=1, source_target_pairs={{0,1},{1,2},{2,3},{3,0},{4,5},{5,6},{6,7},{7,4},{8,9},{9,10},{10,1... | collective-permute-start | bytes 1572872 | tf_op jit(solution)/shard_map/ppermute | solution.py:196
  113.1 9.4 %collective-permute-start.10 = (f32[64,128]{1,0:T(8,128)S(1)}, f32[64,128]{1,0:T(8,128)S(1)}, u32[]{:S(2)}, u32[]{:S(2)}) collective-permute-start(f32[64,128]{1,0:T(8,128)S(1)} %copy-done.8), channel_id=1, source_target_pairs={{0,2},{1,3},{2,0},{3,1},{4,6},{5,7},{6,4},{7,5},{8,10},{9,11},{10,... | collective-permute-start | bytes 98312 | tf_op jit(solution)/shard_map/ppermute | solution.py:196
  113.8 8.6 %collective-permute-start.9 = (f32[64,128]{1,0:T(8,128)S(1)}, f32[64,128]{1,0:T(8,128)S(1)}, u32[]{:S(2)}, u32[]{:S(2)}) collective-permute-start(f32[64,128]{1,0:T(8,128)S(1)} %copy-done.8), channel_id=1, source_target_pairs={{0,3},{1,0},{2,1},{3,2},{4,7},{5,4},{6,5},{7,6},{8,11},{9,8},{10,9... | collective-permute-start | bytes 98312 | tf_op jit(solution)/shard_map/ppermute | solution.py:196
  115.7 8.6 %collective-permute-start.8 = (f32[64,128]{1,0:T(8,128)S(1)}, f32[64,128]{1,0:T(8,128)S(1)}, u32[]{:S(2)}, u32[]{:S(2)}) collective-permute-start(f32[64,128]{1,0:T(8,128)S(1)} %copy-done.8), channel_id=1, source_target_pairs={{0,1},{1,2},{2,3},{3,0},{4,5},{5,6},{6,7},{7,4},{8,9},{9,10},{10,1... | collective-permute-start | bytes 98312 | tf_op jit(solution)/shard_map/ppermute | solution.py:196
  150.0 0.9 copy-start.7
  151.8 25.0 %all-to-all-start.2 = ((bf16[64,8,640]{2,1,0:T(8,128)(2,1)}), bf16[64,8,640]{2,1,0:T(8,128)(2,1)S(1)}, u32[]{:S(2)}, u32[]{:S(2)}) async-start(bf16[64,8,640]{2,1,0:T(8,128)(2,1)} %pad_maximum_fusion), calls=%async_computation.2 | async-start | bytes 1310720 | tf_op jit(solution)/shard_map/all_to_all | solution.py:199
  176.8 0.8 copy-start.3

commit v2 on v1

--- a/solution.py
+++ b/solution.py
@@ -33,13 +33,13 @@
 
 
 def dispatch_kernel(cap, tp_ref, tok_ref, og_ref, ids_ref, rw_ref, send_ref, code_ref, gate_ref):
-    n_tok, width = tok_ref.shape
-    experts = rw_ref.shape[1]
+    n_tok = tok_ref.shape[0]
+    experts = rw_ref.shape[0]
     share = send_ref.shape[1] // 2
     start = pl.multiple_of(tp_ref[0] * share, share)
-    logits = mm(tok_ref[...], rw_ref[...], NN)
-    ids = ids_ref[...]
-    lane = iota((n_tok, experts), 1)
+    logits = mm(tok_ref[...], rw_ref[...], NT)
+    ids = ids_ref[...].astype(F32).T
+    lane = iota((n_tok, experts), 1).astype(F32)
     hit = lane == ids[:, 0:1]
     for k in range(1, ids.shape[1]):
         hit = hit | (lane == ids[:, k : k + 1])
@@ -62,29 +62,36 @@
     send_ref[:, share:] = mm(gate_of, cot, NN, HI).astype(BF16)
 
 
-def expert_kernel(cap, tp_ref, own_ref, prev_ref, next_ref, far0_ref, far1_ref, wg_ref, wu_ref, wd_ref,
-                  hid_ref, dg_ref, du_ref, score_ref):
+def near_kernel(tp_ref, own_ref, p0_ref, p1_ref, n0_ref, n1_ref, wg_ref, wu_ref, wd_ref, gp_ref, up_ref, bk_ref):
     share = own_ref.shape[1] // 2
-    rows = own_ref.shape[0]
-    half = rows // 2
+    half = own_ref.shape[0] // 2
     me = tp_ref[0]
-
-    def terms(x, at, off):
-        start = pl.multiple_of(lax.rem(me + off, 4) * share, share)
-        wg = wg_ref[pl.ds(start, share), :]
-        wu = wu_ref[pl.ds(start, share), :]
-        wd = wd_ref[:, pl.ds(start, share)]
-        t = x[at, :share]
-        return (mm(t, wg, NN), mm(t, wu, NN), mm(x[at, share:], wd, NT))
-
     for h in range(2):
         at = pl.ds(h * half, half)
-        far = far0_ref if h == 0 else far1_ref
-        parts = [terms(own_ref, at, 0), terms(prev_ref, at, 3), terms(next_ref, at, 1),
-                 terms(far, pl.ds(0, half), 2)]
-        gate_pre = sum(p[0] for p in parts)
-        up_pre = sum(p[1] for p in parts)
-        back = sum(p[2] for p in parts)
+        blocks = ((0, own_ref[at, :]), (3, (p0_ref, p1_ref)[h][...]), (1, (n0_ref, n1_ref)[h][...]))
+        gp, up, bk = [], [], []
+        for off, x in blocks:
+            start = pl.multiple_of(lax.rem(me + off, 4) * share, share)
+            gp.append(mm(x[:, :share], wg_ref[pl.ds(start, share), :], NN))
+            up.append(mm(x[:, :share], wu_ref[pl.ds(start, share), :], NN))
+            bk.append(mm(x[:, share:], wd_ref[:, pl.ds(start, share)], NT))
+        gp_ref[at, :] = sum(gp)
+        up_ref[at, :] = sum(up)
+        bk_ref[at, :] = sum(bk)
+
+
+def far_kernel(cap, tp_ref, far0_ref, far1_ref, wg_ref, wu_ref, wd_ref, gp_ref, up_ref, bk_ref,
+               hid_ref, dg_ref, du_ref, score_ref, b2a_ref, b2b_ref):
+    del tp_ref
+    share = far0_ref.shape[1] // 2
+    half = far0_ref.shape[0]
+    for h in range(2):
+        at = pl.ds(h * half, half)
+        far = (far0_ref, far1_ref)[h]
+        t = far[:, :share]
+        gate_pre = gp_ref[at, :] + mm(t, wg_ref[...], NN)
+        up_pre = up_ref[at, :] + mm(t, wu_ref[...], NN)
+        back = bk_ref[at, :] + mm(far[:, share:], wd_ref[...], NT)
         glu = jnp.minimum(gate_pre, 7.0)
         linear = jnp.clip(up_pre, -7.0, 7.0)
         sig = jax.nn.sigmoid(1.702 * glu)
@@ -93,40 +100,43 @@
         slope = (linear + 1.0) * (sig + 1.702 * glu * sig * (1.0 - sig))
         slope = jnp.where(gate_pre < 7.0, slope, 0.0)
         up_slope = jnp.where((up_pre > -7.0) & (up_pre < 7.0), act, 0.0)
+        dg = (back * slope).astype(BF16)
+        du = (back * up_slope).astype(BF16)
         hid_ref[at, :] = hidden.astype(BF16)
-        dg_ref[at, :] = (back * slope).astype(BF16)
-        du_ref[at, :] = (back * up_slope).astype(BF16)
+        dg_ref[at, :] = dg
+        du_ref[at, :] = du
         score = jnp.sum(hidden * back, axis=1, keepdims=True)
         peers = half // cap
         spot = (iota((half, 128), 0) % cap == iota((half, 128), 1)).astype(F32) * score
         group = (iota((peers, half), 1) // cap == iota((peers, half), 0)).astype(F32)
         score_ref[h * peers : (h + 1) * peers, :] = mm(group, spot, NN, HI)
-
-
-def token_kernel(tp_ref, dg_ref, du_ref, wg_ref, wu_ref, b0_ref, b1_ref, b2_ref, b3_ref):
+        out = (b2a_ref, b2b_ref)[h]
+        out[...] = (mm(dg, wg_ref[...], NT) + mm(du, wu_ref[...], NT)).astype(BF16)
+
+
+def token_kernel(tp_ref, dg_ref, du_ref, wg_ref, wu_ref, b0_ref, b1a_ref, b1b_ref, b3a_ref, b3b_ref):
     share = b0_ref.shape[1]
+    half = b0_ref.shape[0] // 2
     me = tp_ref[0]
-    dg, du = dg_ref[...], du_ref[...]
-    for off, out in ((2, b2_ref), (1, b1_ref), (3, b3_ref), (0, b0_ref)):
+    for off, lo, hi in ((1, b1a_ref, b1b_ref), (3, b3a_ref, b3b_ref), (0, b0_ref.at[:half], b0_ref.at[half:])):
         start = pl.multiple_of(lax.rem(me + off, 4) * share, share)
-        part = mm(dg, wg_ref[pl.ds(start, share), :], NT) + mm(du, wu_ref[pl.ds(start, share), :], NT)
-        out[...] = part.astype(out.dtype)
-
-
-def weight_kernel(tp_ref, own_ref, prev_ref, next_ref, far0_ref, far1_ref, hid_ref, dg_ref, du_ref,
+        wg, wu = wg_ref[pl.ds(start, share), :], wu_ref[pl.ds(start, share), :]
+        for h, out in ((0, lo), (1, hi)):
+            at = pl.ds(h * half, half)
+            out[...] = (mm(dg_ref[at, :], wg, NT) + mm(du_ref[at, :], wu, NT)).astype(out.dtype)
+
+
+def weight_kernel(tp_ref, own_ref, p0_ref, p1_ref, n0_ref, n1_ref, far0_ref, far1_ref, hid_ref, dg_ref, du_ref,
                   gwg_ref, gwu_ref, gwd_ref):
     share = own_ref.shape[1] // 2
     half = own_ref.shape[0] // 2
     me = tp_ref[0]
     dg, du, hid = dg_ref[...], du_ref[...], hid_ref[...]
-    for off, x in ((0, own_ref), (3, prev_ref), (1, next_ref), (2, None)):
+    for off, lo, hi in ((0, own_ref.at[:half], own_ref.at[half:]), (3, p0_ref, p1_ref), (1, n0_ref, n1_ref),
+                        (2, far0_ref, far1_ref)):
         start = pl.multiple_of(lax.rem(me + off, 4) * share, share)
-        if x is None:
-            t = jnp.concatenate([far0_ref[:, :share], far1_ref[:, :share]], axis=0)
-            g = jnp.concatenate([far0_ref[:, share:], far1_ref[:, share:]], axis=0)
-        else:
-            t = x[:, :share]
-            g = x[:, share:]
+        t = jnp.concatenate([lo[:, :share], hi[:, :share]], axis=0)
+        g = jnp.concatenate([lo[:, share:], hi[:, share:]], axis=0)
         gwg_ref[pl.ds(start, share), :] = mm(t, dg, TN).astype(BF16)
         gwu_ref[pl.ds(start, share), :] = mm(t, du, TN).astype(BF16)
         gwd_ref[:, pl.ds(start, share)] = mm(hid, g, TN).astype(BF16)
@@ -141,7 +151,7 @@
     for r in range(cap):
         score = score + jnp.where(code == r + 1.0, q[r : r + 1, :], 0.0)
     d_logits = score - gate * jnp.sum(score, axis=1, keepdims=True)
-    part_ref[...] = mm(d_logits, rw_ref[pl.ds(start, share), :].astype(F32), NT, HI)
+    part_ref[...] = mm(d_logits, rw_ref[:, pl.ds(start, share)].astype(F32), NN, HI)
     term = mm(d_logits, tok_ref[:, pl.ds(start, share)].astype(F32), TN, HI)
     high = term.astype(BF16)
     low = (term - high.astype(F32)).astype(BF16)
@@ -167,12 +177,17 @@
     router_ref[...] = both[:pieces] + both[pieces:]
 
 
-def call(body, outs, n_in, scalar=True):
+def cost(flops, data):
+    return pl.CostEstimate(flops=flops, bytes_accessed=data, transcendentals=0)
+
+
+def call(body, outs, n_in, flops, scalar=True):
     return pl.pallas_call(
         body,
         out_shape=outs,
         in_specs=([SMEM] if scalar else []) + [VMEM] * n_in,
         out_specs=[VMEM] * len(outs),
+        cost_estimate=cost(flops, 4 << 20),
     )
 
 
@@ -191,6 +206,8 @@
     rows = peers * cap
     half = rows // 2
     me = jnp.full((1,), lax.axis_index("tp"), jnp.int32)
+    unit = 2 * rows * share * ff
+    router_t = router_weight.T
 
     def hop(value, by):
         return lax.ppermute(value, "tp", [(i, (i + by) % tp) for i in range(tp)])
@@ -202,45 +219,78 @@
         functools.partial(dispatch_kernel, cap),
         [shape((rows, 2 * share), BF16), shape((n_tok, experts), F32), shape((n_tok, experts), F32)],
         4,
-    )(me, tokens, out_grad, expert_ids, router_weight)
+        unit,
+    )(me, tokens, out_grad, expert_ids.T, router_t)
     own = exchange(send.reshape(peers, cap, 2 * share)).reshape(rows, 2 * share)
-    prev, nxt = hop(own, 1), hop(own, -1)
-    far0, far1 = hop(prev[:half], 1), hop(nxt[half:], -1)
+    p0, n1 = hop(own[:half], 1), hop(own[half:], -1)
+    p1, n0 = hop(own[half:], 1), hop(own[:half], -1)
+    far0, far1 = hop(p0, 1), hop(n1, -1)
     wg, wu, wd = w_gate[0], w_up[0], w_down[0]
-    hid, dg, du, score = call(
-        functools.partial(expert_kernel, cap),
-        [shape((rows, ff), BF16)] * 3 + [shape((peers, 128), F32)],
-        8,
-    )(me, own, prev, nxt, far0, far1, wg, wu, wd)
-    b0, b1, b2, b3 = call(
+    near = call(near_kernel, [shape((rows, ff), F32)] * 3, 8, 9 * unit)(me, own, p0, p1, n0, n1, wg, wu, wd)
+
+    def far_block(i, tp_ref):
+        return (lax.rem(tp_ref[0] + 2, 4), 0)
+
+    def far_column(i, tp_ref):
+        return (0, lax.rem(tp_ref[0] + 2, 4))
+
+    def whole(dims):
+        return pl.BlockSpec(dims, lambda i, tp_ref: (0, 0))
+
+    far_outs = [shape((rows, ff), BF16)] * 3 + [shape((peers, 128), F32)] + [shape((half, share), BF16)] * 2
+    hid, dg, du, score, b2a, b2b = pl.pallas_call(
+        functools.partial(far_kernel, cap),
+        out_shape=far_outs,
+        grid_spec=pltpu.PrefetchScalarGridSpec(
+            num_scalar_prefetch=1,
+            grid=(1,),
+            in_specs=[
+                whole((half, 2 * share)),
+                whole((half, 2 * share)),
+                pl.BlockSpec((share, ff), far_block),
+                pl.BlockSpec((share, ff), far_block),
+                pl.BlockSpec((ff, share), far_column),
+            ]
+            + [whole((rows, ff))] * 3,
+            out_specs=[whole(o.shape) for o in far_outs],
+        ),
+        cost_estimate=cost(5 * unit, 4 << 20),
+    )(me, far0, far1, wg, wu, wd, *near)
+    score = score + hop(score, 1) + hop(score, -1) + hop(score, 2)
+    s1, s2 = hop(b2a, 1), hop(b2b, -1)
+    b0, b1a, b1b, b3a, b3b = call(
         token_kernel,
-        [shape((rows, share), F32), shape((rows, share), F32), shape((rows, share), BF16),
-         shape((rows, share), F32)],
+        [shape((rows, share), F32), shape((half, share), F32), shape((half, share), BF16),
+         shape((half, share), BF16), shape((half, share), F32)],
         4,
+        6 * unit,
     )(me, dg, du, wg, wu)
-    score = score + hop(score, 1) + hop(score, -1) + hop(score, 2)
-    s1, s2 = hop(b2[:half], 1), hop(b2[half:], -1)
-    up = jnp.concatenate([b1[:half] + s1.astype(F32), b1[half:]], axis=0).astype(BF16)
-    down = jnp.concatenate([b3[:half], b3[half:] + s2.astype(F32)], axis=0).astype(BF16)
-    r1, r2 = hop(up, 1), hop(down, -1)
-    summed = (b0 + r1.astype(F32) + r2.astype(F32)).astype(BF16)
+    d1, d2 = hop(b1b, 1), hop(b3a, -1)
+    e1 = hop((b1a + s1.astype(F32)).astype(BF16), 1)
+    e2 = hop((b3b + s2.astype(F32)).astype(BF16), -1)
+    summed = b0 + jnp.concatenate(
+        [e1.astype(F32) + d2.astype(F32), d1.astype(F32) + e2.astype(F32)], axis=0
+    )
     gwg, gwu, gwd = call(
         weight_kernel,
         [shape((width, ff), BF16), shape((width, ff), BF16), shape((ff, width), BF16)],
-        8,
-    )(me, own, prev, nxt, far0, far1, hid, dg, du)
+        10,
+        12 * unit,
+    )(me, own, p0, p1, n0, n1, far0, far1, hid, dg, du)
     q = exchange(score.reshape(peers, 1, 128)).reshape(peers, 128)
     part, term = call(
         functools.partial(router_kernel, cap),
         [shape((n_tok, share), F32), shape((peers, cap, 128), BF16)],
         5,
-    )(me, q, code, gate, tokens, router_weight)
-    payload = jnp.concatenate([summed.reshape(peers, cap, share), term], axis=2)
+        unit,
+    )(me, q, code, gate, tokens, router_t)
+    payload = jnp.concatenate([summed.astype(BF16).reshape(peers, cap, share), term], axis=2)
     home = exchange(payload)
     token_grad, router = call(
         functools.partial(home_kernel, cap),
         [shape((n_tok, share), BF16), shape((share // 128, 128), F32)],
         3,
+        unit,
         scalar=False,
     )(home, code, part)
     return (token_grad, router.reshape(share, 1), gwg[None], gwu[None], gwd[None])

time: 180 us -> 161 us (0.89)
  blocking collectives: 64.2 us -> 41.3 us
  starting transfers between devices: 19.4 us -> 40.7 us
  waiting for transfers between devices: 56.3 us -> 38.1 us
  local copies, waits for them, and re-layouts: 7.27 us -> 3.14 us
  Pallas kernels: 30.5 us -> 33.6 us
    ppermute x11 -> x15, waiting for transfers between devices: 43.2 us -> 20.1 us  [hop(): return lax.ppermute(value, 'tp', [(i, (i + by) % tp) for i in range(tp)])]
    all_to_all x2 -> x1, blocking collectives: 64.2 us -> 41.3 us  [exchange(): return lax.all_to_all(value, 'ep', split_axis=0, concat_axis=0, tiled=True)]
    all_to_all x1 -> x2, starting transfers between devices: 4.55 us -> 20.9 us  [exchange(): return lax.all_to_all(value, 'ep', split_axis=0, concat_axis=0, tiled=True)]
    ppermute x11 -> x15, starting transfers between devices: 14.8 us -> 19.8 us  [hop(): return lax.ppermute(value, 'tp', [(i, (i + by) % tp) for i in range(tp)])]
    all_to_all x1 -> x2, waiting for transfers between devices: 13.1 us -> 17.9 us  [exchange(): return lax.all_to_all(value, 'ep', split_axis=0, concat_axis=0, tiled=True)]
    pallas_call x2 -> x3, Pallas kernels: 14.2 us -> 17.6 us  [the longest x1 7.06 us: per_device(): call(near_kernel, [shape((rows, ff), F32)] * 3, 8, 9 * unit)]
    slice x5 -> x1, local copies, waits for them, and re-layouts: 2.39 us -> 0.07 us  [per_device(): p0, n1 = (hop(own[:half], 1), hop(own[half:], -1))]
    unnamed x20 -> x24, local copies, waits for them, and re-layouts: 4.88 us -> 3.07 us
  transfers between devices with their start and end apart: 12 -> 17, of which waited for: 7 -> 6; matrix products, arithmetic and copies ran while one was open for 1% -> 1% of each run, Pallas kernels for 6% -> 14%
where the time goes in v2:
time: 161 us
  blocking collectives  41.3 us (26%)
  starting transfers between devices  40.7 us (25%)
  waiting for transfers between devices  38.1 us (24%)
  Pallas kernels  33.6 us (21%)
  local copies, waits for them, and re-layouts  3.14 us (2%)
  other arithmetic  3.11 us (2%)
    all_to_all x1, blocking collectives, exchange(): return lax.all_to_all(value, 'ep', split_axis=0, concat_axis=0, tiled=True)  41.3 us
    all_to_all x2, starting transfers between devices, exchange(): return lax.all_to_all(value, 'ep', split_axis=0, concat_axis=0, tiled=True)  20.9 us
    ppermute x15, waiting for transfers between devices, hop(): return lax.ppermute(value, 'tp', [(i, (i + by) % tp) for i in range(tp)])  20.1 us
    ppermute x15, starting transfers between devices, hop(): return lax.ppermute(value, 'tp', [(i, (i + by) % tp) for i in range(tp)])  19.8 us
    all_to_all x2, waiting for transfers between devices, exchange(): return lax.all_to_all(value, 'ep', split_axis=0, concat_axis=0, tiled=True)  17.9 us
    pallas_call x1, Pallas kernels, per_device(): call(weight_kernel, [shape((width, ff), BF16), shape((width, ff), BF16),...  7.4 us
    pallas_call x1, Pallas kernels, per_device(): call(near_kernel, [shape((rows, ff), F32)] * 3, 8, 9 * unit)  7.06 us
    pallas_call x1, Pallas kernels, per_device(): pl.pallas_call(functools.partial(far_kernel, cap), out_shape=far_outs, gr...  5.57 us
  transfers between devices with their start and end apart: 17, of which 6 were waited for; matrix products, arithmetic and copies ran while one was open for 1% of the time, Pallas kernels for 14%

profile of v2, /device:TPU:1, one launch (start us, length us, event | category | flops | bytes accessed | tf_op | source)
XLA Modules:
  0.0 160.8 jit_solution(18350589342049656630)
XLA Ops:
  0.6 4.0 %shard_map.110 = (bf16[512,1024]{1,0:T(8,128)(2,1)}, f32[48,64]{1,0:T(8,128)}, f32[48,64]{1,0:T(8,128)}) custom-call(s32[1]{0:T(128)} %bitcast.tp_ref, bf16[48,2048]{1,0:T(8,128)(2,1)} %tok_ref.3, bf16[48,2048]{1,0:T(8,128)(2,1)} %og_ref.1, s32[4,48]{1,0:T(4,128)} %bitcast.36, bf16[64,2048]{1,0:T(8,128)(2,1)} %bitcast.34), custom_call_target="tpu_custom_call" | custom-call | flops 201326592 | bytes 4194304 | tf_op jit(solution)/shard_map/pallas_call | solution.py:218
  4.6 41.3 %all_to_all.15 = bf16[64,8,1024]{2,1,0:T(8,128)(2,1)S(1)} all-to-all(bf16[64,8,1024]{2,1,0:T(8,128)(2,1)} %bitcast.32), channel_id=1, replica_groups=mesh['ep'=64,'tp'=4] {'ep'}, dimensions={0} | all-to-all | bytes 2097152 | tf_op jit(solution)/shard_map/all_to_all | solution.py:216
  46.0 1.3 collective-permute-start
  47.3 1.5 collective-permute-start.2
  48.8 2.7 %collective-permute-start.5 = (bf16[256,1024]{1,0:T(8,128)(2,1)S(1)}, bf16[256,1024]{1,0:T(8,128)(2,1)S(1)}, u32[]{:S(2)}, u32[]{:S(2)}) collective-permute-start(bf16[256,1024]{1,0:T(8,128)(2,1)S(1)} %get-tuple-element.54), channel_id=1, source_target_pairs={{0,3},{1,0},{2,1},{3,2},{4,7},{5,4},{6,5},{7,6},{8,11},{9,8},{10,9... | collective-permute-start | bytes 1572872 | tf_op jit(solution)/shard_map/ppermute | solution.py:213
  51.5 8.2 %collective-permute-done.p0_ref = bf16[256,1024]{1,0:T(8,128)(2,1)S(1)} collective-permute-done((bf16[256,1024]{1,0:T(8,128)(2,1)S(1)}, bf16[256,1024]{1,0:T(8,128)(2,1)S(1)}, u32[]{:S(2)}, u32[]{:S(2)}) %collective-permute-start) | collective-permute-done | bytes 524320 | tf_op jit(solution)/shard_map/ppermute | solution.py:213
  59.7 2.7 %collective-permute-start.3 = (bf16[256,1024]{1,0:T(8,128)(2,1)S(1)}, bf16[256,1024]{1,0:T(8,128)(2,1)}, u32[]{:S(2)}, u32[]{:S(2)}) collective-permute-start(bf16[256,1024]{1,0:T(8,128)(2,1)S(1)} %collective-permute-done.2.n1_ref), channel_id=1, source_target_pairs={{0,3},{1,0},{2,1},{3,2},{4,7},{5,4},{6,5},{7,6},{8,11},{9,8},{10,9... | collective-permute-start | bytes 1572872 | tf_op jit(solution)/shard_map/ppermute | solution.py:213
  62.3 8.5 %collective-permute-done.4.p1_ref = bf16[256,1024]{1,0:T(8,128)(2,1)S(1)} collective-permute-done((bf16[256,1024]{1,0:T(8,128)(2,1)S(1)}, bf16[256,1024]{1,0:T(8,128)(2,1)S(1)}, u32[]{:S(2)}, u32[]{:S(2)}) %collective-permute-start.4) | collective-permute-done | bytes 524320 | tf_op jit(solution)/shard_map/ppermute | solution.py:213
  71.9 7.1 %shard_map.111 = (f32[512,384]{1,0:T(8,128)}, f32[512,384]{1,0:T(8,128)}, f32[512,384]{1,0:T(8,128)}) custom-call(s32[1]{0:T(128)} %bitcast.tp_ref, bf16[512,1024]{1,0:T(8,128)(2,1)} %bitcast.22, bf16[256,1024]{1,0:T(8,128)(2,1)} %copy-done.3, bf16[256,1024]{1,0:T(8,128)(2,1)} %copy-done.5, bf16[256,1024]{1,0:T(8,128)(2,1)} %copy-done.6, ...), custom_call_target="tpu_custom_call" | custom-call | flops 1811939328 | bytes 4194304 | tf_op jit(solution)/shard_map/pallas_call | solution.py:229
  78.9 3.3 %collective-permute-done.1.far0_ref = bf16[256,1024]{1,0:T(8,128)(2,1)} collective-permute-done((bf16[256,1024]{1,0:T(8,128)(2,1)S(1)}, bf16[256,1024]{1,0:T(8,128)(2,1)}, u32[]{:S(2)}, u32[]{:S(2)}) %collective-permute-start.1) | collective-permute-done | bytes 524320 | tf_op jit(solution)/shard_map/ppermute | solution.py:213
  82.2 5.6 %shard_map.112 = (bf16[512,384]{1,0:T(8,128)(2,1)}, bf16[512,384]{1,0:T(8,128)(2,1)}, bf16[512,384]{1,0:T(8,128)(2,1)}, f32[64,128]{1,0:T(8,128)}, bf16[256,512]{1,0:T(8,128)(2,1)}, /*index=5*/bf16[256,512]{1,0:T(8,128)(2,1)}) custom-call(s32[1]{0:T(128)} %bitcast.tp_ref, bf16[256,1024]{1,0:T(8,128)(2,1)} %collective-permute-done.1.far0_ref, ...), custom_call_target="tpu_custom_call" | custom-call | flops 1006632960 | bytes 4194304 | tf_op jit(solution)/shard_map/pallas_call | solution.py:241
  87.8 2.2 %collective-permute-start.14 = (f32[64,128]{1,0:T(8,128)}, f32[64,128]{1,0:T(8,128)S(1)}, u32[]{:S(2)}, u32[]{:S(2)}) collective-permute-start(f32[64,128]{1,0:T(8,128)} %get-tuple-element.42), channel_id=1, source_target_pairs={{0,2},{1,3},{2,0},{3,1},{4,6},{5,7},{6,4},{7,5},{8,10},{9,11},{10,... | collective-permute-start | bytes 98312 | tf_op jit(solution)/shard_map/ppermute | solution.py:213
  90.0 1.1 collective-permute-start.13
  91.4 2.4 %collective-permute-start.10 = (bf16[256,512]{1,0:T(8,128)(2,1)}, bf16[256,512]{1,0:T(8,128)(2,1)S(1)}, u32[]{:S(2)}, u32[]{:S(2)}) collective-permute-start(bf16[256,512]{1,0:T(8,128)(2,1)} %get-tuple-element.41), channel_id=1, source_target_pairs={{0,3},{1,0},{2,1},{3,2},{4,7},{5,4},{6,5},{7,6},{8,11},{9,8},{10,9... | collective-permute-start | bytes 786440 | tf_op jit(solution)/shard_map/ppermute | solution.py:213
  93.8 5.0 %shard_map.113 = (f32[512,512]{1,0:T(8,128)}, f32[256,512]{1,0:T(8,128)}, bf16[256,512]{1,0:T(8,128)(2,1)}, bf16[256,512]{1,0:T(8,128)(2,1)}, f32[256,512]{1,0:T(8,128)}) custom-call(s32[1]{0:T(128)} %bitcast.tp_ref, bf16[512,384]{1,0:T(8,128)(2,1)} %get-tuple-element.33.dg_ref, bf16[512,384]{1,0:T(8,128)(2,1)} %get-tuple-element.34.du_ref, ...), custom_call_target="tpu_custom_call" | custom-call | flops 1207959552 | bytes 4194304 | tf_op jit(solution)/shard_map/pallas_call | solution.py:261
  98.8 2.7 %collective-permute-start.8 = (bf16[256,512]{1,0:T(8,128)(2,1)}, bf16[256,512]{1,0:T(8,128)(2,1)S(1)}, u32[]{:S(2)}, u32[]{:S(2)}) collective-permute-start(bf16[256,512]{1,0:T(8,128)(2,1)} %get-tuple-element.38), channel_id=1, source_target_pairs={{0,3},{1,0},{2,1},{3,2},{4,7},{5,4},{6,5},{7,6},{8,11},{9,8},{10,9... | collective-permute-start | bytes 786440 | tf_op jit(solution)/shard_map/ppermute | solution.py:213
  102.1 9.4 %all-to-all-start.1 = ((f32[64,1,128]{2,1,0:T(1,128)}), f32[64,1,128]{2,1,0:T(1,128)S(1)}, u32[]{:S(2)}, u32[]{:S(2)}) async-start(f32[64,1,128]{2,1,0:T(1,128)} %bitcast.12), calls=%async_computation.1 | async-start | bytes 65536 | tf_op jit(solution)/shard_map/all_to_all | solution.py:216
  112.6 3.0 %collective-permute-start.11 = (bf16[256,512]{1,0:T(8,128)(2,1)S(1)}, bf16[256,512]{1,0:T(8,128)(2,1)S(1)}, u32[]{:S(2)}, u32[]{:S(2)}) collective-permute-start(bf16[256,512]{1,0:T(8,128)(2,1)S(1)} %add_convert_fusion), channel_id=1, source_target_pairs={{0,3},{1,0},{2,1},{3,2},{4,7},{5,4},{6,5},{7,6},{8,11},{9,8},{10,9... | collective-permute-start | bytes 786440 | tf_op jit(solution)/shard_map/ppermute | solution.py:213
  115.8 5.0 %all-to-all-done.1 = f32[64,1,128]{2,1,0:T(1,128)S(1)} async-done(((f32[64,1,128]{2,1,0:T(1,128)}), f32[64,1,128]{2,1,0:T(1,128)S(1)}, u32[]{:S(2)}, u32[]{:S(2)}) %all-to-all-start.1) | async-done | bytes 32800 | tf_op jit(solution)/shard_map/all_to_all | solution.py:216
  121.4 2.5 %shard_map.114 = (f32[48,512]{1,0:T(8,128)}, bf16[64,8,128]{2,1,0:T(8,128)(2,1)}) custom-call(s32[1]{0:T(128)} %bitcast.tp_ref, f32[64,128]{1,0:T(8,128)} %bitcast.33, f32[48,64]{1,0:T(8,128)} %get-tuple-element.43.code_ref, f32[48,64]{1,0:T(8,128)} %get-tuple-element.44.gate_ref, bf16[48,2048]{1,0:T(8,128)(2,1)} %tok_ref.3, bf16[64,2048]{1,0:T(8,128)(2,1)} %bitcast.35), custom_call_target="tpu_custom_call" | custom-call | flops 201326592 | bytes 4194304 | tf_op jit(solution)/shard_map/pallas_call | solution.py:281
  126.0 11.5 %all-to-all-start.2 = ((bf16[64,8,640]{2,1,0:T(8,128)(2,1)}), bf16[64,8,640]{2,1,0:T(8,128)(2,1)S(1)}, u32[]{:S(2)}, u32[]{:S(2)}) async-start(bf16[64,8,640]{2,1,0:T(8,128)(2,1)} %pad_maximum_fusion), calls=%async_computation.2 | async-start | bytes 1310720 | tf_op jit(solution)/shard_map/all_to_all | solution.py:216
  137.5 7.4 %shard_map.116 = (bf16[2048,384]{1,0:T(8,128)(2,1)}, bf16[2048,384]{1,0:T(8,128)(2,1)}, bf16[384,2048]{1,0:T(8,128)(2,1)}) custom-call(s32[1]{0:T(128)} %bitcast.tp_ref, bf16[512,1024]{1,0:T(8,128)(2,1)} %bitcast.23, bf16[256,1024]{1,0:T(8,128)(2,1)} %copy-done.3, bf16[256,1024]{1,0:T(8,128)(2,1)} %copy-done.5, bf16[256,1024]{1,0:T(8,128)(2,1)} %copy-done.6, ...), custom_call_target="tpu_custom_call" | custom-call | flops 2415919104 | bytes 4194304 | tf_op jit(solution)/shard_map/pallas_call | solution.py:274
  144.9 12.9 %all-to-all-done.2.home_ref = bf16[64,8,640]{2,1,0:T(8,128)(2,1)S(1)} async-done(((bf16[64,8,640]{2,1,0:T(8,128)(2,1)}), bf16[64,8,640]{2,1,0:T(8,128)(2,1)S(1)}, u32[]{:S(2)}, u32[]{:S(2)}) %all-to-all-start.2) | async-done | bytes 655392 | tf_op jit(solution)/shard_map/all_to_all | solution.py:216
  158.7 2.1 %shard_map.115 = (bf16[48,512]{1,0:T(8,128)(2,1)}, f32[4,128]{1,0:T(4,128)}) custom-call(bf16[64,8,640]{2,1,0:T(8,128)(2,1)} %copy-done.1, f32[48,64]{1,0:T(8,128)} %get-tuple-element.43.code_ref, f32[48,512]{1,0:T(8,128)} %get-tuple-element.46.part_ref), custom_call_target="tpu_custom_call" | custom-call | flops 201326592 | bytes 4194304 | tf_op jit(solution)/shard_map/pallas_call | solution.py:289
  (50 shorter events, 6.8 us)
Async XLA Ops:
  46.0 24.9 %copy-start = (bf16[64,8,1024]{2,1,0:T(8,128)(2,1)}, bf16[64,8,1024]{2,1,0:T(8,128)(2,1)S(1)}, u32[]{:S(2)}) copy-start(bf16[64,8,1024]{2,1,0:T(8,128)(2,1)S(1)} %all_to_all.15) | copy-start | bytes 3145732
  46.0 13.6 %collective-permute-start = (bf16[256,1024]{1,0:T(8,128)(2,1)S(1)}, bf16[256,1024]{1,0:T(8,128)(2,1)S(1)}, u32[]{:S(2)}, u32[]{:S(2)}) collective-permute-start(bf16[256,1024]{1,0:T(8,128)(2,1)S(1)} %get-tuple-element.54), channel_id=1, source_target_pairs={{0,1},{1,2},{2,3},{3,0},{4,5},{5,6},{6,7},{7,4},{8,9},{9,10},{10,1... | collective-permute-start | bytes 1572872 | tf_op jit(solution)/shard_map/ppermute | solution.py:213
  47.3 12.3 %collective-permute-start.2 = (bf16[256,1024]{1,0:T(8,128)(2,1)S(1)}, bf16[256,1024]{1,0:T(8,128)(2,1)S(1)}, u32[]{:S(2)}, u32[]{:S(2)}) collective-permute-start(bf16[256,1024]{1,0:T(8,128)(2,1)S(1)} %get-tuple-element.53), channel_id=1, source_target_pairs={{0,3},{1,0},{2,1},{3,2},{4,7},{5,4},{6,5},{7,6},{8,11},{9,8},{10,9... | collective-permute-start | bytes 1572872 | tf_op jit(solution)/shard_map/ppermute | solution.py:213
  48.8 22.1 %collective-permute-start.4 = (bf16[256,1024]{1,0:T(8,128)(2,1)S(1)}, bf16[256,1024]{1,0:T(8,128)(2,1)S(1)}, u32[]{:S(2)}, u32[]{:S(2)}) collective-permute-start(bf16[256,1024]{1,0:T(8,128)(2,1)S(1)} %get-tuple-element.53), channel_id=1, source_target_pairs={{0,1},{1,2},{2,3},{3,0},{4,5},{5,6},{6,7},{7,4},{8,9},{9,10},{10,1... | collective-permute-start | bytes 1572872 | tf_op jit(solution)/shard_map/ppermute | solution.py:213
  48.8 22.1 %collective-permute-start.5 = (bf16[256,1024]{1,0:T(8,128)(2,1)S(1)}, bf16[256,1024]{1,0:T(8,128)(2,1)S(1)}, u32[]{:S(2)}, u32[]{:S(2)}) collective-permute-start(bf16[256,1024]{1,0:T(8,128)(2,1)S(1)} %get-tuple-element.54), channel_id=1, source_target_pairs={{0,3},{1,0},{2,1},{3,2},{4,7},{5,4},{6,5},{7,6},{8,11},{9,8},{10,9... | collective-permute-start | bytes 1572872 | tf_op jit(solution)/shard_map/ppermute | solution.py:213
  59.6 11.3 %copy-start.3 = (bf16[256,1024]{1,0:T(8,128)(2,1)}, bf16[256,1024]{1,0:T(8,128)(2,1)S(1)}, u32[]{:S(2)}) copy-start(bf16[256,1024]{1,0:T(8,128)(2,1)S(1)} %collective-permute-done.p0_ref) | copy-start | bytes 1572868
  59.6 22.6 %collective-permute-start.1 = (bf16[256,1024]{1,0:T(8,128)(2,1)S(1)}, bf16[256,1024]{1,0:T(8,128)(2,1)}, u32[]{:S(2)}, u32[]{:S(2)}) collective-permute-start(bf16[256,1024]{1,0:T(8,128)(2,1)S(1)} %collective-permute-done.p0_ref), channel_id=1, source_target_pairs={{0,1},{1,2},{2,3},{3,0},{4,5},{5,6},{6,7},{7,4},{8,9},{9,10},{10,1... | collective-permute-start | bytes 1572872 | tf_op jit(solution)/shard_map/ppermute | solution.py:213
  59.7 11.2 %copy-start.4 = (bf16[256,1024]{1,0:T(8,128)(2,1)}, bf16[256,1024]{1,0:T(8,128)(2,1)S(1)}, u32[]{:S(2)}) copy-start(bf16[256,1024]{1,0:T(8,128)(2,1)S(1)} %collective-permute-done.2.n1_ref) | copy-start | bytes 1572868
  59.7 22.6 %collective-permute-start.3 = (bf16[256,1024]{1,0:T(8,128)(2,1)S(1)}, bf16[256,1024]{1,0:T(8,128)(2,1)}, u32[]{:S(2)}, u32[]{:S(2)}) collective-permute-start(bf16[256,1024]{1,0:T(8,128)(2,1)S(1)} %collective-permute-done.2.n1_ref), channel_id=1, source_target_pairs={{0,3},{1,0},{2,1},{3,2},{4,7},{5,4},{6,5},{7,6},{8,11},{9,8},{10,9... | collective-permute-start | bytes 1572872 | tf_op jit(solution)/shard_map/ppermute | solution.py:213
  87.8 11.0 %collective-permute-start.14 = (f32[64,128]{1,0:T(8,128)}, f32[64,128]{1,0:T(8,128)S(1)}, u32[]{:S(2)}, u32[]{:S(2)}) collective-permute-start(f32[64,128]{1,0:T(8,128)} %get-tuple-element.42), channel_id=1, source_target_pairs={{0,2},{1,3},{2,0},{3,1},{4,6},{5,7},{6,4},{7,5},{8,10},{9,11},{10,... | collective-permute-start | bytes 98312 | tf_op jit(solution)/shard_map/ppermute | solution.py:213
  90.0 11.5 %collective-permute-start.13 = (f32[64,128]{1,0:T(8,128)}, f32[64,128]{1,0:T(8,128)S(1)}, u32[]{:S(2)}, u32[]{:S(2)}) collective-permute-start(f32[64,128]{1,0:T(8,128)} %get-tuple-element.42), channel_id=1, source_target_pairs={{0,3},{1,0},{2,1},{3,2},{4,7},{5,4},{6,5},{7,6},{8,11},{9,8},{10,9... | collective-permute-start | bytes 98312 | tf_op jit(solution)/shard_map/ppermute | solution.py:213
  91.1 10.3 %collective-permute-start.12 = (f32[64,128]{1,0:T(8,128)}, f32[64,128]{1,0:T(8,128)S(1)}, u32[]{:S(2)}, u32[]{:S(2)}) collective-permute-start(f32[64,128]{1,0:T(8,128)} %get-tuple-element.42), channel_id=1, source_target_pairs={{0,1},{1,2},{2,3},{3,0},{4,5},{5,6},{6,7},{7,4},{8,9},{9,10},{10,1... | collective-permute-start | bytes 98312 | tf_op jit(solution)/shard_map/ppermute | solution.py:213
  91.4 20.0 %collective-permute-start.10 = (bf16[256,512]{1,0:T(8,128)(2,1)}, bf16[256,512]{1,0:T(8,128)(2,1)S(1)}, u32[]{:S(2)}, u32[]{:S(2)}) collective-permute-start(bf16[256,512]{1,0:T(8,128)(2,1)} %get-tuple-element.41), channel_id=1, source_target_pairs={{0,3},{1,0},{2,1},{3,2},{4,7},{5,4},{6,5},{7,6},{8,11},{9,8},{10,9... | collective-permute-start | bytes 786440 | tf_op jit(solution)/shard_map/ppermute | solution.py:213
  93.8 7.7 %copy-start.11 = (bf16[256,512]{1,0:T(8,128)(2,1)S(1)}, bf16[256,512]{1,0:T(8,128)(2,1)}, u32[]{:S(2)}) copy-start(bf16[256,512]{1,0:T(8,128)(2,1)} %get-tuple-element.37) | copy-start | bytes 786436
  93.8 7.7 %copy-start.9 = (f32[64,128]{1,0:T(8,128)S(1)}, f32[64,128]{1,0:T(8,128)}, u32[]{:S(2)}) copy-start(f32[64,128]{1,0:T(8,128)} %get-tuple-element.42) | copy-start | bytes 98308
  98.7 16.9 %copy-start.7 = (f32[256,512]{1,0:T(8,128)S(1)}, f32[256,512]{1,0:T(8,128)}, u32[]{:S(2)}) copy-start(f32[256,512]{1,0:T(8,128)} %get-tuple-element.36) | copy-start | bytes 1572868
  98.7 25.2 %collective-permute-start.9 = (bf16[256,512]{1,0:T(8,128)(2,1)}, bf16[256,512]{1,0:T(8,128)(2,1)S(1)}, u32[]{:S(2)}, u32[]{:S(2)}) collective-permute-start(bf16[256,512]{1,0:T(8,128)(2,1)} %get-tuple-element.39), channel_id=1, source_target_pairs={{0,1},{1,2},{2,3},{3,0},{4,5},{5,6},{6,7},{7,4},{8,9},{9,10},{10,1... | collective-permute-start | bytes 786440 | tf_op jit(solution)/shard_map/ppermute | solution.py:213
  98.8 25.3 %collective-permute-start.8 = (bf16[256,512]{1,0:T(8,128)(2,1)}, bf16[256,512]{1,0:T(8,128)(2,1)S(1)}, u32[]{:S(2)}, u32[]{:S(2)}) collective-permute-start(bf16[256,512]{1,0:T(8,128)(2,1)} %get-tuple-element.38), channel_id=1, source_target_pairs={{0,3},{1,0},{2,1},{3,2},{4,7},{5,4},{6,5},{7,6},{8,11},{9,8},{10,9... | collective-permute-start | bytes 786440 | tf_op jit(solution)/shard_map/ppermute | solution.py:213
  101.4 14.2 %collective-permute-start.6 = (bf16[256,512]{1,0:T(8,128)(2,1)S(1)}, bf16[256,512]{1,0:T(8,128)(2,1)S(1)}, u32[]{:S(2)}, u32[]{:S(2)}) collective-permute-start(bf16[256,512]{1,0:T(8,128)(2,1)S(1)} %copy-done.11), channel_id=1, source_target_pairs={{0,1},{1,2},{2,3},{3,0},{4,5},{5,6},{6,7},{7,4},{8,9},{9,10},{10,1... | collective-permute-start | bytes 786440 | tf_op jit(solution)/shard_map/ppermute | solution.py:213
  102.1 18.7 %all-to-all-start.1 = ((f32[64,1,128]{2,1,0:T(1,128)}), f32[64,1,128]{2,1,0:T(1,128)S(1)}, u32[]{:S(2)}, u32[]{:S(2)}) async-start(f32[64,1,128]{2,1,0:T(1,128)} %bitcast.12), calls=%async_computation.1 | async-start | bytes 65536 | tf_op jit(solution)/shard_map/all_to_all | solution.py:216
  112.6 11.4 %collective-permute-start.11 = (bf16[256,512]{1,0:T(8,128)(2,1)S(1)}, bf16[256,512]{1,0:T(8,128)(2,1)S(1)}, u32[]{:S(2)}, u32[]{:S(2)}) collective-permute-start(bf16[256,512]{1,0:T(8,128)(2,1)S(1)} %add_convert_fusion), channel_id=1, source_target_pairs={{0,3},{1,0},{2,1},{3,2},{4,7},{5,4},{6,5},{7,6},{8,11},{9,8},{10,9... | collective-permute-start | bytes 786440 | tf_op jit(solution)/shard_map/ppermute | solution.py:213
  115.7 8.5 %copy-start.2 = (f32[512,512]{1,0:T(8,128)S(1)}, f32[512,512]{1,0:T(8,128)}, u32[]{:S(2)}) copy-start(f32[512,512]{1,0:T(8,128)} %get-tuple-element.35) | copy-start | bytes 3145732
  115.7 8.4 %collective-permute-start.7 = (bf16[256,512]{1,0:T(8,128)(2,1)S(1)}, bf16[256,512]{1,0:T(8,128)(2,1)S(1)}, u32[]{:S(2)}, u32[]{:S(2)}) collective-permute-start(bf16[256,512]{1,0:T(8,128)(2,1)S(1)} %add_convert_fusion.1), channel_id=1, source_target_pairs={{0,1},{1,2},{2,3},{3,0},{4,5},{5,6},{6,7},{7,4},{8,9},{9,10},{10,1... | collective-permute-start | bytes 786440 | tf_op jit(solution)/shard_map/ppermute | solution.py:213
  126.0 31.9 %all-to-all-start.2 = ((bf16[64,8,640]{2,1,0:T(8,128)(2,1)}), bf16[64,8,640]{2,1,0:T(8,128)(2,1)S(1)}, u32[]{:S(2)}, u32[]{:S(2)}) async-start(bf16[64,8,640]{2,1,0:T(8,128)(2,1)} %pad_maximum_fusion), calls=%async_computation.2 | async-start | bytes 1310720 | tf_op jit(solution)/shard_map/all_to_all | solution.py:216
  (5 other events, 4.2 us)

commit v3 on v1

v3 whole, which is shorter than its diff:
```python
import functools

import jax
import jax.numpy as jnp
from jax import lax
from jax.experimental import pallas as pl
from jax.experimental.pallas import tpu as pltpu
from jax.sharding import PartitionSpec as P


F32 = jnp.float32
BF16 = jnp.bfloat16
HI = lax.Precision.HIGHEST
VMEM = pl.BlockSpec(memory_space=pltpu.VMEM)
SMEM = pl.BlockSpec(memory_space=pltpu.SMEM)


def mm(a, b, dims, precision=None):
    return lax.dot_general(a, b, (dims, ((), ())), precision=precision, preferred_element_type=F32)


NN = ((1,), (0,))
NT = ((1,), (1,))
TN = ((0,), (0,))


def iota(shape, dim):
    return lax.broadcasted_iota(jnp.int32, shape, dim)


def spread(experts, cap):
    rows = experts * cap
    return (iota((rows, experts), 0) // cap == iota((rows, experts), 1)).astype(F32)


def dispatch_kernel(cap, tp_ref, tok_ref, og_ref, ids_ref, rw_ref, send_ref, code_ref, gate_ref):
    n_tok = tok_ref.shape[0]
    experts = rw_ref.shape[0]
    share = send_ref.shape[1] // 2
    start = pl.multiple_of(tp_ref[0] * share, share)
    logits = mm(tok_ref[...], rw_ref[...], NT)
    ids = ids_ref[...].astype(F32).T
    lane = iota((n_tok, experts), 1).astype(F32)
    hit = lane == ids[:, 0:1]
    for k in range(1, ids.shape[1]):
        hit = hit | (lane == ids[:, k : k + 1])
    mask = hit.astype(F32)
    top = jnp.max(jnp.where(hit, logits, -jnp.inf), axis=1, keepdims=True)
    weight = jnp.where(hit, jnp.exp(jnp.where(hit, logits - top, 0.0)), 0.0)
    gate = weight / jnp.sum(weight, axis=1, keepdims=True)
    earlier = (iota((n_tok, n_tok), 1) < iota((n_tok, n_tok), 0)).astype(BF16)
    rank = mm(earlier, mask.astype(BF16), NN)
    code = mask * (rank + 1.0)
    code_ref[...] = code
    gate_ref[...] = gate
    expand = spread(experts, cap)
    rows = experts * cap
    code_of = mm(expand.astype(BF16), code.astype(BF16), NT)
    pick = code_of == (iota((rows, n_tok), 0) % cap + 1).astype(F32)
    gate_of = jnp.where(pick, mm(expand, gate, NT, HI), 0.0)
    send_ref[:, :share] = mm(pick.astype(F32).astype(BF16), tok_ref[:, pl.ds(start, share)], NN).astype(BF16)
    cot = og_ref[:, pl.ds(start, share)].astype(F32)
    send_ref[:, share:] = mm(gate_of, cot, NN, HI).astype(BF16)


def expert_kernel(cap, first, tp_ref, own_ref, p0_ref, p1_ref, n0_ref, n1_ref, f0_ref, f1_ref, wg_ref, wu_ref, wd_ref,
                  hid_ref, dg_ref, du_ref, score_ref, plus_ref, minus_ref, b1_ref, b3_ref, b0_ref):
    rows, share = b0_ref.shape
    half = rows // 2
    me = tp_ref[0]

    def at(off):
        return pl.ds(pl.multiple_of(lax.rem(me + off, 4) * share, share), share)

    def joined(lo, hi, cols):
        return jnp.concatenate([lo[:, cols], hi[:, cols]], axis=0)

    left, right = slice(0, share), slice(share, 2 * share)
    gate_pre = up_pre = back = None
    for off, lo, hi in ((0, own_ref.at[pl.ds(first, half)], own_ref.at[pl.ds(first + half, half)]),
                        (3, p0_ref, p1_ref), (1, n0_ref, n1_ref), (2, f0_ref, f1_ref)):
        t, g = joined(lo, hi, left), joined(lo, hi, right)
        terms = (mm(t, wg_ref[at(off), :], NN), mm(t, wu_ref[at(off), :], NN), mm(g, wd_ref[:, at(off)], NT))
        if gate_pre is None:
            gate_pre, up_pre, back = terms
        else:
            gate_pre, up_pre, back = gate_pre + terms[0], up_pre + terms[1], back + terms[2]
    glu = jnp.minimum(gate_pre, 7.0)
    linear = jnp.clip(up_pre, -7.0, 7.0)
    sig = jax.nn.sigmoid(1.702 * glu)
    act = glu * sig
    hidden = (linear + 1.0) * act
    slope = (linear + 1.0) * (sig + 1.702 * glu * sig * (1.0 - sig))
    slope = jnp.where(gate_pre < 7.0, slope, 0.0)
    up_slope = jnp.where((up_pre > -7.0) & (up_pre < 7.0), act, 0.0)
    dg = (back * slope).astype(BF16)
    du = (back * up_slope).astype(BF16)
    hid_ref[...] = hidden.astype(BF16)
    dg_ref[...] = dg
    du_ref[...] = du
    score = jnp.sum(hidden * back, axis=1, keepdims=True)
    peers = rows // cap
    spot = (iota((rows, 128), 0) % cap == iota((rows, 128), 1)).astype(F32) * score
    group = (iota((peers, rows), 1) // cap == iota((peers, rows), 0)).astype(F32)
    score_ref[...] = mm(group, spot, NN, HI)

    def part(off):
        return mm(dg, wg_ref[at(off), :], NT) + mm(du, wu_ref[at(off), :], NT)

    far = part(2).astype(BF16)
    plus_ref[:half, :] = far[:half]
    minus_ref[half:, :] = far[half:]
    ahead = part(1)
    b1_ref[...] = ahead[:half]
    plus_ref[half:, :] = ahead[half:].astype(BF16)
    behind = part(3)
    minus_ref[:half, :] = behind[:half].astype(BF16)
    b3_ref[...] = behind[half:]
    b0_ref[...] = part(0)


def weight_kernel(tp_ref, own, p0, p1a, p1b, n0, n1a, n1b, f0a, f0b, f1a, f1b, hid0, hid1, dg0, dg1, du0, du1,
                  gwg_ref, gwu_ref, gwd_ref):
    share = own.shape[1] // 2
    me = tp_ref[0]

    def rows(pieces, cols):
        return jnp.concatenate([x[:, cols] for x in pieces], axis=0)

    every = slice(None)
    hid, dg, du = rows((hid0, hid1), every), rows((dg0, dg1), every), rows((du0, du1), every)
    for off, pieces in ((0, (own,)), (3, (p0, p1a, p1b)), (1, (n0, n1b, n1a)), (2, (f0a, f0b, f1a, f1b))):
        at = pl.ds(pl.multiple_of(lax.rem(me + off, 4) * share, share), share)
        t = rows(pieces, slice(0, share))
        g = rows(pieces, slice(share, 2 * share))
        gwg_ref[at, :] = mm(t, dg, TN).astype(BF16)
        gwu_ref[at, :] = mm(t, du, TN).astype(BF16)
        gwd_ref[:, at] = mm(hid, g, TN).astype(BF16)


def router_kernel(cap, tp_ref, q_ref, code_ref, gate_ref, tok_ref, rw_ref, part_ref, term_ref):
    share = part_ref.shape[1]
    start = pl.multiple_of(tp_ref[0] * share, share)
    code, gate = code_ref[...], gate_ref[...]
    q = q_ref[...].T
    score = jnp.zeros_like(code)
    for r in range(cap):
        score = score + jnp.where(code == r + 1.0, q[r : r + 1, :], 0.0)
    d_logits = score - gate * jnp.sum(score, axis=1, keepdims=True)
    part_ref[...] = mm(d_logits, rw_ref[:, pl.ds(start, share)].astype(F32), NN, HI)
    term = mm(d_logits, tok_ref[:, pl.ds(start, share)].astype(F32), TN, HI)
    high = term.astype(BF16)
    low = (term - high.astype(F32)).astype(BF16)
    pieces = share // 128
    for j in range(pieces):
        term_ref[:, j, :] = high[:, j * 128 : (j + 1) * 128]
        term_ref[:, pieces + j, :] = low[:, j * 128 : (j + 1) * 128]


def home_kernel(cap, home_ref, code_ref, part_ref, tok_out_ref, router_ref):
    share = part_ref.shape[1]
    code = code_ref[...]
    n_tok, experts = code.shape
    rows = experts * cap
    code_of = mm(code.astype(BF16), spread(experts, cap).astype(BF16), NT)
    pick = code_of == (iota((n_tok, rows), 1) % cap + 1).astype(F32)
    flat = home_ref[...].reshape(rows, home_ref.shape[2])
    tok_out_ref[...] = (
        mm(pick.astype(F32).astype(BF16), flat[:, :share], NN) + part_ref[...]
    ).astype(BF16)
    both = jnp.sum(home_ref[:, :, share:].astype(F32), axis=0)
    pieces = share // 128
    router_ref[...] = both[:pieces] + both[pieces:]


def cost(flops, data):
    return pl.CostEstimate(flops=flops, bytes_accessed=data, transcendentals=0)


def call(body, outs, n_in, flops, scalar=True):
    return pl.pallas_call(
        body,
        out_shape=outs,
        in_specs=([SMEM] if scalar else []) + [VMEM] * n_in,
        out_specs=[VMEM] * len(outs),
        cost_estimate=cost(flops, 4 << 20),
    )


def shape(dims, dtype):
    return jax.ShapeDtypeStruct(dims, dtype)


def per_device(tokens, out_grad, expert_ids, router_weight, w_gate, w_up, w_down):
    n_tok, width = tokens.shape
    experts = router_weight.shape[1]
    peers = lax.axis_size("ep")
    tp = lax.axis_size("tp")
    cap = 8
    share = width // tp
    ff = w_gate.shape[2]
    rows = peers * cap
    half = rows // 2
    me = jnp.full((1,), lax.axis_index("tp"), jnp.int32)
    unit = 2 * rows * share * ff
    router_t = router_weight.T

    def hop(value, by):
        return lax.ppermute(value, "tp", [(i, (i + by) % tp) for i in range(tp)])

    def exchange(value):
        return lax.all_to_all(value, "ep", split_axis=0, concat_axis=0, tiled=True)

    send, code, gate = call(
        functools.partial(dispatch_kernel, cap),
        [shape((rows, 2 * share), BF16), shape((n_tok, experts), F32), shape((n_tok, experts), F32)],
        4,
        unit,
    )(me, tokens, out_grad, expert_ids.T, router_t)
    own = exchange(send.reshape(peers, cap, 2 * share)).reshape(rows, 2 * share)
    piece = half // 2
    own1a, own1b = own[half : half + piece], own[half + piece :]
    p0, n0 = hop(own[:half], 1), hop(own[:half], -1)
    p1a, n1a = hop(own1a, 1), hop(own1b, -1)
    f0a, f0b = hop(p0[:piece], 1), hop(n0[piece:], -1)
    p1b, n1b = hop(own1b, 1), hop(own1a, -1)
    f1a, f1b = hop(p1a, 1), hop(n1a, -1)
    wg, wu, wd = w_gate[0], w_up[0], w_down[0]

    def expert(h, *blocks):
        hid, dg, du, score, plus, minus, b1, b3, b0 = call(
            functools.partial(expert_kernel, cap, h * half),
            [shape((half, ff), BF16)] * 3
            + [shape((half // cap, 128), F32)]
            + [shape((half, share), BF16)] * 2
            + [shape((piece, share), F32)] * 2
            + [shape((half, share), F32)],
            10,
            10 * unit,
        )(me, own, *blocks, wg, wu, wd)
        rp, rm = hop(plus, 1), hop(minus, -1)
        ep = hop((b1 + rp[:piece].astype(F32)).astype(BF16), 1)
        em = hop((b3 + rm[piece:].astype(F32)).astype(BF16), -1)
        top = b0[:piece] + ep.astype(F32) + rm[:piece].astype(F32)
        low = b0[piece:] + rp[piece:].astype(F32) + em.astype(F32)
        return hid, dg, du, score, [top, low]

    hid0, dg0, du0, score0, sum0 = expert(0, p0[:piece], p0[piece:], n0[:piece], n0[piece:], f0a, f0b)
    hid1, dg1, du1, score1, sum1 = expert(1, p1a, p1b, n1b, n1a, f1a, f1b)
    score = jnp.concatenate([score0, score1], axis=0)
    score = score + hop(score, 1) + hop(score, -1) + hop(score, 2)
    summed = jnp.concatenate(sum0 + sum1, axis=0)
    gwg, gwu, gwd = call(
        weight_kernel,
        [shape((width, ff), BF16), shape((width, ff), BF16), shape((ff, width), BF16)],
        17,
        12 * unit,
    )(me, own, p0, p1a, p1b, n0, n1a, n1b, f0a, f0b, f1a, f1b, hid0, hid1, dg0, dg1, du0, du1)
    q = exchange(score.reshape(peers, 1, 128)).reshape(peers, 128)
    part, term = call(
        functools.partial(router_kernel, cap), [shape((n_tok, share), F32), shape((peers, cap, 128), BF16)], 5, unit
    )(me, q, code, gate, tokens, router_t)
    payload = jnp.concatenate([summed.astype(BF16).reshape(peers, cap, share), term], axis=2)
    home = exchange(payload)
    token_grad, router = call(
        functools.partial(home_kernel, cap),
        [shape((n_tok, share), BF16), shape((share // 128, 128), F32)],
        3,
        unit,
        scalar=False,
    )(home, code, part)
    return (token_grad, router.reshape(share, 1), gwg[None], gwu[None], gwd[None])


def solution(mesh):
    in_specs = (
        P("ep", None),
        P("ep", None),
        P("ep", None),
        P(),
        P("ep", None, "tp"),
        P("ep", None, "tp"),
        P("ep", "tp", None),
    )
    out_specs = (
        P("ep", "tp"),
        P("tp", "ep"),
        P("ep", None, "tp"),
        P("ep", None, "tp"),
        P("ep", "tp", None),
    )

    return jax.shard_map(per_device, mesh=mesh, in_specs=in_specs, out_specs=out_specs, check_vma=False)
```

time: 180 us -> 167 us (0.928)
  starting transfers between devices: 19.4 us -> 43.4 us
  blocking collectives: 64.2 us -> 41.3 us
  waiting for transfers between devices: 56.3 us -> 42.2 us
    ppermute x11 -> x21, waiting for transfers between devices: 43.2 us -> 20 us  [hop(): return lax.ppermute(value, 'tp', [(i, (i + by) % tp) for i in range(tp)])]
    all_to_all x2 -> x1, blocking collectives: 64.2 us -> 41.3 us  [exchange(): return lax.all_to_all(value, 'ep', split_axis=0, concat_axis=0, tiled=True)]
    all_to_all x1 -> x2, starting transfers between devices: 4.55 us -> 20 us  [exchange(): return lax.all_to_all(value, 'ep', split_axis=0, concat_axis=0, tiled=True)]
    all_to_all x1 -> x2, waiting for transfers between devices: 13.1 us -> 22.2 us  [exchange(): return lax.all_to_all(value, 'ep', split_axis=0, concat_axis=0, tiled=True)]
    ppermute x11 -> x21, starting transfers between devices: 14.8 us -> 23.4 us  [hop(): return lax.ppermute(value, 'tp', [(i, (i + by) % tp) for i in range(tp)])]
    unnamed x20 -> x47, local copies, waits for them, and re-layouts: 4.88 us -> 4.53 us
  transfers between devices with their start and end apart: 12 -> 23, of which waited for: 7 -> 6; matrix products, arithmetic and copies ran while one was open for 1% -> 2% of each run, Pallas kernels for 6% -> 15%
where the time goes in v3:
time: 167 us
  starting transfers between devices  43.4 us (26%)
  waiting for transfers between devices  42.2 us (25%)
  blocking collectives  41.3 us (25%)
  Pallas kernels  30.9 us (19%)
  local copies, waits for them, and re-layouts  6.21 us (4%)
  other arithmetic  1.88 us (1%)
    all_to_all x1, blocking collectives, exchange(): return lax.all_to_all(value, 'ep', split_axis=0, concat_axis=0, tiled=True)  41.3 us
    ppermute x21, starting transfers between devices, hop(): return lax.ppermute(value, 'tp', [(i, (i + by) % tp) for i in range(tp)])  23.4 us
    all_to_all x2, waiting for transfers between devices, exchange(): return lax.all_to_all(value, 'ep', split_axis=0, concat_axis=0, tiled=True)  22.2 us
    all_to_all x2, starting transfers between devices, exchange(): return lax.all_to_all(value, 'ep', split_axis=0, concat_axis=0, tiled=True)  20 us
    ppermute x21, waiting for transfers between devices, hop(): return lax.ppermute(value, 'tp', [(i, (i + by) % tp) for i in range(tp)])  20 us
    pallas_call x2, Pallas kernels, expert(): call(functools.partial(expert_kernel, cap, h * half), [shape((half, ff),...  14.9 us
    pallas_call x1, Pallas kernels, per_device(): call(weight_kernel, [shape((width, ff), BF16), shape((width, ff), BF16),...  7.41 us
    unnamed x47, local copies, waits for them, and re-layouts  4.53 us
  transfers between devices with their start and end apart: 23, of which 6 were waited for; matrix products, arithmetic and copies ran while one was open for 2% of the time, Pallas kernels for 15%

profile of v3, /device:TPU:1, one launch (start us, length us, event | category | flops | bytes accessed | tf_op | source)
XLA Modules:
  0.0 166.8 jit_solution(10115517712507863498)
XLA Ops:
  0.6 4.0 %shard_map.110 = (bf16[512,1024]{1,0:T(8,128)(2,1)}, f32[48,64]{1,0:T(8,128)}, f32[48,64]{1,0:T(8,128)}) custom-call(s32[1]{0:T(128)} %bitcast.tp_ref, bf16[48,2048]{1,0:T(8,128)(2,1)} %tok_ref.3, bf16[48,2048]{1,0:T(8,128)(2,1)} %og_ref.1, s32[4,48]{1,0:T(4,128)} %bitcast.37, bf16[64,2048]{1,0:T(8,128)(2,1)} %bitcast.35), custom_call_target="tpu_custom_call" | custom-call | flops 201326592 | bytes 4194304 | tf_op jit(solution)/shard_map/pallas_call | solution.py:214
  4.6 41.3 %all_to_all.15 = bf16[64,8,1024]{2,1,0:T(8,128)(2,1)S(1)} all-to-all(bf16[64,8,1024]{2,1,0:T(8,128)(2,1)} %bitcast.27), channel_id=1, replica_groups=mesh['ep'=64,'tp'=4] {'ep'}, dimensions={0} | all-to-all | bytes 2097152 | tf_op jit(solution)/shard_map/all_to_all | solution.py:212
  46.0 1.3 collective-permute-start
  47.3 1.5 collective-permute-start.1
  48.9 2.7 %collective-permute-start.11 = (bf16[128,1024]{1,0:T(8,128)(2,1)S(1)}, bf16[128,1024]{1,0:T(8,128)(2,1)S(1)}, u32[]{:S(2)}, u32[]{:S(2)}) collective-permute-start(bf16[128,1024]{1,0:T(8,128)(2,1)S(1)} %get-tuple-element.61), channel_id=1, source_target_pairs={{0,3},{1,0},{2,1},{3,2},{4,7},{5,4},{6,5},{7,6},{8,11},{9,8},{10,9... | collective-permute-start | bytes 786440 | tf_op jit(solution)/shard_map/ppermute | solution.py:209
  51.5 13.7 %collective-permute-done.8.p0_ref.p1a = bf16[128,1024]{1,0:T(8,128)(2,1)S(1)} collective-permute-done((bf16[128,1024]{1,0:T(8,128)(2,1)S(1)}, bf16[128,1024]{1,0:T(8,128)(2,1)S(1)}, u32[]{:S(2)}, u32[]{:S(2)}) %collective-permute-start.8) | collective-permute-done | bytes 262176 | tf_op jit(solution)/shard_map/ppermute | solution.py:209
  65.2 1.3 collective-permute-start.10
  66.7 2.5 %collective-permute-start.13 = (bf16[128,1024]{1,0:T(8,128)(2,1)S(1)}, bf16[128,1024]{1,0:T(8,128)(2,1)S(1)}, u32[]{:S(2)}, u32[]{:S(2)}) collective-permute-start(bf16[128,1024]{1,0:T(8,128)(2,1)S(1)} %collective-permute-done.11.n1_ref.n1a), channel_id=1, source_target_pairs={{0,3},{1,0},{2,1},{3,2},{4,7},{5,4},{6,5},{7,6},{8,11},{9,8},{10,9... | collective-permute-start | bytes 786440 | tf_op jit(solution)/shard_map/ppermute | solution.py:209
  70.9 2.6 %collective-permute-start.3 = (bf16[128,1024]{1,0:T(8,128)(2,1)S(1)}, bf16[128,1024]{1,0:T(8,128)(2,1)S(1)}, u32[]{:S(2)}, u32[]{:S(2)}) collective-permute-start(bf16[128,1024]{1,0:T(8,128)(2,1)S(1)} %get-tuple-element.67.n1_ref), channel_id=1, source_target_pairs={{0,3},{1,0},{2,1},{3,2},{4,7},{5,4},{6,5},{7,6},{8,11},{9,8},{10,9... | collective-permute-start | bytes 786440 | tf_op jit(solution)/shard_map/ppermute | solution.py:209
  73.5 2.2 %collective-permute-done.12.f0_ref.f1a = bf16[128,1024]{1,0:T(8,128)(2,1)S(1)} collective-permute-done((bf16[128,1024]{1,0:T(8,128)(2,1)S(1)}, bf16[128,1024]{1,0:T(8,128)(2,1)S(1)}, u32[]{:S(2)}, u32[]{:S(2)}) %collective-permute-start.12) | collective-permute-done | bytes 262176 | tf_op jit(solution)/shard_map/ppermute | solution.py:209
  77.2 7.4 %shard_map.112 = (bf16[256,384]{1,0:T(8,128)(2,1)}, bf16[256,384]{1,0:T(8,128)(2,1)}, bf16[256,384]{1,0:T(8,128)(2,1)}, f32[32,128]{1,0:T(8,128)}, bf16[256,512]...) custom-call(s32[1]{0:T(128)} %bitcast.tp_ref, ...), custom_call_target="tpu_custom_call" | custom-call | flops 2013265920 | bytes 4194304 | tf_op jit(solution)/shard_map/pallas_call | solution.py:231
  85.4 2.0 %collective-permute-start.16 = (bf16[256,512]{1,0:T(8,128)(2,1)}, bf16[256,512]{1,0:T(8,128)(2,1)S(1)}, u32[]{:S(2)}, u32[]{:S(2)}) collective-permute-start(bf16[256,512]{1,0:T(8,128)(2,1)} %get-tuple-element.42), channel_id=1, source_target_pairs={{0,3},{1,0},{2,1},{3,2},{4,7},{5,4},{6,5},{7,6},{8,11},{9,8},{10,9... | collective-permute-start | bytes 786440 | tf_op jit(solution)/shard_map/ppermute | solution.py:209
  88.2 7.5 %shard_map.111 = (bf16[256,384]{1,0:T(8,128)(2,1)}, bf16[256,384]{1,0:T(8,128)(2,1)}, bf16[256,384]{1,0:T(8,128)(2,1)}, f32[32,128]{1,0:T(8,128)}, bf16[256,512]...) custom-call(s32[1]{0:T(128)} %bitcast.tp_ref, ...), custom_call_target="tpu_custom_call" | custom-call | flops 2013265920 | bytes 4194304 | tf_op jit(solution)/shard_map/pallas_call | solution.py:231
  99.4 1.3 collective-permute-done.20
  100.8 2.7 %collective-permute-start.6 = (bf16[256,512]{1,0:T(8,128)(2,1)}, bf16[256,512]{1,0:T(8,128)(2,1)S(1)}, u32[]{:S(2)}, u32[]{:S(2)}) collective-permute-start(bf16[256,512]{1,0:T(8,128)(2,1)} %get-tuple-element.37), channel_id=1, source_target_pairs={{0,3},{1,0},{2,1},{3,2},{4,7},{5,4},{6,5},{7,6},{8,11},{9,8},{10,9... | collective-permute-start | bytes 786440 | tf_op jit(solution)/shard_map/ppermute | solution.py:209
  104.1 14.4 %all-to-all-start.1 = ((f32[64,1,128]{2,1,0:T(1,128)}), f32[64,1,128]{2,1,0:T(1,128)S(1)}, u32[]{:S(2)}, u32[]{:S(2)}) async-start(f32[64,1,128]{2,1,0:T(1,128)} %bitcast.13), calls=%async_computation.1 | async-start | bytes 65536 | tf_op jit(solution)/shard_map/all_to_all | solution.py:212
  118.7 9.1 %all-to-all-done.1 = f32[64,1,128]{2,1,0:T(1,128)S(1)} async-done(((f32[64,1,128]{2,1,0:T(1,128)}), f32[64,1,128]{2,1,0:T(1,128)S(1)}, u32[]{:S(2)}, u32[]{:S(2)}) %all-to-all-start.1) | async-done | bytes 32800 | tf_op jit(solution)/shard_map/all_to_all | solution.py:212
  128.5 2.5 %shard_map.113 = (f32[48,512]{1,0:T(8,128)}, bf16[64,8,128]{2,1,0:T(8,128)(2,1)}) custom-call(s32[1]{0:T(128)} %bitcast.tp_ref, f32[64,128]{1,0:T(8,128)} %bitcast.28, f32[48,64]{1,0:T(8,128)} %get-tuple-element.46.code_ref, f32[48,64]{1,0:T(8,128)} %get-tuple-element.47.gate_ref, bf16[48,2048]{1,0:T(8,128)(2,1)} %tok_ref.3, bf16[64,2048]{1,0:T(8,128)(2,1)} %bitcast.36), custom_call_target="tpu_custom_call" | custom-call | flops 201326592 | bytes 4194304 | tf_op jit(solution)/shard_map/pallas_call | solution.py:260
  131.2 2.7 %collective-permute-start.7 = (bf16[128,512]{1,0:T(8,128)(2,1)S(1)}, bf16[128,512]{1,0:T(8,128)(2,1)S(1)}, u32[]{:S(2)}, u32[]{:S(2)}) collective-permute-start(bf16[128,512]{1,0:T(8,128)(2,1)S(1)} %add_convert_fusion.5), channel_id=1, source_target_pairs={{0,3},{1,0},{2,1},{3,2},{4,7},{5,4},{6,5},{7,6},{8,11},{9,8},{10,9... | collective-permute-start | bytes 393224 | tf_op jit(solution)/shard_map/ppermute | solution.py:209
  134.0 2.7 %collective-permute-done.5 = bf16[128,512]{1,0:T(8,128)(2,1)S(1)} collective-permute-done((bf16[128,512]{1,0:T(8,128)(2,1)S(1)}, bf16[128,512]{1,0:T(8,128)(2,1)S(1)}, u32[]{:S(2)}, u32[]{:S(2)}) %collective-permute-start.5) | collective-permute-done | bytes 131104 | tf_op jit(solution)/shard_map/ppermute | solution.py:209
  137.8 5.6 %all-to-all-start.2 = ((bf16[64,8,640]{2,1,0:T(8,128)(2,1)}), bf16[64,8,640]{2,1,0:T(8,128)(2,1)S(1)}, u32[]{:S(2)}, u32[]{:S(2)}) async-start(bf16[64,8,640]{2,1,0:T(8,128)(2,1)} %pad_maximum_fusion), calls=%async_computation.2 | async-start | bytes 1310720 | tf_op jit(solution)/shard_map/all_to_all | solution.py:212
  143.4 7.4 %shard_map.115 = (bf16[2048,384]{1,0:T(8,128)(2,1)}, bf16[2048,384]{1,0:T(8,128)(2,1)}, bf16[384,2048]{1,0:T(8,128)(2,1)}) custom-call(s32[1]{0:T(128)} %bitcast.tp_ref, bf16[512,1024]{1,0:T(8,128)(2,1)} %bitcast.26, bf16[256,1024]{1,0:T(8,128)(2,1)} %copy-done.2, bf16[128,1024]{1,0:T(8,128)(2,1)} %copy-done.15, bf16[128,1024]{1,0:T(8,128)(2,1)} %copy-done.17, ...), custom_call_target="tpu_custom_call" | custom-call | flops 2415919104 | bytes 4194304 | tf_op jit(solution)/shard_map/pallas_call | solution.py:253
  150.8 13.1 %all-to-all-done.2.home_ref = bf16[64,8,640]{2,1,0:T(8,128)(2,1)S(1)} async-done(((bf16[64,8,640]{2,1,0:T(8,128)(2,1)}), bf16[64,8,640]{2,1,0:T(8,128)(2,1)S(1)}, u32[]{:S(2)}, u32[]{:S(2)}) %all-to-all-start.2) | async-done | bytes 655392 | tf_op jit(solution)/shard_map/all_to_all | solution.py:212
  164.7 2.1 %shard_map.114 = (bf16[48,512]{1,0:T(8,128)(2,1)}, f32[4,128]{1,0:T(4,128)}) custom-call(bf16[64,8,640]{2,1,0:T(8,128)(2,1)} %copy-done.1, f32[48,64]{1,0:T(8,128)} %get-tuple-element.46.code_ref, f32[48,512]{1,0:T(8,128)} %get-tuple-element.49.part_ref), custom_call_target="tpu_custom_call" | custom-call | flops 201326592 | bytes 4194304 | tf_op jit(solution)/shard_map/pallas_call | solution.py:265
  (90 shorter events, 12.4 us)
Async XLA Ops:
  46.0 20.7 %collective-permute-start = (bf16[256,1024]{1,0:T(8,128)(2,1)S(1)}, bf16[256,1024]{1,0:T(8,128)(2,1)S(1)}, u32[]{:S(2)}, u32[]{:S(2)}) collective-permute-start(bf16[256,1024]{1,0:T(8,128)(2,1)S(1)} %slice_bitcast_fusion), channel_id=1, source_target_pairs={{0,1},{1,2},{2,3},{3,0},{4,5},{5,6},{6,7},{7,4},{8,9},{9,10},{10,1... | collective-permute-start | bytes 1572872 | tf_op jit(solution)/shard_map/ppermute | solution.py:209
  47.3 22.7 %collective-permute-start.1 = (bf16[256,1024]{1,0:T(8,128)(2,1)S(1)}, bf16[256,1024]{1,0:T(8,128)(2,1)S(1)}, u32[]{:S(2)}, u32[]{:S(2)}) collective-permute-start(bf16[256,1024]{1,0:T(8,128)(2,1)S(1)} %slice_bitcast_fusion), channel_id=1, source_target_pairs={{0,3},{1,0},{2,1},{3,2},{4,7},{5,4},{6,5},{7,6},{8,11},{9,8},{10,9... | collective-permute-start | bytes 1572872 | tf_op jit(solution)/shard_map/ppermute | solution.py:209
  48.8 16.4 %collective-permute-start.8 = (bf16[128,1024]{1,0:T(8,128)(2,1)S(1)}, bf16[128,1024]{1,0:T(8,128)(2,1)S(1)}, u32[]{:S(2)}, u32[]{:S(2)}) collective-permute-start(bf16[128,1024]{1,0:T(8,128)(2,1)S(1)} %get-tuple-element.62), channel_id=1, source_target_pairs={{0,1},{1,2},{2,3},{3,0},{4,5},{5,6},{6,7},{7,4},{8,9},{9,10},{10,1... | collective-permute-start | bytes 786440 | tf_op jit(solution)/shard_map/ppermute | solution.py:209
  48.9 17.6 %collective-permute-start.11 = (bf16[128,1024]{1,0:T(8,128)(2,1)S(1)}, bf16[128,1024]{1,0:T(8,128)(2,1)S(1)}, u32[]{:S(2)}, u32[]{:S(2)}) collective-permute-start(bf16[128,1024]{1,0:T(8,128)(2,1)S(1)} %get-tuple-element.61), channel_id=1, source_target_pairs={{0,3},{1,0},{2,1},{3,2},{4,7},{5,4},{6,5},{7,6},{8,11},{9,8},{10,9... | collective-permute-start | bytes 786440 | tf_op jit(solution)/shard_map/ppermute | solution.py:209
  51.5 19.4 %collective-permute-start.9 = (bf16[128,1024]{1,0:T(8,128)(2,1)S(1)}, bf16[128,1024]{1,0:T(8,128)(2,1)S(1)}, u32[]{:S(2)}, u32[]{:S(2)}) collective-permute-start(bf16[128,1024]{1,0:T(8,128)(2,1)S(1)} %get-tuple-element.61), channel_id=1, source_target_pairs={{0,1},{1,2},{2,3},{3,0},{4,5},{5,6},{6,7},{7,4},{8,9},{9,10},{10,1... | collective-permute-start | bytes 786440 | tf_op jit(solution)/shard_map/ppermute | solution.py:209
  65.2 8.3 %collective-permute-start.10 = (bf16[128,1024]{1,0:T(8,128)(2,1)S(1)}, bf16[128,1024]{1,0:T(8,128)(2,1)S(1)}, u32[]{:S(2)}, u32[]{:S(2)}) collective-permute-start(bf16[128,1024]{1,0:T(8,128)(2,1)S(1)} %get-tuple-element.62), channel_id=1, source_target_pairs={{0,3},{1,0},{2,1},{3,2},{4,7},{5,4},{6,5},{7,6},{8,11},{9,8},{10,9... | collective-permute-start | bytes 786440 | tf_op jit(solution)/shard_map/ppermute | solution.py:209
  66.5 9.3 %collective-permute-start.12 = (bf16[128,1024]{1,0:T(8,128)(2,1)S(1)}, bf16[128,1024]{1,0:T(8,128)(2,1)S(1)}, u32[]{:S(2)}, u32[]{:S(2)}) collective-permute-start(bf16[128,1024]{1,0:T(8,128)(2,1)S(1)} %collective-permute-done.8.p0_ref.p1a), channel_id=1, source_target_pairs={{0,1},{1,2},{2,3},{3,0},{4,5},{5,6},{6,7},{7,4},{8,9},{9,10},{10,1... | collective-permute-start | bytes 786440 | tf_op jit(solution)/shard_map/ppermute | solution.py:209
  66.7 9.1 %collective-permute-start.13 = (bf16[128,1024]{1,0:T(8,128)(2,1)S(1)}, bf16[128,1024]{1,0:T(8,128)(2,1)S(1)}, u32[]{:S(2)}, u32[]{:S(2)}) collective-permute-start(bf16[128,1024]{1,0:T(8,128)(2,1)S(1)} %collective-permute-done.11.n1_ref.n1a), channel_id=1, source_target_pairs={{0,3},{1,0},{2,1},{3,2},{4,7},{5,4},{6,5},{7,6},{8,11},{9,8},{10,9... | collective-permute-start | bytes 786440 | tf_op jit(solution)/shard_map/ppermute | solution.py:209
  69.9 17.4 %collective-permute-start.2 = (bf16[128,1024]{1,0:T(8,128)(2,1)S(1)}, bf16[128,1024]{1,0:T(8,128)(2,1)S(1)}, u32[]{:S(2)}, u32[]{:S(2)}) collective-permute-start(bf16[128,1024]{1,0:T(8,128)(2,1)S(1)} %get-tuple-element.70.p0_ref), channel_id=1, source_target_pairs={{0,1},{1,2},{2,3},{3,0},{4,5},{5,6},{6,7},{7,4},{8,9},{9,10},{10,1... | collective-permute-start | bytes 786440 | tf_op jit(solution)/shard_map/ppermute | solution.py:209
  70.9 16.5 %collective-permute-start.3 = (bf16[128,1024]{1,0:T(8,128)(2,1)S(1)}, bf16[128,1024]{1,0:T(8,128)(2,1)S(1)}, u32[]{:S(2)}, u32[]{:S(2)}) collective-permute-start(bf16[128,1024]{1,0:T(8,128)(2,1)S(1)} %get-tuple-element.67.n1_ref), channel_id=1, source_target_pairs={{0,3},{1,0},{2,1},{3,2},{4,7},{5,4},{6,5},{7,6},{8,11},{9,8},{10,9... | collective-permute-start | bytes 786440 | tf_op jit(solution)/shard_map/ppermute | solution.py:209
  84.6 14.4 %collective-permute-start.14 = (bf16[256,512]{1,0:T(8,128)(2,1)}, bf16[256,512]{1,0:T(8,128)(2,1)S(1)}, u32[]{:S(2)}, u32[]{:S(2)}) collective-permute-start(bf16[256,512]{1,0:T(8,128)(2,1)} %get-tuple-element.41), channel_id=1, source_target_pairs={{0,1},{1,2},{2,3},{3,0},{4,5},{5,6},{6,7},{7,4},{8,9},{9,10},{10,1... | collective-permute-start | bytes 786440 | tf_op jit(solution)/shard_map/ppermute | solution.py:209
  85.4 33.1 %collective-permute-start.16 = (bf16[256,512]{1,0:T(8,128)(2,1)}, bf16[256,512]{1,0:T(8,128)(2,1)S(1)}, u32[]{:S(2)}, u32[]{:S(2)}) collective-permute-start(bf16[256,512]{1,0:T(8,128)(2,1)} %get-tuple-element.42), channel_id=1, source_target_pairs={{0,3},{1,0},{2,1},{3,2},{4,7},{5,4},{6,5},{7,6},{8,11},{9,8},{10,9... | collective-permute-start | bytes 786440 | tf_op jit(solution)/shard_map/ppermute | solution.py:209
  95.7 38.3 %copy-start.4 = (f32[256,512]{1,0:T(8,128)S(1)}, f32[256,512]{1,0:T(8,128)}, u32[]{:S(2)}) copy-start(f32[256,512]{1,0:T(8,128)} %get-tuple-element.39) | copy-start | bytes 1572868
  96.5 4.3 %collective-permute-start.20 = (f32[64,128]{1,0:T(8,128)S(1)}, f32[64,128]{1,0:T(8,128)S(1)}, u32[]{:S(2)}, u32[]{:S(2)}) collective-permute-start(f32[64,128]{1,0:T(8,128)S(1)} %constant_dynamic-update-slice_fusion), channel_id=1, source_target_pairs={{0,2},{1,3},{2,0},{3,1},{4,6},{5,7},{6,4},{7,5},{8,10},{9,11},{10,... | collective-permute-start | bytes 98312 | tf_op jit(solution)/shard_map/ppermute | solution.py:209
  97.5 3.3 %collective-permute-start.19 = (f32[64,128]{1,0:T(8,128)S(1)}, f32[64,128]{1,0:T(8,128)S(1)}, u32[]{:S(2)}, u32[]{:S(2)}) collective-permute-start(f32[64,128]{1,0:T(8,128)S(1)} %constant_dynamic-update-slice_fusion), channel_id=1, source_target_pairs={{0,3},{1,0},{2,1},{3,2},{4,7},{5,4},{6,5},{7,6},{8,11},{9,8},{10,9... | collective-permute-start | bytes 98312 | tf_op jit(solution)/shard_map/ppermute | solution.py:209
  98.4 5.1 %collective-permute-start.18 = (f32[64,128]{1,0:T(8,128)S(1)}, f32[64,128]{1,0:T(8,128)S(1)}, u32[]{:S(2)}, u32[]{:S(2)}) collective-permute-start(f32[64,128]{1,0:T(8,128)S(1)} %constant_dynamic-update-slice_fusion), channel_id=1, source_target_pairs={{0,1},{1,2},{2,3},{3,0},{4,5},{5,6},{6,7},{7,4},{8,9},{9,10},{10,1... | collective-permute-start | bytes 98312 | tf_op jit(solution)/shard_map/ppermute | solution.py:209
  99.0 34.9 %collective-permute-start.15 = (bf16[128,512]{1,0:T(8,128)(2,1)S(1)}, bf16[128,512]{1,0:T(8,128)(2,1)S(1)}, u32[]{:S(2)}, u32[]{:S(2)}) collective-permute-start(bf16[128,512]{1,0:T(8,128)(2,1)S(1)} %add_convert_fusion.3), channel_id=1, source_target_pairs={{0,1},{1,2},{2,3},{3,0},{4,5},{5,6},{6,7},{7,4},{8,9},{9,10},{10,1... | collective-permute-start | bytes 393224 | tf_op jit(solution)/shard_map/ppermute | solution.py:209
  100.8 30.2 %collective-permute-start.4 = (bf16[256,512]{1,0:T(8,128)(2,1)}, bf16[256,512]{1,0:T(8,128)(2,1)S(1)}, u32[]{:S(2)}, u32[]{:S(2)}) collective-permute-start(bf16[256,512]{1,0:T(8,128)(2,1)} %get-tuple-element.36), channel_id=1, source_target_pairs={{0,1},{1,2},{2,3},{3,0},{4,5},{5,6},{6,7},{7,4},{8,9},{9,10},{10,1... | collective-permute-start | bytes 786440 | tf_op jit(solution)/shard_map/ppermute | solution.py:209
  100.8 30.4 %collective-permute-start.6 = (bf16[256,512]{1,0:T(8,128)(2,1)}, bf16[256,512]{1,0:T(8,128)(2,1)S(1)}, u32[]{:S(2)}, u32[]{:S(2)}) collective-permute-start(bf16[256,512]{1,0:T(8,128)(2,1)} %get-tuple-element.37), channel_id=1, source_target_pairs={{0,3},{1,0},{2,1},{3,2},{4,7},{5,4},{6,5},{7,6},{8,11},{9,8},{10,9... | collective-permute-start | bytes 786440 | tf_op jit(solution)/shard_map/ppermute | solution.py:209
  104.1 23.8 %all-to-all-start.1 = ((f32[64,1,128]{2,1,0:T(1,128)}), f32[64,1,128]{2,1,0:T(1,128)S(1)}, u32[]{:S(2)}, u32[]{:S(2)}) async-start(f32[64,1,128]{2,1,0:T(1,128)} %bitcast.13), calls=%async_computation.1 | async-start | bytes 65536 | tf_op jit(solution)/shard_map/all_to_all | solution.py:212
  118.6 15.3 %collective-permute-start.17 = (bf16[128,512]{1,0:T(8,128)(2,1)S(1)}, bf16[128,512]{1,0:T(8,128)(2,1)S(1)}, u32[]{:S(2)}, u32[]{:S(2)}) collective-permute-start(bf16[128,512]{1,0:T(8,128)(2,1)S(1)} %add_convert_fusion.1), channel_id=1, source_target_pairs={{0,3},{1,0},{2,1},{3,2},{4,7},{5,4},{6,5},{7,6},{8,11},{9,8},{10,9... | collective-permute-start | bytes 393224 | tf_op jit(solution)/shard_map/ppermute | solution.py:209
  131.0 5.7 %collective-permute-start.5 = (bf16[128,512]{1,0:T(8,128)(2,1)S(1)}, bf16[128,512]{1,0:T(8,128)(2,1)S(1)}, u32[]{:S(2)}, u32[]{:S(2)}) collective-permute-start(bf16[128,512]{1,0:T(8,128)(2,1)S(1)} %add_convert_fusion.7), channel_id=1, source_target_pairs={{0,1},{1,2},{2,3},{3,0},{4,5},{5,6},{6,7},{7,4},{8,9},{9,10},{10,1... | collective-permute-start | bytes 393224 | tf_op jit(solution)/shard_map/ppermute | solution.py:209
  131.2 5.5 %collective-permute-start.7 = (bf16[128,512]{1,0:T(8,128)(2,1)S(1)}, bf16[128,512]{1,0:T(8,128)(2,1)S(1)}, u32[]{:S(2)}, u32[]{:S(2)}) collective-permute-start(bf16[128,512]{1,0:T(8,128)(2,1)S(1)} %add_convert_fusion.5), channel_id=1, source_target_pairs={{0,3},{1,0},{2,1},{3,2},{4,7},{5,4},{6,5},{7,6},{8,11},{9,8},{10,9... | collective-permute-start | bytes 393224 | tf_op jit(solution)/shard_map/ppermute | solution.py:209
  137.8 26.1 %all-to-all-start.2 = ((bf16[64,8,640]{2,1,0:T(8,128)(2,1)}), bf16[64,8,640]{2,1,0:T(8,128)(2,1)S(1)}, u32[]{:S(2)}, u32[]{:S(2)}) async-start(bf16[64,8,640]{2,1,0:T(8,128)(2,1)} %pad_maximum_fusion), calls=%async_computation.2 | async-start | bytes 1310720 | tf_op jit(solution)/shard_map/all_to_all | solution.py:212
  (22 other events, 263.1 us)

commit v4 on v3

v4 whole, which is shorter than its diff:
```python
import functools

import jax
import jax.numpy as jnp
from jax import lax
from jax.experimental import pallas as pl
from jax.experimental.pallas import tpu as pltpu
from jax.sharding import PartitionSpec as P


F32 = jnp.float32
BF16 = jnp.bfloat16
HI = lax.Precision.HIGHEST
VMEM = pl.BlockSpec(memory_space=pltpu.VMEM)
SMEM = pl.BlockSpec(memory_space=pltpu.SMEM)


def mm(a, b, dims, precision=None):
    return lax.dot_general(a, b, (dims, ((), ())), precision=precision, preferred_element_type=F32)


NN = ((1,), (0,))
NT = ((1,), (1,))
TN = ((0,), (0,))


def iota(shape, dim):
    return lax.broadcasted_iota(jnp.int32, shape, dim)


def bits(cap):
    return cap.bit_length() - 1


def spread(experts, cap):
    rows = experts * cap
    return ((iota((rows, experts), 0) >> bits(cap)) == iota((rows, experts), 1)).astype(F32)


def dispatch_kernel(cap, tp_ref, tok_ref, og_ref, ids_ref, rw_ref, send_ref, code_ref, gate_ref):
    n_tok = tok_ref.shape[0]
    experts = rw_ref.shape[0]
    share = send_ref.shape[1] // 2
    start = pl.multiple_of(tp_ref[0] * share, share)
    logits = mm(tok_ref[...], rw_ref[...], NT)
    ids = ids_ref[...].astype(F32).T
    lane = iota((n_tok, experts), 1).astype(F32)
    hit = lane == ids[:, 0:1]
    for k in range(1, ids.shape[1]):
        hit = hit | (lane == ids[:, k : k + 1])
    mask = hit.astype(F32)
    top = jnp.max(jnp.where(hit, logits, -jnp.inf), axis=1, keepdims=True)
    weight = jnp.where(hit, jnp.exp(jnp.where(hit, logits - top, 0.0)), 0.0)
    gate = weight / jnp.sum(weight, axis=1, keepdims=True)
    earlier = (iota((n_tok, n_tok), 1) < iota((n_tok, n_tok), 0)).astype(BF16)
    rank = mm(earlier, mask.astype(BF16), NN)
    code = mask * (rank + 1.0)
    code_ref[...] = code
    gate_ref[...] = gate
    expand = spread(experts, cap)
    rows = experts * cap
    code_of = mm(expand.astype(BF16), code.astype(BF16), NT)
    pick = code_of == ((iota((rows, n_tok), 0) & (cap - 1)) + 1).astype(F32)
    gate_of = jnp.where(pick, mm(expand, gate, NT, HI), 0.0)
    send_ref[:, :share] = mm(pick.astype(F32).astype(BF16), tok_ref[:, pl.ds(start, share)], NN).astype(BF16)
    cot = og_ref[:, pl.ds(start, share)].astype(F32)
    send_ref[:, share:] = mm(gate_of, cot, NN, HI).astype(BF16)


LEFT, RIGHT = 0, 1


def joined(refs, side):
    share = refs[0].shape[1] // 2
    return jnp.concatenate([r[:, side * share : (side + 1) * share] for r in refs], axis=0)


def block(tp_ref, off, share):
    return pl.ds(pl.multiple_of(lax.rem(tp_ref[0] + off, 4) * share, share), share)


def fetch(tp_ref, offs, share, hbm, vmem, sems):
    copies = {}
    for i, off in enumerate(offs):
        at = block(tp_ref, off, share)
        row = []
        for j, (source, target) in enumerate(zip(hbm, vmem)):
            where = (slice(None), at) if j == 2 else (at, slice(None))
            row.append(pltpu.make_async_copy(source.at[where], target.at[where], sems.at[i * len(hbm) + j]))
            row[-1].start()
        copies[off] = row
    return copies


def forward(tp_ref, groups, copies, share, wg, wu, wd, start=None):
    total = start
    for off, refs in groups:
        for copy in copies[off]:
            copy.wait()
        at = block(tp_ref, off, share)
        t, g = joined(refs, LEFT), joined(refs, RIGHT)
        terms = (mm(t, wg[at, :], NN), mm(t, wu[at, :], NN), mm(g, wd[:, at], NT))
        total = terms if total is None else tuple(a + b for a, b in zip(total, terms))
    return total


def units(cap, gate_pre, up_pre, back):
    rows = gate_pre.shape[0]
    glu = jnp.minimum(gate_pre, 7.0)
    linear = jnp.clip(up_pre, -7.0, 7.0)
    sig = jax.nn.sigmoid(1.702 * glu)
    act = glu * sig
    hidden = (linear + 1.0) * act
    slope = (linear + 1.0) * (sig + 1.702 * glu * sig * (1.0 - sig))
    slope = jnp.where(gate_pre < 7.0, slope, 0.0)
    up_slope = jnp.where((up_pre > -7.0) & (up_pre < 7.0), act, 0.0)
    score = jnp.sum(hidden * back, axis=1, keepdims=True)
    peers = rows // cap
    spot = ((iota((rows, 128), 0) & (cap - 1)) == iota((rows, 128), 1)).astype(F32) * score
    group = ((iota((peers, rows), 1) >> bits(cap)) == iota((peers, rows), 0)).astype(F32)
    return (
        hidden.astype(BF16),
        (back * slope).astype(BF16),
        (back * up_slope).astype(BF16),
        mm(group, spot, NN, HI),
    )


def token_parts(tp_ref, dg, du, wg, wu, outs, copies=None):
    plus_ref, minus_ref, b1_ref, b3_ref, b0_ref = outs
    rows, share = b0_ref.shape
    half = rows // 2

    def part(off):
        for copy in copies[off] if copies else ():
            copy.wait()
        at = block(tp_ref, off, share)
        return mm(dg, wg[at, :], NT) + mm(du, wu[at, :], NT)

    far = part(2).astype(BF16)
    plus_ref[:half, :] = far[:half]
    minus_ref[half:, :] = far[half:]
    ahead = part(1)
    b1_ref[...] = ahead[:half]
    plus_ref[half:, :] = ahead[half:].astype(BF16)
    behind = part(3)
    minus_ref[:half, :] = behind[:half].astype(BF16)
    b3_ref[...] = behind[half:]
    b0_ref[...] = part(0)


def first_kernel(cap, tp_ref, own, p0, n0, f0a, f0b, wg_hbm, wu_hbm, wd_hbm,
                 hid_ref, dg_ref, du_ref, score_ref, plus_ref, minus_ref, b1_ref, b3_ref, b0_ref,
                 wg, wu, wd, sems):
    share = b0_ref.shape[1]
    copies = fetch(tp_ref, (0, 3, 1, 2), share, (wg_hbm, wu_hbm, wd_hbm), (wg, wu, wd), sems)
    groups = ((0, (own,)), (3, (p0,)), (1, (n0,)), (2, (f0a, f0b)))
    hid, dg, du, score = units(cap, *forward(tp_ref, groups, copies, share, wg, wu, wd))
    hid_ref[...], dg_ref[...], du_ref[...], score_ref[...] = hid, dg, du, score
    token_parts(tp_ref, dg, du, wg, wu, (plus_ref, minus_ref, b1_ref, b3_ref, b0_ref))


def near_kernel(tp_ref, own, p1a, p1b, n1a, n1b, wg_hbm, wu_hbm, wd_hbm, gp_ref, up_ref, bk_ref, wg, wu, wd, sems):
    share = own.shape[1] // 2
    copies = fetch(tp_ref, (0, 3, 1), share, (wg_hbm, wu_hbm, wd_hbm), (wg, wu, wd), sems)
    groups = ((0, (own,)), (3, (p1a, p1b)), (1, (n1b, n1a)))
    gp_ref[...], up_ref[...], bk_ref[...] = forward(tp_ref, groups, copies, share, wg, wu, wd)


def far_kernel(cap, tp_ref, f1a, f1b, gp, up, bk, score0, wg_hbm, wu_hbm, wd_hbm,
               hid_ref, dg_ref, du_ref, score_ref, wg, wu, wd, sems):
    share = f1a.shape[1] // 2
    copies = fetch(tp_ref, (2,), share, (wg_hbm, wu_hbm, wd_hbm), (wg, wu, wd), sems)
    start = (gp[...], up[...], bk[...])
    hid, dg, du, score = units(cap, *forward(tp_ref, ((2, (f1a, f1b)),), copies, share, wg, wu, wd, start))
    hid_ref[...], dg_ref[...], du_ref[...] = hid, dg, du
    score_ref[...] = jnp.concatenate([score0[...], score], axis=0)


def token_kernel(tp_ref, dg_ref, du_ref, wg_hbm, wu_hbm, plus_ref, minus_ref, b1_ref, b3_ref, b0_ref, wg, wu, sems):
    share = b0_ref.shape[1]
    copies = fetch(tp_ref, (2, 1, 3, 0), share, (wg_hbm, wu_hbm), (wg, wu), sems)
    token_parts(tp_ref, dg_ref[...], du_ref[...], wg, wu, (plus_ref, minus_ref, b1_ref, b3_ref, b0_ref), copies)


def weight_kernel(tp_ref, own, p0, p1a, p1b, n0, n1a, n1b, f0a, f0b, f1a, f1b, hid0, hid1, dg0, dg1, du0, du1,
                  d_logits_ref, rw_ref, gwg_ref, gwu_ref, gwd_ref, part_ref):
    share = own.shape[1] // 2
    part_ref[...] = mm(d_logits_ref[...], rw_ref[:, block(tp_ref, 0, share)].astype(F32), NN, HI)

    def rows(a, b):
        return jnp.concatenate([a[...], b[...]], axis=0)

    hid, dg, du = rows(hid0, hid1), rows(dg0, dg1), rows(du0, du1)
    for off, refs in ((0, (own,)), (3, (p0, p1a, p1b)), (1, (n0, n1b, n1a)), (2, (f0a, f0b, f1a, f1b))):
        at = block(tp_ref, off, share)
        t, g = joined(refs, LEFT), joined(refs, RIGHT)
        gwg_ref[at, :] = mm(t, dg, TN).astype(BF16)
        gwu_ref[at, :] = mm(t, du, TN).astype(BF16)
        gwd_ref[:, at] = mm(hid, g, TN).astype(BF16)


def router_kernel(cap, tp_ref, q_ref, code_ref, gate_ref, tok_ref, *refs):
    sums, (payload_ref, d_logits_ref) = refs[:10], refs[10:]
    share = sums[0].shape[1]
    for h in range(2):
        b0, rp, rm, ep, em = sums[5 * h : 5 * h + 5]
        half = b0.shape[0] // 2
        top = b0[:half] + ep[...].astype(F32) + rm[:half].astype(F32)
        low = b0[half:] + rp[half:].astype(F32) + em[...].astype(F32)
        for i, value in enumerate((top, low)):
            n = half // cap
            at = pl.ds((2 * h + i) * n, n)
            payload_ref[at, :, :share] = value.astype(BF16).reshape(n, cap, share)
    code, gate = code_ref[...], gate_ref[...]
    q = q_ref[...].T
    score = jnp.zeros_like(code)
    for r in range(cap):
        score = score + jnp.where(code == r + 1.0, q[r : r + 1, :], 0.0)
    d_logits = score - gate * jnp.sum(score, axis=1, keepdims=True)
    d_logits_ref[...] = d_logits
    term = mm(d_logits, tok_ref[:, block(tp_ref, 0, share)].astype(F32), TN, HI)
    high = term.astype(BF16)
    low = (term - high.astype(F32)).astype(BF16)
    pieces = share // 128
    for j in range(pieces):
        payload_ref[:, j, share:] = high[:, j * 128 : (j + 1) * 128]
        payload_ref[:, pieces + j, share:] = low[:, j * 128 : (j + 1) * 128]


def home_kernel(cap, home_ref, code_ref, part_ref, tok_out_ref, router_ref):
    share = part_ref.shape[1]
    code = code_ref[...]
    n_tok, experts = code.shape
    rows = experts * cap
    code_of = mm(code.astype(BF16), spread(experts, cap).astype(BF16), NT)
    pick = code_of == ((iota((n_tok, rows), 1) & (cap - 1)) + 1).astype(F32)
    flat = home_ref[...].reshape(rows, home_ref.shape[2])
    tok_out_ref[...] = (
        mm(pick.astype(F32).astype(BF16), flat[:, :share], NN) + part_ref[...]
    ).astype(BF16)
    both = jnp.sum(home_ref[:, :, share:].astype(F32), axis=0)
    pieces = share // 128
    router_ref[...] = both[:pieces] + both[pieces:]


def cost(flops, data):
    return pl.CostEstimate(flops=flops, bytes_accessed=data, transcendentals=0)


def call(body, outs, n_in, flops, scalar=True, hbm=0, scratch=(), own=None):
    ins = ([SMEM] if scalar else []) + [VMEM] * n_in + [pl.BlockSpec(memory_space=pl.ANY)] * hbm
    if own is not None:
        dims, at = own
        ins[1] = pl.BlockSpec(dims, lambda i: (at, 0))
    return pl.pallas_call(
        body,
        out_shape=outs,
        grid=(1,),
        in_specs=ins,
        out_specs=[VMEM] * len(outs),
        scratch_shapes=list(scratch),
        cost_estimate=cost(flops, 4 << 20),
    )


def shape(dims, dtype):
    return jax.ShapeDtypeStruct(dims, dtype)


def per_device(tokens, out_grad, expert_ids, router_weight, w_gate, w_up, w_down):
    n_tok, width = tokens.shape
    experts = router_weight.shape[1]
    peers = lax.axis_size("ep")
    tp = lax.axis_size("tp")
    cap = 8
    share = width // tp
    ff = w_gate.shape[2]
    rows = peers * cap
    half = rows // 2
    me = jnp.full((1,), lax.axis_index("tp"), jnp.int32)
    unit = 2 * rows * share * ff
    router_t = router_weight.T

    def hop(value, by):
        return lax.ppermute(value, "tp", [(i, (i + by) % tp) for i in range(tp)])

    def exchange(value):
        return lax.all_to_all(value, "ep", split_axis=0, concat_axis=0, tiled=True)

    send, code, gate = call(
        functools.partial(dispatch_kernel, cap),
        [shape((rows, 2 * share), BF16), shape((n_tok, experts), F32), shape((n_tok, experts), F32)],
        4,
        unit,
    )(me, tokens, out_grad, expert_ids.T, router_t)
    own = exchange(send.reshape(peers, cap, 2 * share)).reshape(rows, 2 * share)
    piece = half // 2
    own1a, own1b = own[half : half + piece], own[half + piece :]
    p0, n0 = hop(own[:half], 1), hop(own[:half], -1)
    p1a, n1a = hop(own1a, 1), hop(own1b, -1)
    f0a, f0b = hop(p0[:piece], 1), hop(n0[piece:], -1)
    p1b, n1b = hop(own1b, 1), hop(own1a, -1)
    f1a, f1b = hop(p1a, 1), hop(n1a, -1)
    wg, wu, wd = w_gate[0], w_up[0], w_down[0]
    w_scratch = [pltpu.VMEM((width, ff), BF16), pltpu.VMEM((width, ff), BF16), pltpu.VMEM((ff, width), BF16)]

    def sems(n):
        return [pltpu.SemaphoreType.DMA((n,))]

    grads = [shape((half, ff), BF16)] * 3
    parts = (
        [shape((half, share), BF16)] * 2 + [shape((piece, share), F32)] * 2 + [shape((half, share), F32)]
    )
    hid0, dg0, du0, score0, *parts0 = call(
        functools.partial(first_kernel, cap),
        grads + [shape((half // cap, 128), F32)] + parts,
        5,
        10 * unit,
        hbm=3,
        scratch=w_scratch + sems(12),
        own=((half, 2 * share), 0),
    )(me, own, p0, n0, f0a, f0b, wg, wu, wd)
    near = call(
        near_kernel,
        [shape((half, ff), F32)] * 3,
        5,
        5 * unit,
        hbm=3,
        scratch=w_scratch + sems(9),
        own=((half, 2 * share), 1),
    )(me, own, p1a, p1b, n1a, n1b, wg, wu, wd)
    hid1, dg1, du1, score = call(
        functools.partial(far_kernel, cap),
        grads + [shape((peers, 128), F32)],
        6,
        3 * unit,
        hbm=3,
        scratch=w_scratch + sems(3),
    )(me, f1a, f1b, *near, score0, wg, wu, wd)
    parts1 = call(token_kernel, parts, 2, 4 * unit, hbm=2, scratch=w_scratch[:2] + sems(8))(me, dg1, du1, wg, wu)

    def summed(plus, minus, b1, b3, b0):
        rp, rm = hop(plus, 1), hop(minus, -1)
        ep = hop((b1 + rp[:piece].astype(F32)).astype(BF16), 1)
        em = hop((b3 + rm[piece:].astype(F32)).astype(BF16), -1)
        return b0, rp, rm, ep, em

    sums = summed(*parts0) + summed(*parts1)
    score = score + hop(score, 1) + hop(score, -1) + hop(score, 2)
    q = exchange(score.reshape(peers, 1, 128)).reshape(peers, 128)
    payload, d_logits = call(
        functools.partial(router_kernel, cap),
        [shape((peers, cap, share + 128), BF16), shape((n_tok, experts), F32)],
        14,
        unit,
    )(me, q, code, gate, tokens, *sums)
    home = exchange(payload)
    gwg, gwu, gwd, part = call(
        weight_kernel,
        [shape((width, ff), BF16), shape((width, ff), BF16), shape((ff, width), BF16), shape((n_tok, share), F32)],
        19,
        12 * unit,
    )(me, own, p0, p1a, p1b, n0, n1a, n1b, f0a, f0b, f1a, f1b, hid0, hid1, dg0, dg1, du0, du1, d_logits, router_t)
    token_grad, router = call(
        functools.partial(home_kernel, cap),
        [shape((n_tok, share), BF16), shape((share // 128, 128), F32)],
        3,
        unit,
        scalar=False,
    )(home, code, part)
    return (token_grad, router.reshape(share, 1), gwg[None], gwu[None], gwd[None])


def solution(mesh):
    in_specs = (
        P("ep", None),
        P("ep", None),
        P("ep", None),
        P(),
        P("ep", None, "tp"),
        P("ep", None, "tp"),
        P("ep", "tp", None),
    )
    out_specs = (
        P("ep", "tp"),
        P("tp", "ep"),
        P("ep", None, "tp"),
        P("ep", None, "tp"),
        P("ep", "tp", None),
    )

    return jax.shard_map(per_device, mesh=mesh, in_specs=in_specs, out_specs=out_specs, check_vma=False)
```

time: 167 us -> 174 us (1.042)
  blocking collectives: 41.3 us -> 66.3 us
  starting transfers between devices: 43.4 us -> 29.5 us
  waiting for transfers between devices: 42.2 us -> 31 us
  Pallas kernels: 30.9 us -> 39.6 us
    all_to_all x1 -> x2, blocking collectives: 41.3 us -> 66.3 us  [exchange(): return lax.all_to_all(value, 'ep', split_axis=0, concat_axis=0, tiled=True)]
    all_to_all x2 -> x1, starting transfers between devices: 20 us -> 4.55 us  [exchange(): return lax.all_to_all(value, 'ep', split_axis=0, concat_axis=0, tiled=True)]
    all_to_all x2 -> x1, waiting for transfers between devices: 22.2 us -> 12.9 us  [exchange(): return lax.all_to_all(value, 'ep', split_axis=0, concat_axis=0, tiled=True)]
    pallas_call x3 -> x5, Pallas kernels: 17.4 us -> 25.9 us  [the longest x1 7.63 us: per_device(): call(functools.partial(first_kernel, cap), grads + [shape((half // cap, 1...]
    ppermute x21, waiting for transfers between devices: 20 us -> 18.1 us  [hop(): return lax.ppermute(value, 'tp', [(i, (i + by) % tp) for i in range(tp)])]
    unnamed x47 -> x50, local copies, waits for them, and re-layouts: 4.53 us -> 5.34 us
  transfers between devices with their start and end apart: 23 -> 22, of which waited for: 6 -> 5; matrix products, arithmetic and copies ran while one was open for 2% -> 1% of each run, Pallas kernels for 15% -> 17%
where the time goes in v4:
time: 174 us
  blocking collectives  66.3 us (38%)
  Pallas kernels  39.6 us (23%)
  waiting for transfers between devices  31 us (18%)
  starting transfers between devices  29.5 us (17%)
  local copies, waits for them, and re-layouts  5.44 us (3%)
    all_to_all x2, blocking collectives, exchange(): return lax.all_to_all(value, 'ep', split_axis=0, concat_axis=0, tiled=True)  66.3 us
    ppermute x21, starting transfers between devices, hop(): return lax.ppermute(value, 'tp', [(i, (i + by) % tp) for i in range(tp)])  24.9 us
    ppermute x21, waiting for transfers between devices, hop(): return lax.ppermute(value, 'tp', [(i, (i + by) % tp) for i in range(tp)])  18.1 us
    all_to_all x1, waiting for transfers between devices, exchange(): return lax.all_to_all(value, 'ep', split_axis=0, concat_axis=0, tiled=True)  12.9 us
    pallas_call x1, Pallas kernels, per_device(): call(functools.partial(first_kernel, cap), grads + [shape((half // cap, 1...  7.63 us
    pallas_call x1, Pallas kernels, per_device(): call(weight_kernel, [shape((width, ff), BF16), shape((width, ff), BF16),...  7.61 us
    pallas_call x1, Pallas kernels, per_device(): call(near_kernel, [shape((half, ff), F32)] * 3, 5, 5 * unit, hbm=3, scrat...  5.35 us
    unnamed x50, local copies, waits for them, and re-layouts  5.34 us
  transfers between devices with their start and end apart: 22, of which 5 were waited for; matrix products, arithmetic and copies ran while one was open for 1% of the time, Pallas kernels for 17%

profile of v4, /device:TPU:1, one launch (start us, length us, event | category | flops | bytes accessed | tf_op | source)
XLA Modules:
  0.0 173.9 jit_solution(8216613022320297623)
XLA Ops:
  0.6 4.0 %shard_map.110 = (bf16[512,1024]{1,0:T(8,128)(2,1)}, f32[48,64]{1,0:T(8,128)}, f32[48,64]{1,0:T(8,128)}) custom-call(s32[1]{0:T(128)} %bitcast.tp_ref, bf16[48,2048]{1,0:T(8,128)(2,1)} %tok_ref.3, bf16[48,2048]{1,0:T(8,128)(2,1)} %og_ref.1, s32[4,48]{1,0:T(4,128)} %bitcast.41, bf16[64,2048]{1,0:T(8,128)(2,1)} %bitcast.39), custom_call_target="tpu_custom_call" | custom-call | flops 201326592 | bytes 4194304 | tf_op jit(solution)/shard_map/pallas_call | solution.py:291
  4.6 41.3 %all_to_all.15 = bf16[64,8,1024]{2,1,0:T(8,128)(2,1)S(1)} all-to-all(bf16[64,8,1024]{2,1,0:T(8,128)(2,1)} %bitcast.36), channel_id=1, replica_groups=mesh['ep'=64,'tp'=4] {'ep'}, dimensions={0} | all-to-all | bytes 2097152 | tf_op jit(solution)/shard_map/all_to_all | solution.py:289
  47.3 1.5 collective-permute-start.7
  48.9 2.7 %collective-permute-start.2 = (bf16[128,1024]{1,0:T(8,128)(2,1)S(1)}, bf16[128,1024]{1,0:T(8,128)(2,1)S(1)}, u32[]{:S(2)}, u32[]{:S(2)}) collective-permute-start(bf16[128,1024]{1,0:T(8,128)(2,1)S(1)} %get-tuple-element.69), channel_id=1, source_target_pairs={{0,3},{1,0},{2,1},{3,2},{4,7},{5,4},{6,5},{7,6},{8,11},{9,8},{10,9... | collective-permute-start | bytes 786440 | tf_op jit(solution)/shard_map/ppermute | solution.py:286
  51.5 8.1 %collective-permute-done.6.p0 = bf16[256,1024]{1,0:T(8,128)(2,1)S(1)} collective-permute-done((bf16[256,1024]{1,0:T(8,128)(2,1)S(1)}, bf16[256,1024]{1,0:T(8,128)(2,1)S(1)}, u32[]{:S(2)}, u32[]{:S(2)}) %collective-permute-start.6) | collective-permute-done | bytes 524320 | tf_op jit(solution)/shard_map/ppermute | solution.py:286
  60.6 2.6 %collective-permute-start.9 = (bf16[128,1024]{1,0:T(8,128)(2,1)S(1)}, bf16[128,1024]{1,0:T(8,128)(2,1)S(1)}, u32[]{:S(2)}, u32[]{:S(2)}) collective-permute-start(bf16[128,1024]{1,0:T(8,128)(2,1)S(1)} %slice.53), channel_id=1, source_target_pairs={{0,3},{1,0},{2,1},{3,2},{4,7},{5,4},{6,5},{7,6},{8,11},{9,8},{10,9... | collective-permute-start | bytes 786440 | tf_op jit(solution)/shard_map/ppermute | solution.py:286
  63.2 2.0 %collective-permute-done.p1a = bf16[128,1024]{1,0:T(8,128)(2,1)S(1)} collective-permute-done((bf16[128,1024]{1,0:T(8,128)(2,1)S(1)}, bf16[128,1024]{1,0:T(8,128)(2,1)S(1)}, u32[]{:S(2)}, u32[]{:S(2)}) %collective-permute-start) | collective-permute-done | bytes 262176 | tf_op jit(solution)/shard_map/ppermute | solution.py:286
  66.7 4.1 %collective-permute-done.8.f0a = bf16[128,1024]{1,0:T(8,128)(2,1)S(1)} collective-permute-done((bf16[128,1024]{1,0:T(8,128)(2,1)S(1)}, bf16[128,1024]{1,0:T(8,128)(2,1)S(1)}, u32[]{:S(2)}, u32[]{:S(2)}) %collective-permute-start.8) | collective-permute-done | bytes 262176 | tf_op jit(solution)/shard_map/ppermute | solution.py:286
  72.8 7.6 %shard_map.112 = (bf16[256,384]{1,0:T(8,128)(2,1)}, bf16[256,384]{1,0:T(8,128)(2,1)}, bf16[256,384]{1,0:T(8,128)(2,1)}, f32[32,128]{1,0:T(8,128)}, bf16[256,512]...) custom-call(s32[1]{0:T(128)} %bitcast.tp_ref, ...), custom_call_target="tpu_custom_call" | custom-call | flops 2013265920 | bytes 4194304 | tf_op jit(solution)/shard_map/pallas_call | solution.py:315
  82.2 5.4 %shard_map.111 = (f32[256,384]{1,0:T(8,128)}, f32[256,384]{1,0:T(8,128)}, f32[256,384]{1,0:T(8,128)}) custom-call(s32[1]{0:T(128)} %bitcast.tp_ref, bf16[512,1024]{1,0:T(8,128)(2,1)} %bitcast.31, bf16[128,1024]{1,0:T(8,128)(2,1)} %copy-done.6, bf16[128,1024]{1,0:T(8,128)(2,1)} %copy-done.8, bf16[128,1024]{1,0:T(8,128)(2,1)} %copy-done.7, ...), custom_call_target="tpu_custom_call" | custom-call | flops 1006632960 | bytes 4194304 | tf_op jit(solution)/shard_map/pallas_call | solution.py:324
  88.4 4.4 %shard_map.113 = (bf16[256,384]{1,0:T(8,128)(2,1)}, bf16[256,384]{1,0:T(8,128)(2,1)}, bf16[256,384]{1,0:T(8,128)(2,1)}, f32[64,128]{1,0:T(8,128)}) custom-call(s32[1]{0:T(128)} %bitcast.tp_ref, bf16[128,1024]{1,0:T(8,128)(2,1)} %copy-done.10, bf16[128,1024]{1,0:T(8,128)(2,1)} %copy-done.11, f32[256,384]{1,0:T(8,128)} %get-tuple-element.38.gp, ...), custom_call_target="tpu_custom_call" | custom-call | flops 603979776 | bytes 4194304 | tf_op jit(solution)/shard_map/pallas_call | solution.py:333
  92.7 2.1 %collective-permute-start.12 = (f32[64,128]{1,0:T(8,128)}, f32[64,128]{1,0:T(8,128)S(1)}, u32[]{:S(2)}, u32[]{:S(2)}) collective-permute-start(f32[64,128]{1,0:T(8,128)} %get-tuple-element.42), channel_id=1, source_target_pairs={{0,2},{1,3},{2,0},{3,1},{4,6},{5,7},{6,4},{7,5},{8,10},{9,11},{10,... | collective-permute-start | bytes 98312 | tf_op jit(solution)/shard_map/ppermute | solution.py:286
  96.3 1.9 %collective-permute-start.14 = (bf16[256,512]{1,0:T(8,128)(2,1)S(1)}, bf16[256,512]{1,0:T(8,128)(2,1)S(1)}, u32[]{:S(2)}, u32[]{:S(2)}) collective-permute-start(bf16[256,512]{1,0:T(8,128)(2,1)S(1)} %copy-done.24), channel_id=1, source_target_pairs={{0,3},{1,0},{2,1},{3,2},{4,7},{5,4},{6,5},{7,6},{8,11},{9,8},{10,9... | collective-permute-start | bytes 786440 | tf_op jit(solution)/shard_map/ppermute | solution.py:286
  98.3 4.9 %shard_map.114 = (bf16[256,512]{1,0:T(8,128)(2,1)}, bf16[256,512]{1,0:T(8,128)(2,1)}, f32[128,512]{1,0:T(8,128)}, f32[128,512]{1,0:T(8,128)}, f32[256,512]{1,0:T(8,128)}) custom-call(s32[1]{0:T(128)} %bitcast.tp_ref, bf16[256,384]{1,0:T(8,128)(2,1)} %get-tuple-element.50.dg_ref.dg1, bf16[256,384]{1,0:T(8,128)(2,1)} %get-tuple-element.51.du_ref.du1, ...), custom_call_target="tpu_custom_call" | custom-call | flops 805306368 | bytes 4194304 | tf_op jit(solution)/shard_map/pallas_call | solution.py:341
  103.4 2.7 %collective-permute-start.18 = (bf16[256,512]{1,0:T(8,128)(2,1)}, bf16[256,512]{1,0:T(8,128)(2,1)S(1)}, u32[]{:S(2)}, u32[]{:S(2)}) collective-permute-start(bf16[256,512]{1,0:T(8,128)(2,1)} %get-tuple-element.54), channel_id=1, source_target_pairs={{0,3},{1,0},{2,1},{3,2},{4,7},{5,4},{6,5},{7,6},{8,11},{9,8},{10,9... | collective-permute-start | bytes 786440 | tf_op jit(solution)/shard_map/ppermute | solution.py:286
  106.2 3.8 %collective-permute-done.17.refs_6_ = bf16[256,512]{1,0:T(8,128)(2,1)S(1)} collective-permute-done((bf16[256,512]{1,0:T(8,128)(2,1)}, bf16[256,512]{1,0:T(8,128)(2,1)S(1)}, u32[]{:S(2)}, u32[]{:S(2)}) %collective-permute-start.17) | collective-permute-done | bytes 262176 | tf_op jit(solution)/shard_map/ppermute | solution.py:286
  111.1 2.7 %collective-permute-start.16 = (bf16[128,512]{1,0:T(8,128)(2,1)S(1)}, bf16[128,512]{1,0:T(8,128)(2,1)S(1)}, u32[]{:S(2)}, u32[]{:S(2)}) collective-permute-start(bf16[128,512]{1,0:T(8,128)(2,1)S(1)} %add_convert_fusion.2), channel_id=1, source_target_pairs={{0,3},{1,0},{2,1},{3,2},{4,7},{5,4},{6,5},{7,6},{8,11},{9,8},{10,9... | collective-permute-start | bytes 393224 | tf_op jit(solution)/shard_map/ppermute | solution.py:286
  113.9 2.7 %collective-permute-start.20 = (bf16[128,512]{1,0:T(8,128)(2,1)S(1)}, bf16[128,512]{1,0:T(8,128)(2,1)S(1)}, u32[]{:S(2)}, u32[]{:S(2)}) collective-permute-start(bf16[128,512]{1,0:T(8,128)(2,1)S(1)} %add_convert_fusion), channel_id=1, source_target_pairs={{0,3},{1,0},{2,1},{3,2},{4,7},{5,4},{6,5},{7,6},{8,11},{9,8},{10,9... | collective-permute-start | bytes 393224 | tf_op jit(solution)/shard_map/ppermute | solution.py:286
  116.5 24.9 %all_to_all.16 = f32[64,1,128]{2,1,0:T(1,128)} all-to-all(f32[64,1,128]{2,1,0:T(1,128)S(1)} %bitcast.38), channel_id=1, replica_groups=mesh['ep'=64,'tp'=4] {'ep'}, dimensions={0} | all-to-all | bytes 65536 | tf_op jit(solution)/shard_map/all_to_all | solution.py:289
  142.3 3.7 %shard_map.115 = (bf16[64,8,640]{2,1,0:T(8,128)(2,1)}, f32[48,64]{1,0:T(8,128)}) custom-call(s32[1]{0:T(128)} %bitcast.tp_ref, f32[64,128]{1,0:T(8,128)} %bitcast.37, f32[48,64]{1,0:T(8,128)} %get-tuple-element.43.code_ref, f32[48,64]{1,0:T(8,128)} %get-tuple-element.44.gate_ref, bf16[48,2048]{1,0:T(8,128)(2,1)} %tok_ref.3, ...), custom_call_target="tpu_custom_call" | custom-call | flops 201326592 | bytes 4194304 | tf_op jit(solution)/shard_map/pallas_call | solution.py:352
  146.0 4.5 %all-to-all-start.2 = ((bf16[64,8,640]{2,1,0:T(8,128)(2,1)}), bf16[64,8,640]{2,1,0:T(8,128)(2,1)S(1)}, u32[]{:S(2)}, u32[]{:S(2)}) async-start(bf16[64,8,640]{2,1,0:T(8,128)(2,1)} %get-tuple-element.57), calls=%async_computation.2 | async-start | bytes 1310720 | tf_op jit(solution)/shard_map/all_to_all | solution.py:289
  150.5 7.6 %shard_map.116 = (bf16[2048,384]{1,0:T(8,128)(2,1)}, bf16[2048,384]{1,0:T(8,128)(2,1)}, bf16[384,2048]{1,0:T(8,128)(2,1)}, f32[48,512]{1,0:T(8,128)}) custom-call(s32[1]{0:T(128)} %bitcast.tp_ref, bf16[512,1024]{1,0:T(8,128)(2,1)} %bitcast.32, bf16[256,1024]{1,0:T(8,128)(2,1)} %copy-done.19, bf16[128,1024]{1,0:T(8,128)(2,1)} %copy-done.6, ...), custom_call_target="tpu_custom_call" | custom-call | flops 2415919104 | bytes 4194304 | tf_op jit(solution)/shard_map/pallas_call | solution.py:359
  158.1 12.9 %all-to-all-done.2.home_ref = bf16[64,8,640]{2,1,0:T(8,128)(2,1)S(1)} async-done(((bf16[64,8,640]{2,1,0:T(8,128)(2,1)}), bf16[64,8,640]{2,1,0:T(8,128)(2,1)S(1)}, u32[]{:S(2)}, u32[]{:S(2)}) %all-to-all-start.2) | async-done | bytes 655392 | tf_op jit(solution)/shard_map/all_to_all | solution.py:289
  171.9 2.1 %shard_map.117 = (bf16[48,512]{1,0:T(8,128)(2,1)}, f32[4,128]{1,0:T(4,128)}) custom-call(bf16[64,8,640]{2,1,0:T(8,128)(2,1)} %copy-done.1, f32[48,64]{1,0:T(8,128)} %get-tuple-element.43.code_ref, f32[48,512]{1,0:T(8,128)} %get-tuple-element.63.part_ref), custom_call_target="tpu_custom_call" | custom-call | flops 201326592 | bytes 4194304 | tf_op jit(solution)/shard_map/pallas_call | solution.py:365
  (89 shorter events, 12.7 us)
Async XLA Ops:
  46.0 13.6 %collective-permute-start.6 = (bf16[256,1024]{1,0:T(8,128)(2,1)S(1)}, bf16[256,1024]{1,0:T(8,128)(2,1)S(1)}, u32[]{:S(2)}, u32[]{:S(2)}) collective-permute-start(bf16[256,1024]{1,0:T(8,128)(2,1)S(1)} %slice_bitcast_fusion), channel_id=1, source_target_pairs={{0,1},{1,2},{2,3},{3,0},{4,5},{5,6},{6,7},{7,4},{8,9},{9,10},{10,1... | collective-permute-start | bytes 1572872 | tf_op jit(solution)/shard_map/ppermute | solution.py:286
  47.3 12.5 %collective-permute-start.7 = (bf16[256,1024]{1,0:T(8,128)(2,1)S(1)}, bf16[256,1024]{1,0:T(8,128)(2,1)S(1)}, u32[]{:S(2)}, u32[]{:S(2)}) collective-permute-start(bf16[256,1024]{1,0:T(8,128)(2,1)S(1)} %slice_bitcast_fusion), channel_id=1, source_target_pairs={{0,3},{1,0},{2,1},{3,2},{4,7},{5,4},{6,5},{7,6},{8,11},{9,8},{10,9... | collective-permute-start | bytes 1572872 | tf_op jit(solution)/shard_map/ppermute | solution.py:286
  48.8 16.4 %collective-permute-start = (bf16[128,1024]{1,0:T(8,128)(2,1)S(1)}, bf16[128,1024]{1,0:T(8,128)(2,1)S(1)}, u32[]{:S(2)}, u32[]{:S(2)}) collective-permute-start(bf16[128,1024]{1,0:T(8,128)(2,1)S(1)} %get-tuple-element.70), channel_id=1, source_target_pairs={{0,1},{1,2},{2,3},{3,0},{4,5},{5,6},{6,7},{7,4},{8,9},{9,10},{10,1... | collective-permute-start | bytes 786440 | tf_op jit(solution)/shard_map/ppermute | solution.py:286
  48.9 17.6 %collective-permute-start.2 = (bf16[128,1024]{1,0:T(8,128)(2,1)S(1)}, bf16[128,1024]{1,0:T(8,128)(2,1)S(1)}, u32[]{:S(2)}, u32[]{:S(2)}) collective-permute-start(bf16[128,1024]{1,0:T(8,128)(2,1)S(1)} %get-tuple-element.69), channel_id=1, source_target_pairs={{0,3},{1,0},{2,1},{3,2},{4,7},{5,4},{6,5},{7,6},{8,11},{9,8},{10,9... | collective-permute-start | bytes 786440 | tf_op jit(solution)/shard_map/ppermute | solution.py:286
  59.6 11.2 %collective-permute-start.8 = (bf16[128,1024]{1,0:T(8,128)(2,1)S(1)}, bf16[128,1024]{1,0:T(8,128)(2,1)S(1)}, u32[]{:S(2)}, u32[]{:S(2)}) collective-permute-start(bf16[128,1024]{1,0:T(8,128)(2,1)S(1)} %slice.52), channel_id=1, source_target_pairs={{0,1},{1,2},{2,3},{3,0},{4,5},{5,6},{6,7},{7,4},{8,9},{9,10},{10,1... | collective-permute-start | bytes 786440 | tf_op jit(solution)/shard_map/ppermute | solution.py:286
  60.6 11.5 %collective-permute-start.9 = (bf16[128,1024]{1,0:T(8,128)(2,1)S(1)}, bf16[128,1024]{1,0:T(8,128)(2,1)S(1)}, u32[]{:S(2)}, u32[]{:S(2)}) collective-permute-start(bf16[128,1024]{1,0:T(8,128)(2,1)S(1)} %slice.53), channel_id=1, source_target_pairs={{0,3},{1,0},{2,1},{3,2},{4,7},{5,4},{6,5},{7,6},{8,11},{9,8},{10,9... | collective-permute-start | bytes 786440 | tf_op jit(solution)/shard_map/ppermute | solution.py:286
  63.2 17.6 %collective-permute-start.4 = (bf16[128,1024]{1,0:T(8,128)(2,1)S(1)}, bf16[128,1024]{1,0:T(8,128)(2,1)S(1)}, u32[]{:S(2)}, u32[]{:S(2)}) collective-permute-start(bf16[128,1024]{1,0:T(8,128)(2,1)S(1)} %get-tuple-element.69), channel_id=1, source_target_pairs={{0,1},{1,2},{2,3},{3,0},{4,5},{5,6},{6,7},{7,4},{8,9},{9,10},{10,1... | collective-permute-start | bytes 786440 | tf_op jit(solution)/shard_map/ppermute | solution.py:286
  65.2 15.5 %collective-permute-start.5 = (bf16[128,1024]{1,0:T(8,128)(2,1)S(1)}, bf16[128,1024]{1,0:T(8,128)(2,1)S(1)}, u32[]{:S(2)}, u32[]{:S(2)}) collective-permute-start(bf16[128,1024]{1,0:T(8,128)(2,1)S(1)} %get-tuple-element.70), channel_id=1, source_target_pairs={{0,3},{1,0},{2,1},{3,2},{4,7},{5,4},{6,5},{7,6},{8,11},{9,8},{10,9... | collective-permute-start | bytes 786440 | tf_op jit(solution)/shard_map/ppermute | solution.py:286
  66.5 21.0 %collective-permute-start.1 = (bf16[128,1024]{1,0:T(8,128)(2,1)S(1)}, bf16[128,1024]{1,0:T(8,128)(2,1)S(1)}, u32[]{:S(2)}, u32[]{:S(2)}) collective-permute-start(bf16[128,1024]{1,0:T(8,128)(2,1)S(1)} %collective-permute-done.p1a), channel_id=1, source_target_pairs={{0,1},{1,2},{2,3},{3,0},{4,5},{5,6},{6,7},{7,4},{8,9},{9,10},{10,1... | collective-permute-start | bytes 786440 | tf_op jit(solution)/shard_map/ppermute | solution.py:286
  70.8 16.7 %collective-permute-start.3 = (bf16[128,1024]{1,0:T(8,128)(2,1)S(1)}, bf16[128,1024]{1,0:T(8,128)(2,1)S(1)}, u32[]{:S(2)}, u32[]{:S(2)}) collective-permute-start(bf16[128,1024]{1,0:T(8,128)(2,1)S(1)} %collective-permute-done.2.n1a), channel_id=1, source_target_pairs={{0,3},{1,0},{2,1},{3,2},{4,7},{5,4},{6,5},{7,6},{8,11},{9,8},{10,9... | collective-permute-start | bytes 786440 | tf_op jit(solution)/shard_map/ppermute | solution.py:286
  80.5 22.8 %collective-permute-start.13 = (bf16[256,512]{1,0:T(8,128)(2,1)}, bf16[256,512]{1,0:T(8,128)(2,1)S(1)}, u32[]{:S(2)}, u32[]{:S(2)}) collective-permute-start(bf16[256,512]{1,0:T(8,128)(2,1)} %get-tuple-element.46), channel_id=1, source_target_pairs={{0,1},{1,2},{2,3},{3,0},{4,5},{5,6},{6,7},{7,4},{8,9},{9,10},{10,1... | collective-permute-start | bytes 786440 | tf_op jit(solution)/shard_map/ppermute | solution.py:286
  92.7 21.0 %collective-permute-start.12 = (f32[64,128]{1,0:T(8,128)}, f32[64,128]{1,0:T(8,128)S(1)}, u32[]{:S(2)}, u32[]{:S(2)}) collective-permute-start(f32[64,128]{1,0:T(8,128)} %get-tuple-element.42), channel_id=1, source_target_pairs={{0,2},{1,3},{2,0},{3,1},{4,6},{5,7},{6,4},{7,5},{8,10},{9,11},{10,... | collective-permute-start | bytes 98312 | tf_op jit(solution)/shard_map/ppermute | solution.py:286
  94.9 19.0 %collective-permute-start.11 = (f32[64,128]{1,0:T(8,128)}, f32[64,128]{1,0:T(8,128)S(1)}, u32[]{:S(2)}, u32[]{:S(2)}) collective-permute-start(f32[64,128]{1,0:T(8,128)} %get-tuple-element.42), channel_id=1, source_target_pairs={{0,3},{1,0},{2,1},{3,2},{4,7},{5,4},{6,5},{7,6},{8,11},{9,8},{10,9... | collective-permute-start | bytes 98312 | tf_op jit(solution)/shard_map/ppermute | solution.py:286
  95.6 21.0 %collective-permute-start.10 = (f32[64,128]{1,0:T(8,128)}, f32[64,128]{1,0:T(8,128)S(1)}, u32[]{:S(2)}, u32[]{:S(2)}) collective-permute-start(f32[64,128]{1,0:T(8,128)} %get-tuple-element.42), channel_id=1, source_target_pairs={{0,1},{1,2},{2,3},{3,0},{4,5},{5,6},{6,7},{7,4},{8,9},{9,10},{10,1... | collective-permute-start | bytes 98312 | tf_op jit(solution)/shard_map/ppermute | solution.py:286
  96.3 7.1 %collective-permute-start.14 = (bf16[256,512]{1,0:T(8,128)(2,1)S(1)}, bf16[256,512]{1,0:T(8,128)(2,1)S(1)}, u32[]{:S(2)}, u32[]{:S(2)}) collective-permute-start(bf16[256,512]{1,0:T(8,128)(2,1)S(1)} %copy-done.24), channel_id=1, source_target_pairs={{0,3},{1,0},{2,1},{3,2},{4,7},{5,4},{6,5},{7,6},{8,11},{9,8},{10,9... | collective-permute-start | bytes 786440 | tf_op jit(solution)/shard_map/ppermute | solution.py:286
  103.2 38.3 %copy-start.2 = (bf16[256,512]{1,0:T(8,128)(2,1)}, bf16[256,512]{1,0:T(8,128)(2,1)S(1)}, u32[]{:S(2)}) copy-start(bf16[256,512]{1,0:T(8,128)(2,1)S(1)} %collective-permute-done.13.refs_1_) | copy-start | bytes 786436
  103.2 6.7 %collective-permute-start.17 = (bf16[256,512]{1,0:T(8,128)(2,1)}, bf16[256,512]{1,0:T(8,128)(2,1)S(1)}, u32[]{:S(2)}, u32[]{:S(2)}) collective-permute-start(bf16[256,512]{1,0:T(8,128)(2,1)} %get-tuple-element.53), channel_id=1, source_target_pairs={{0,1},{1,2},{2,3},{3,0},{4,5},{5,6},{6,7},{7,4},{8,9},{9,10},{10,1... | collective-permute-start | bytes 786440 | tf_op jit(solution)/shard_map/ppermute | solution.py:286
  103.4 38.2 %copy-start.3 = (bf16[256,512]{1,0:T(8,128)(2,1)}, bf16[256,512]{1,0:T(8,128)(2,1)S(1)}, u32[]{:S(2)}) copy-start(bf16[256,512]{1,0:T(8,128)(2,1)S(1)} %collective-permute-done.14.refs_2_) | copy-start | bytes 786436
  103.4 7.6 %collective-permute-start.18 = (bf16[256,512]{1,0:T(8,128)(2,1)}, bf16[256,512]{1,0:T(8,128)(2,1)S(1)}, u32[]{:S(2)}, u32[]{:S(2)}) collective-permute-start(bf16[256,512]{1,0:T(8,128)(2,1)} %get-tuple-element.54), channel_id=1, source_target_pairs={{0,3},{1,0},{2,1},{3,2},{4,7},{5,4},{6,5},{7,6},{8,11},{9,8},{10,9... | collective-permute-start | bytes 786440 | tf_op jit(solution)/shard_map/ppermute | solution.py:286
  110.0 31.5 %collective-permute-start.15 = (bf16[128,512]{1,0:T(8,128)(2,1)S(1)}, bf16[128,512]{1,0:T(8,128)(2,1)S(1)}, u32[]{:S(2)}, u32[]{:S(2)}) collective-permute-start(bf16[128,512]{1,0:T(8,128)(2,1)S(1)} %add_convert_fusion.3), channel_id=1, source_target_pairs={{0,1},{1,2},{2,3},{3,0},{4,5},{5,6},{6,7},{7,4},{8,9},{9,10},{10,1... | collective-permute-start | bytes 393224 | tf_op jit(solution)/shard_map/ppermute | solution.py:286
  111.1 30.4 %collective-permute-start.16 = (bf16[128,512]{1,0:T(8,128)(2,1)S(1)}, bf16[128,512]{1,0:T(8,128)(2,1)S(1)}, u32[]{:S(2)}, u32[]{:S(2)}) collective-permute-start(bf16[128,512]{1,0:T(8,128)(2,1)S(1)} %add_convert_fusion.2), channel_id=1, source_target_pairs={{0,3},{1,0},{2,1},{3,2},{4,7},{5,4},{6,5},{7,6},{8,11},{9,8},{10,9... | collective-permute-start | bytes 393224 | tf_op jit(solution)/shard_map/ppermute | solution.py:286
  113.8 27.7 %collective-permute-start.19 = (bf16[128,512]{1,0:T(8,128)(2,1)S(1)}, bf16[128,512]{1,0:T(8,128)(2,1)S(1)}, u32[]{:S(2)}, u32[]{:S(2)}) collective-permute-start(bf16[128,512]{1,0:T(8,128)(2,1)S(1)} %add_convert_fusion.1), channel_id=1, source_target_pairs={{0,1},{1,2},{2,3},{3,0},{4,5},{5,6},{6,7},{7,4},{8,9},{9,10},{10,1... | collective-permute-start | bytes 393224 | tf_op jit(solution)/shard_map/ppermute | solution.py:286
  113.9 27.7 %collective-permute-start.20 = (bf16[128,512]{1,0:T(8,128)(2,1)S(1)}, bf16[128,512]{1,0:T(8,128)(2,1)S(1)}, u32[]{:S(2)}, u32[]{:S(2)}) collective-permute-start(bf16[128,512]{1,0:T(8,128)(2,1)S(1)} %add_convert_fusion), channel_id=1, source_target_pairs={{0,3},{1,0},{2,1},{3,2},{4,7},{5,4},{6,5},{7,6},{8,11},{9,8},{10,9... | collective-permute-start | bytes 393224 | tf_op jit(solution)/shard_map/ppermute | solution.py:286
  146.0 25.0 %all-to-all-start.2 = ((bf16[64,8,640]{2,1,0:T(8,128)(2,1)}), bf16[64,8,640]{2,1,0:T(8,128)(2,1)S(1)}, u32[]{:S(2)}, u32[]{:S(2)}) async-start(bf16[64,8,640]{2,1,0:T(8,128)(2,1)} %get-tuple-element.57), calls=%async_computation.2 | async-start | bytes 1310720 | tf_op jit(solution)/shard_map/all_to_all | solution.py:289
  (23 other events, 171.9 us)

commit v5 on v4

v5 whole, which is shorter than its diff:
```python
import functools

import jax
import jax.numpy as jnp
from jax import lax
from jax.experimental import pallas as pl
from jax.experimental.pallas import tpu as pltpu
from jax.sharding import PartitionSpec as P


F32 = jnp.float32
BF16 = jnp.bfloat16
HI = lax.Precision.HIGHEST
VMEM = pl.BlockSpec(memory_space=pltpu.VMEM)
SMEM = pl.BlockSpec(memory_space=pltpu.SMEM)


def mm(a, b, dims, precision=None):
    return lax.dot_general(a, b, (dims, ((), ())), precision=precision, preferred_element_type=F32)


NN = ((1,), (0,))
NT = ((1,), (1,))
TN = ((0,), (0,))


def iota(shape, dim):
    return lax.broadcasted_iota(jnp.int32, shape, dim)


def bits(cap):
    return cap.bit_length() - 1


def spread(experts, cap):
    rows = experts * cap
    return ((iota((rows, experts), 0) >> bits(cap)) == iota((rows, experts), 1)).astype(F32)


def dispatch_kernel(cap, tp_ref, tok_ref, og_ref, ids_ref, rw_ref, send_ref, code_ref, gate_ref, mine_ref):
    n_tok = tok_ref.shape[0]
    experts = rw_ref.shape[0]
    share = send_ref.shape[1] // 2
    start = pl.multiple_of(tp_ref[0] * share, share)
    logits = mm(tok_ref[...], rw_ref[...], NT)
    ids = ids_ref[...].astype(F32).T
    lane = iota((n_tok, experts), 1).astype(F32)
    hit = lane == ids[:, 0:1]
    for k in range(1, ids.shape[1]):
        hit = hit | (lane == ids[:, k : k + 1])
    mask = hit.astype(F32)
    top = jnp.max(jnp.where(hit, logits, -jnp.inf), axis=1, keepdims=True)
    weight = jnp.where(hit, jnp.exp(jnp.where(hit, logits - top, 0.0)), 0.0)
    gate = weight / jnp.sum(weight, axis=1, keepdims=True)
    earlier = (iota((n_tok, n_tok), 1) < iota((n_tok, n_tok), 0)).astype(BF16)
    rank = mm(earlier, mask.astype(BF16), NN)
    code = mask * (rank + 1.0)
    code_ref[...] = code
    gate_ref[...] = gate
    expand = spread(experts, cap).astype(BF16)
    rows = experts * cap
    code_of = mm(expand, code.astype(BF16), NT)
    pick = code_of == ((iota((rows, n_tok), 0) & (cap - 1)) + 1).astype(F32)
    gate_of, rest = None, gate
    for _ in range(3):
        piece = rest.astype(BF16)
        rest = rest - piece.astype(F32)
        term = mm(expand, piece, NT)
        gate_of = term if gate_of is None else gate_of + term
    gate_of = jnp.sum(jnp.where(pick, gate_of, 0.0), axis=1, keepdims=True)
    mine = tok_ref[:, pl.ds(start, share)]
    mine_ref[...] = mine
    both = mm(pick.astype(F32).astype(BF16), jnp.concatenate([mine, og_ref[:, pl.ds(start, share)]], axis=1), NN)
    send_ref[:, :share] = both[:, :share].astype(BF16)
    send_ref[:, share:] = (both[:, share:] * gate_of).astype(BF16)


LEFT, RIGHT = 0, 1


def joined(refs, side):
    share = refs[0].shape[1] // 2
    return jnp.concatenate([r[:, side * share : (side + 1) * share] for r in refs], axis=0)


def block(tp_ref, off, share):
    return pl.ds(pl.multiple_of(lax.rem(tp_ref[0] + off, 4) * share, share), share)


def forward(tp_ref, groups, share, wgu, wd, start=None):
    total = start
    for off, refs in groups:
        at = block(tp_ref, off, share)
        terms = (mm(joined(refs, LEFT), wgu[at, :], NN), mm(joined(refs, RIGHT), wd[:, at], NT))
        total = terms if total is None else tuple(a + b for a, b in zip(total, terms))
    return total


def units(cap, both_pre, back):
    rows, ff = back.shape
    gate_pre, up_pre = both_pre[:, :ff], both_pre[:, ff:]
    glu = jnp.minimum(gate_pre, 7.0)
    linear = jnp.clip(up_pre, -7.0, 7.0)
    sig = jax.nn.sigmoid(1.702 * glu)
    act = glu * sig
    hidden = (linear + 1.0) * act
    slope = (linear + 1.0) * (sig + 1.702 * glu * sig * (1.0 - sig))
    slope = jnp.where(gate_pre < 7.0, slope, 0.0)
    up_slope = jnp.where((up_pre > -7.0) & (up_pre < 7.0), act, 0.0)
    score = jnp.sum(hidden * back, axis=1, keepdims=True)
    peers = rows // cap
    spot = ((iota((rows, 128), 0) & (cap - 1)) == iota((rows, 128), 1)).astype(F32) * score
    group = ((iota((peers, rows), 1) >> bits(cap)) == iota((peers, rows), 0)).astype(F32)
    grads = jnp.concatenate([(back * slope).astype(BF16), (back * up_slope).astype(BF16)], axis=1)
    return hidden.astype(BF16), grads, mm(group, spot, NN, HI)


def token_parts(tp_ref, grads, wgu, outs):
    plus_ref, minus_ref, b0_ref, b1_ref, b3_ref = outs
    rows, share = b0_ref.shape
    half = rows // 2

    def part(off):
        return mm(grads, wgu[block(tp_ref, off, share), :], NT)

    far = part(2).astype(BF16)
    plus_ref[:half, :] = far[:half]
    minus_ref[half:, :] = far[half:]
    ahead = part(1)
    b1_ref[...] = ahead[:half]
    plus_ref[half:, :] = ahead[half:].astype(BF16)
    behind = part(3)
    minus_ref[:half, :] = behind[:half].astype(BF16)
    b3_ref[...] = behind[half:]
    b0_ref[...] = part(0)


def first_kernel(cap, tp_ref, own, p0, n0, f0a, f0b, wgu, wd, b1, b3, hid, grads, score, plus, minus, b0):
    groups = ((0, (own,)), (3, (p0,)), (1, (n0,)), (2, (f0a, f0b)))
    hid[...], values, score[...] = units(cap, *forward(tp_ref, groups, b0.shape[1], wgu, wd))
    grads[...] = values
    token_parts(tp_ref, values, wgu, (plus, minus, b0, b1, b3))


def near_kernel(tp_ref, own, p1a, p1b, n1a, n1b, wgu, wd, pre, bk):
    groups = ((0, (own,)), (3, (p1a, p1b)), (1, (n1b, n1a)))
    pre[...], bk[...] = forward(tp_ref, groups, own.shape[1] // 2, wgu, wd)


def far_kernel(cap, tp_ref, f1a, f1b, pre, bk, score0, wgu, wd, hid, grads, score):
    start = (pre[...], bk[...])
    share = f1a.shape[1] // 2
    hid[...], grads[...], mine = units(cap, *forward(tp_ref, ((2, (f1a, f1b)),), share, wgu, wd, start))
    score[...] = jnp.concatenate([score0[...], mine], axis=0)


def token_kernel(tp_ref, grads, wgu, b1, b3, plus, minus, b0):
    token_parts(tp_ref, grads[...], wgu, (plus, minus, b0, b1, b3))


def weight_kernel(tp_ref, own, p0, p1a, p1b, n0, n1a, n1b, f0a, f0b, f1a, f1b, hid0, hid1, grads0, grads1,
                  d_logits_ref, rw_ref, gwg_ref, gwu_ref, gwd_ref, part_ref):
    share = own.shape[1] // 2
    ff = gwg_ref.shape[1]
    part_ref[...] = mm(d_logits_ref[...], rw_ref[:, block(tp_ref, 0, share)].astype(F32), NN, HI)
    hid = jnp.concatenate([hid0[...], hid1[...]], axis=0)
    grads = jnp.concatenate([grads0[...], grads1[...]], axis=0)
    for off, refs in ((0, (own,)), (3, (p0, p1a, p1b)), (1, (n0, n1b, n1a)), (2, (f0a, f0b, f1a, f1b))):
        at = block(tp_ref, off, share)
        t, g = joined(refs, LEFT), joined(refs, RIGHT)
        both = mm(t, grads, TN).astype(BF16)
        gwg_ref[at, :] = both[:, :ff]
        gwu_ref[at, :] = both[:, ff:]
        gwd_ref[:, at] = mm(hid, g, TN).astype(BF16)


def router_kernel(cap, q_ref, code_ref, gate_ref, tok_ref, *refs):
    sums, (payload_ref, d_logits_ref) = refs[:10], refs[10:]
    share = sums[0].shape[1]
    for h in range(2):
        b0, rp, rm, ep, em = sums[5 * h : 5 * h + 5]
        half = b0.shape[0] // 2
        top = b0[:half] + ep[...].astype(F32) + rm[:half].astype(F32)
        low = b0[half:] + rp[half:].astype(F32) + em[...].astype(F32)
        for i, value in enumerate((top, low)):
            n = half // cap
            at = pl.ds((2 * h + i) * n, n)
            payload_ref[at, :, :share] = value.astype(BF16).reshape(n, cap, share)
    code, gate = code_ref[...], gate_ref[...]
    q = q_ref[...].T
    score = jnp.zeros_like(code)
    for r in range(cap):
        score = score + jnp.where(code == r + 1.0, q[r : r + 1, :], 0.0)
    d_logits = score - gate * jnp.sum(score, axis=1, keepdims=True)
    d_logits_ref[...] = d_logits
    term = mm(d_logits, tok_ref[...].astype(F32), TN, HI)
    high = term.astype(BF16)
    low = (term - high.astype(F32)).astype(BF16)
    pieces = share // 128
    for j in range(pieces):
        payload_ref[:, j, share:] = high[:, j * 128 : (j + 1) * 128]
        payload_ref[:, pieces + j, share:] = low[:, j * 128 : (j + 1) * 128]


def home_kernel(cap, home_ref, code_ref, part_ref, tok_out_ref, router_ref):
    share = part_ref.shape[1]
    code = code_ref[...]
    n_tok, experts = code.shape
    rows = experts * cap
    code_of = mm(code.astype(BF16), spread(experts, cap).astype(BF16), NT)
    pick = code_of == ((iota((n_tok, rows), 1) & (cap - 1)) + 1).astype(F32)
    flat = home_ref[...].reshape(rows, home_ref.shape[2])
    tok_out_ref[...] = (
        mm(pick.astype(F32).astype(BF16), flat[:, :share], NN) + part_ref[...]
    ).astype(BF16)
    both = jnp.sum(home_ref[:, :, share:].astype(F32), axis=0)
    pieces = share // 128
    router_ref[...] = both[:pieces] + both[pieces:]


def cost(flops, data):
    return pl.CostEstimate(flops=flops, bytes_accessed=data, transcendentals=0)


def call(body, outs, flops, scalar=True, to_hbm=0, raw=()):
    def place(i, x):
        return pltpu.with_memory_space_constraint(x, pltpu.HBM if i in raw else pltpu.VMEM)

    def run(*args):
        ins = args[1:] if scalar else args
        return pl.pallas_call(
            body,
            out_shape=outs[:to_hbm] + [pltpu.VMEM(o.shape, o.dtype) for o in outs[to_hbm:]],
            in_specs=([SMEM] if scalar else []) + [VMEM] * len(ins),
            out_specs=[VMEM] * len(outs),
            cost_estimate=cost(flops, 4 << 20),
            compiler_params=pltpu.CompilerParams(vmem_limit_bytes=24 << 20),
        )(*args[: len(args) - len(ins)], *(place(i, x) for i, x in enumerate(ins)))

    return run


def shape(dims, dtype):
    return jax.ShapeDtypeStruct(dims, dtype)


def per_device(tokens, out_grad, expert_ids, router_weight, w_gate, w_up, w_down):
    n_tok, width = tokens.shape
    experts = router_weight.shape[1]
    peers = lax.axis_size("ep")
    tp = lax.axis_size("tp")
    cap = 8
    share = width // tp
    ff = w_gate.shape[2]
    rows = peers * cap
    half = rows // 2
    me = jnp.full((1,), lax.axis_index("tp"), jnp.int32)
    unit = 2 * rows * share * ff
    router_t = router_weight.T

    def hop(value, by):
        return lax.ppermute(value, "tp", [(i, (i + by) % tp) for i in range(tp)])

    def exchange(value):
        return lax.all_to_all(value, "ep", split_axis=0, concat_axis=0, tiled=True)

    send, code, gate, mine = call(
        functools.partial(dispatch_kernel, cap),
        [shape((rows, 2 * share), BF16), shape((n_tok, experts), F32), shape((n_tok, experts), F32),
         shape((n_tok, share), BF16)],
        unit,
        raw=(0, 1, 2, 3),
    )(me, tokens, out_grad, expert_ids.T, router_t)
    own = exchange(send.reshape(peers, cap, 2 * share)).reshape(rows, 2 * share)
    piece = half // 2
    own1a, own1b = own[half : half + piece], own[half + piece :]
    p0, n0 = hop(own[:half], 1), hop(own[:half], -1)
    p1a, n1a = hop(own1a, 1), hop(own1b, -1)
    f0a, f0b = hop(p0[:piece], 1), hop(n0[piece:], -1)
    p1b, n1b = hop(own1b, 1), hop(own1a, -1)
    f1a, f1b = hop(p1a, 1), hop(n1a, -1)

    def load_kernel(wg, wu, wd, wgu_out, wd_out, sems):
        copies = [
            pltpu.make_async_copy(wg, wgu_out.at[:, :ff], sems.at[0]),
            pltpu.make_async_copy(wu, wgu_out.at[:, ff:], sems.at[1]),
            pltpu.make_async_copy(wd, wd_out, sems.at[2]),
        ]
        for copy in copies:
            copy.start()
        for copy in copies:
            copy.wait()

    wgu, wd = pl.pallas_call(
        load_kernel,
        out_shape=[pltpu.VMEM((width, 2 * ff), BF16), pltpu.VMEM((ff, width), BF16)],
        in_specs=[pl.BlockSpec(memory_space=pl.ANY)] * 3,
        out_specs=[VMEM] * 2,
        scratch_shapes=[pltpu.SemaphoreType.DMA((3,))],
        cost_estimate=cost(unit, 4 << 20),
        compiler_params=pltpu.CompilerParams(vmem_limit_bytes=24 << 20),
    )(*(pltpu.with_memory_space_constraint(w[0], pltpu.HBM) for w in (w_gate, w_up, w_down)))

    grads = [shape((half, ff), BF16), shape((half, 2 * ff), BF16)]
    kept = [shape((piece, share), F32)] * 2
    parts = [shape((half, share), BF16)] * 2 + [shape((half, share), F32)]
    b10, b30, hid0, grads0, score0, plus0, minus0, b00 = call(
        functools.partial(first_kernel, cap),
        kept + grads + [shape((half // cap, 128), F32)] + parts,
        10 * unit,
        to_hbm=2,
    )(me, own[:half], p0, n0, f0a, f0b, wgu, wd)
    near = call(
        near_kernel, [shape((half, 2 * ff), F32), shape((half, ff), F32)], 5 * unit
    )(me, own[half:], p1a, p1b, n1a, n1b, wgu, wd)
    hid1, grads1, score = call(
        functools.partial(far_kernel, cap), grads + [shape((peers, 128), F32)], 3 * unit
    )(me, f1a, f1b, *near, score0, wgu, wd)
    b11, b31, plus1, minus1, b01 = call(token_kernel, kept + parts, 4 * unit, to_hbm=2)(me, grads1, wgu)

    def summed(plus, minus, b1, b3, b0):
        rp, rm = hop(plus, 1), hop(minus, -1)
        ep = hop((b1 + rp[:piece].astype(F32)).astype(BF16), 1)
        em = hop((b3 + rm[piece:].astype(F32)).astype(BF16), -1)
        return b0, rp, rm, ep, em

    sums = summed(plus0, minus0, b10, b30, b00) + summed(plus1, minus1, b11, b31, b01)
    score = score + hop(score, 1) + hop(score, -1) + hop(score, 2)
    q = exchange(score.reshape(peers, 1, 128)).reshape(peers, 128)
    payload, d_logits = call(
        functools.partial(router_kernel, cap),
        [shape((peers, cap, share + 128), BF16), shape((n_tok, experts), F32)],
        unit,
        scalar=False,
    )(q, code, gate, mine, *sums)
    home = exchange(payload)
    gwg, gwu, gwd, part = call(
        weight_kernel,
        [shape((width, ff), BF16), shape((width, ff), BF16), shape((ff, width), BF16), shape((n_tok, share), F32)],
        12 * unit,
        to_hbm=3,
        raw=range(17),
    )(me, own, p0, p1a, p1b, n0, n1a, n1b, f0a, f0b, f1a, f1b, hid0, hid1, grads0, grads1, d_logits, router_t)
    token_grad, router = call(
        functools.partial(home_kernel, cap),
        [shape((n_tok, share), BF16), shape((share // 128, 128), F32)],
        unit,
        to_hbm=2,
        scalar=False,
    )(home, code, part)
    return (token_grad, router.reshape(share, 1), gwg[None], gwu[None], gwd[None])


def solution(mesh):
    in_specs = (
        P("ep", None),
        P("ep", None),
        P("ep", None),
        P(),
        P("ep", None, "tp"),
        P("ep", None, "tp"),
        P("ep", "tp", None),
    )
    out_specs = (
        P("ep", "tp"),
        P("tp", "ep"),
        P("ep", None, "tp"),
        P("ep", None, "tp"),
        P("ep", "tp", None),
    )

    return jax.shard_map(per_device, mesh=mesh, in_specs=in_specs, out_specs=out_specs, check_vma=False)
```

time: 174 us -> 154 us (0.89)
  Pallas kernels: 39.6 us -> 21.3 us
  waiting for transfers between devices: 31 us -> 39 us
  local copies, waits for them, and re-layouts: 5.44 us -> 0.81 us
  blocking collectives: 66.3 us -> 62.7 us
    pallas_call x8 -> x9, Pallas kernels: 39.6 us -> 21.3 us  [the longest x8 18.8 us: run(): pl.pallas_call(body, out_shape=outs[:to_hbm] + [pltpu.VMEM(o.shape, o.dty...]
    ppermute x21, waiting for transfers between devices: 18.1 us -> 25.9 us  [hop(): return lax.ppermute(value, 'tp', [(i, (i + by) % tp) for i in range(tp)])]
    unnamed x50 -> x32, local copies, waits for them, and re-layouts: 5.34 us -> 0.67 us
    all_to_all x2, blocking collectives: 66.3 us -> 62.7 us  [exchange(): return lax.all_to_all(value, 'ep', split_axis=0, concat_axis=0, tiled=True)]
  transfers between devices with their start and end apart: 22 -> 22, of which waited for: 5 -> 9; matrix products, arithmetic and copies ran while one was open for 1% -> 0% of each run, Pallas kernels for 17% -> 9%
where the time goes in v5:
time: 154 us
  blocking collectives  62.7 us (41%)
  waiting for transfers between devices  39 us (25%)
  starting transfers between devices  29.3 us (19%)
  Pallas kernels  21.3 us (14%)
    all_to_all x2, blocking collectives, exchange(): return lax.all_to_all(value, 'ep', split_axis=0, concat_axis=0, tiled=True)  62.7 us
    ppermute x21, waiting for transfers between devices, hop(): return lax.ppermute(value, 'tp', [(i, (i + by) % tp) for i in range(tp)])  25.9 us
    ppermute x21, starting transfers between devices, hop(): return lax.ppermute(value, 'tp', [(i, (i + by) % tp) for i in range(tp)])  24.5 us
    pallas_call x8, Pallas kernels, run(): pl.pallas_call(body, out_shape=outs[:to_hbm] + [pltpu.VMEM(o.shape, o.dty...  18.8 us
    all_to_all x1, waiting for transfers between devices, exchange(): return lax.all_to_all(value, 'ep', split_axis=0, concat_axis=0, tiled=True)  13.2 us
    all_to_all x1, starting transfers between devices, exchange(): return lax.all_to_all(value, 'ep', split_axis=0, concat_axis=0, tiled=True)  4.75 us
  transfers between devices with their start and end apart: 22, of which 9 were waited for; matrix products, arithmetic and copies ran while one was open for 0% of the time, Pallas kernels for 9%

profile of v5, /device:TPU:1, one launch (start us, length us, event | category | flops | bytes accessed | tf_op | source)
XLA Modules:
  0.0 154.2 jit_solution(12646228652287171349)
XLA Ops:
  0.6 2.2 %shard_map.110 = (bf16[512,1024]{1,0:T(8,128)(2,1)S(1)}, f32[48,64]{1,0:T(8,128)S(1)}, f32[48,64]{1,0:T(8,128)S(1)}, bf16[48,512]{1,0:T(8,128)(2,1)S(1)}) custom-call(s32[1]{0:T(128)} %bitcast.tp_ref, bf16[48,2048]{1,0:T(8,128)(2,1)} %tok_ref.1, bf16[48,2048]{1,0:T(8,128)(2,1)} %og_ref.1, s32[4,48]{1,0:T(4,128)} %bitcast.33, bf16[64,2048]{1,0:T(8,128)(2,1)} %bitcast.31), custom_call_target="tpu_custom_call" | custom-call | flops 201326592 | bytes 4194304 | tf_op jit(solution)/shard_map/pallas_call | solution.py:231
  2.8 41.1 %all_to_all.15 = bf16[64,8,1024]{2,1,0:T(8,128)(2,1)S(1)} all-to-all(bf16[64,8,1024]{2,1,0:T(8,128)(2,1)S(1)} %bitcast.24), channel_id=1, replica_groups=mesh['ep'=64,'tp'=4] {'ep'}, dimensions={0} | all-to-all | bytes 2097152 | tf_op jit(solution)/shard_map/all_to_all | solution.py:265
  44.0 2.6 %collective-permute-start.7 = (bf16[256,1024]{1,0:T(8,128)(2,1)S(1)}, bf16[256,1024]{1,0:T(8,128)(2,1)S(1)}, u32[]{:S(2)}, u32[]{:S(2)}) collective-permute-start(bf16[256,1024]{1,0:T(8,128)(2,1)S(1)} %get-tuple-element.69.own), channel_id=1, source_target_pairs={{0,3},{1,0},{2,1},{3,2},{4,7},{5,4},{6,5},{7,6},{8,11},{9,8},{10,9... | collective-permute-start | bytes 1572872 | tf_op jit(solution)/shard_map/ppermute | solution.py:262
  46.9 2.6 %collective-permute-start.2 = (bf16[128,1024]{1,0:T(8,128)(2,1)S(1)}, bf16[128,1024]{1,0:T(8,128)(2,1)S(1)}, u32[]{:S(2)}, u32[]{:S(2)}) collective-permute-start(bf16[128,1024]{1,0:T(8,128)(2,1)S(1)} %get-tuple-element.71), channel_id=1, source_target_pairs={{0,3},{1,0},{2,1},{3,2},{4,7},{5,4},{6,5},{7,6},{8,11},{9,8},{10,9... | collective-permute-start | bytes 786440 | tf_op jit(solution)/shard_map/ppermute | solution.py:262
  49.4 7.2 %collective-permute-done.7.n0 = bf16[256,1024]{1,0:T(8,128)(2,1)S(1)} collective-permute-done((bf16[256,1024]{1,0:T(8,128)(2,1)S(1)}, bf16[256,1024]{1,0:T(8,128)(2,1)S(1)}, u32[]{:S(2)}, u32[]{:S(2)}) %collective-permute-start.7) | collective-permute-done | bytes 524320 | tf_op jit(solution)/shard_map/ppermute | solution.py:262
  56.7 3.4 %collective-permute-start.5 = (bf16[128,1024]{1,0:T(8,128)(2,1)S(1)}, bf16[128,1024]{1,0:T(8,128)(2,1)S(1)}, u32[]{:S(2)}, u32[]{:S(2)}) collective-permute-start(bf16[128,1024]{1,0:T(8,128)(2,1)S(1)} %get-tuple-element.72), channel_id=1, source_target_pairs={{0,3},{1,0},{2,1},{3,2},{4,7},{5,4},{6,5},{7,6},{8,11},{9,8},{10,9... | collective-permute-start | bytes 786440 | tf_op jit(solution)/shard_map/ppermute | solution.py:262
  60.2 5.2 %collective-permute-done.4.p1b = bf16[128,1024]{1,0:T(8,128)(2,1)S(1)} collective-permute-done((bf16[128,1024]{1,0:T(8,128)(2,1)S(1)}, bf16[128,1024]{1,0:T(8,128)(2,1)S(1)}, u32[]{:S(2)}, u32[]{:S(2)}) %collective-permute-start.4) | collective-permute-done | bytes 262176 | tf_op jit(solution)/shard_map/ppermute | solution.py:262
  65.4 2.5 %shard_map.111 = (bf16[2048,768]{1,0:T(8,128)(2,1)S(1)}, bf16[384,2048]{1,0:T(8,128)(2,1)S(1)}) custom-call(bf16[2048,384]{1,0:T(8,128)(2,1)} %bitcast.27, bf16[2048,384]{1,0:T(8,128)(2,1)} %bitcast.28, bf16[384,2048]{1,0:T(8,128)(2,1)} %bitcast.29), custom_call_target="tpu_custom_call" | custom-call | flops 201326592 | bytes 4194304 | tf_op jit(solution)/shard_map/pallas_call | solution.py:294
  67.9 2.7 %collective-permute-start.3 = (bf16[128,1024]{1,0:T(8,128)(2,1)S(1)}, bf16[128,1024]{1,0:T(8,128)(2,1)S(1)}, u32[]{:S(2)}, u32[]{:S(2)}) collective-permute-start(bf16[128,1024]{1,0:T(8,128)(2,1)S(1)} %collective-permute-done.2.n1a), channel_id=1, source_target_pairs={{0,3},{1,0},{2,1},{3,2},{4,7},{5,4},{6,5},{7,6},{8,11},{9,8},{10,9... | collective-permute-start | bytes 786440 | tf_op jit(solution)/shard_map/ppermute | solution.py:262
  73.5 3.1 %collective-permute-done.8.f0a = bf16[128,1024]{1,0:T(8,128)(2,1)S(1)} collective-permute-done((bf16[128,1024]{1,0:T(8,128)(2,1)S(1)}, bf16[128,1024]{1,0:T(8,128)(2,1)S(1)}, u32[]{:S(2)}, u32[]{:S(2)}) %collective-permute-start.8) | collective-permute-done | bytes 262176 | tf_op jit(solution)/shard_map/ppermute | solution.py:262
  76.7 3.3 %shard_map.113 = (f32[128,512]{1,0:T(8,128)S(1)}, f32[128,512]{1,0:T(8,128)S(1)}, bf16[256,384]{1,0:T(8,128)(2,1)S(1)}, bf16[256,768]{1,0:T(8,128)(2,1)S(1)}, f3...) custom-call(s32[1]{0:T(128)} %bitcast.tp_ref, ...), custom_call_target="tpu_custom_call" | custom-call | flops 2013265920 | bytes 4194304 | tf_op jit(solution)/shard_map/pallas_call | solution.py:231
  80.0 2.2 %collective-permute-done.1.f1a = bf16[128,1024]{1,0:T(8,128)(2,1)S(1)} collective-permute-done((bf16[128,1024]{1,0:T(8,128)(2,1)S(1)}, bf16[128,1024]{1,0:T(8,128)(2,1)S(1)}, u32[]{:S(2)}, u32[]{:S(2)}) %collective-permute-start.1) | collective-permute-done | bytes 262176 | tf_op jit(solution)/shard_map/ppermute | solution.py:262
  84.5 2.7 %collective-permute-start.18 = (bf16[256,512]{1,0:T(8,128)(2,1)S(1)}, bf16[256,512]{1,0:T(8,128)(2,1)S(1)}, u32[]{:S(2)}, u32[]{:S(2)}) collective-permute-start(bf16[256,512]{1,0:T(8,128)(2,1)S(1)} %get-tuple-element.55), channel_id=1, source_target_pairs={{0,3},{1,0},{2,1},{3,2},{4,7},{5,4},{6,5},{7,6},{8,11},{9,8},{10,9... | collective-permute-start | bytes 786440 | tf_op jit(solution)/shard_map/ppermute | solution.py:262
  87.1 1.3 collective-permute-start.11
  88.6 2.6 %collective-permute-done.17.refs_6_ = bf16[256,512]{1,0:T(8,128)(2,1)S(1)} collective-permute-done((bf16[256,512]{1,0:T(8,128)(2,1)S(1)}, bf16[256,512]{1,0:T(8,128)(2,1)S(1)}, u32[]{:S(2)}, u32[]{:S(2)}) %collective-permute-start.17) | collective-permute-done | bytes 262176 | tf_op jit(solution)/shard_map/ppermute | solution.py:262
  91.3 3.0 %collective-permute-start.14 = (bf16[256,512]{1,0:T(8,128)(2,1)S(1)}, bf16[256,512]{1,0:T(8,128)(2,1)S(1)}, u32[]{:S(2)}, u32[]{:S(2)}) collective-permute-start(bf16[256,512]{1,0:T(8,128)(2,1)S(1)} %get-tuple-element.49), channel_id=1, source_target_pairs={{0,3},{1,0},{2,1},{3,2},{4,7},{5,4},{6,5},{7,6},{8,11},{9,8},{10,9... | collective-permute-start | bytes 786440 | tf_op jit(solution)/shard_map/ppermute | solution.py:262
  94.4 3.8 %collective-permute-done.13.refs_1_ = bf16[256,512]{1,0:T(8,128)(2,1)S(1)} collective-permute-done((bf16[256,512]{1,0:T(8,128)(2,1)S(1)}, bf16[256,512]{1,0:T(8,128)(2,1)S(1)}, u32[]{:S(2)}, u32[]{:S(2)}) %collective-permute-start.13) | collective-permute-done | bytes 262176 | tf_op jit(solution)/shard_map/ppermute | solution.py:262
  98.2 2.8 %collective-permute-start.20 = (bf16[128,512]{1,0:T(8,128)(2,1)S(1)}, bf16[128,512]{1,0:T(8,128)(2,1)S(1)}, u32[]{:S(2)}, u32[]{:S(2)}) collective-permute-start(bf16[128,512]{1,0:T(8,128)(2,1)S(1)} %add_convert_fusion), channel_id=1, source_target_pairs={{0,3},{1,0},{2,1},{3,2},{4,7},{5,4},{6,5},{7,6},{8,11},{9,8},{10,9... | collective-permute-start | bytes 393224 | tf_op jit(solution)/shard_map/ppermute | solution.py:262
  101.3 2.7 %collective-permute-start.16 = (bf16[128,512]{1,0:T(8,128)(2,1)S(1)}, bf16[128,512]{1,0:T(8,128)(2,1)S(1)}, u32[]{:S(2)}, u32[]{:S(2)}) collective-permute-start(bf16[128,512]{1,0:T(8,128)(2,1)S(1)} %add_convert_fusion.2), channel_id=1, source_target_pairs={{0,3},{1,0},{2,1},{3,2},{4,7},{5,4},{6,5},{7,6},{8,11},{9,8},{10,9... | collective-permute-start | bytes 393224 | tf_op jit(solution)/shard_map/ppermute | solution.py:262
  104.0 21.6 %all_to_all.16 = f32[64,1,128]{2,1,0:T(1,128)S(1)} all-to-all(f32[64,1,128]{2,1,0:T(1,128)S(1)} %bitcast.30), channel_id=1, replica_groups=mesh['ep'=64,'tp'=4] {'ep'}, dimensions={0} | all-to-all | bytes 65536 | tf_op jit(solution)/shard_map/all_to_all | solution.py:265
  125.6 1.9 %shard_map.116 = (bf16[64,8,640]{2,1,0:T(8,128)(2,1)}, f32[48,64]{1,0:T(8,128)S(1)}) custom-call(f32[64,128]{1,0:T(8,128)S(1)} %bitcast.25, f32[48,64]{1,0:T(8,128)S(1)} %get-tuple-element.44.code_ref, f32[48,64]{1,0:T(8,128)S(1)} %get-tuple-element.45.gate_ref, bf16[48,512]{1,0:T(8,128)(2,1)S(1)} %get-tuple-element.46.tok_ref, ...), custom_call_target="tpu_custom_call" | custom-call | flops 201326592 | bytes 4194304 | tf_op jit(solution)/shard_map/pallas_call | solution.py:231
  128.0 4.7 %all-to-all-start.2 = ((bf16[64,8,640]{2,1,0:T(8,128)(2,1)}), bf16[64,8,640]{2,1,0:T(8,128)(2,1)S(1)}, u32[]{:S(2)}, u32[]{:S(2)}) async-start(bf16[64,8,640]{2,1,0:T(8,128)(2,1)} %get-tuple-element.58), calls=%async_computation.2 | async-start | bytes 1310720 | tf_op jit(solution)/shard_map/all_to_all | solution.py:265
  132.8 7.3 %shard_map.117 = (bf16[2048,384]{1,0:T(8,128)(2,1)}, bf16[2048,384]{1,0:T(8,128)(2,1)}, bf16[384,2048]{1,0:T(8,128)(2,1)}, f32[48,512]{1,0:T(8,128)S(1)}) custom-call(s32[1]{0:T(128)} %bitcast.tp_ref, bf16[512,1024]{1,0:T(8,128)(2,1)} %bitcast.26, bf16[256,1024]{1,0:T(8,128)(2,1)} %copy-done.8, bf16[128,1024]{1,0:T(8,128)(2,1)} %copy-done.3, ...), custom_call_target="tpu_custom_call" | custom-call | flops 2415919104 | bytes 4194304 | tf_op jit(solution)/shard_map/pallas_call | solution.py:231
  140.1 13.2 %all-to-all-done.2.home_ref = bf16[64,8,640]{2,1,0:T(8,128)(2,1)S(1)} async-done(((bf16[64,8,640]{2,1,0:T(8,128)(2,1)}), bf16[64,8,640]{2,1,0:T(8,128)(2,1)S(1)}, u32[]{:S(2)}, u32[]{:S(2)}) %all-to-all-start.2) | async-done | bytes 655392 | tf_op jit(solution)/shard_map/all_to_all | solution.py:265
  (72 shorter events, 7.7 us)
Async XLA Ops:
  44.0 12.7 %collective-permute-start.7 = (bf16[256,1024]{1,0:T(8,128)(2,1)S(1)}, bf16[256,1024]{1,0:T(8,128)(2,1)S(1)}, u32[]{:S(2)}, u32[]{:S(2)}) collective-permute-start(bf16[256,1024]{1,0:T(8,128)(2,1)S(1)} %get-tuple-element.69.own), channel_id=1, source_target_pairs={{0,3},{1,0},{2,1},{3,2},{4,7},{5,4},{6,5},{7,6},{8,11},{9,8},{10,9... | collective-permute-start | bytes 1572872 | tf_op jit(solution)/shard_map/ppermute | solution.py:262
  46.5 13.6 %collective-permute-start.6 = (bf16[256,1024]{1,0:T(8,128)(2,1)S(1)}, bf16[256,1024]{1,0:T(8,128)(2,1)S(1)}, u32[]{:S(2)}, u32[]{:S(2)}) collective-permute-start(bf16[256,1024]{1,0:T(8,128)(2,1)S(1)} %get-tuple-element.69.own), channel_id=1, source_target_pairs={{0,1},{1,2},{2,3},{3,0},{4,5},{5,6},{6,7},{7,4},{8,9},{9,10},{10,1... | collective-permute-start | bytes 1572872 | tf_op jit(solution)/shard_map/ppermute | solution.py:262
  46.6 18.8 %collective-permute-start.4 = (bf16[128,1024]{1,0:T(8,128)(2,1)S(1)}, bf16[128,1024]{1,0:T(8,128)(2,1)S(1)}, u32[]{:S(2)}, u32[]{:S(2)}) collective-permute-start(bf16[128,1024]{1,0:T(8,128)(2,1)S(1)} %get-tuple-element.71), channel_id=1, source_target_pairs={{0,1},{1,2},{2,3},{3,0},{4,5},{5,6},{6,7},{7,4},{8,9},{9,10},{10,1... | collective-permute-start | bytes 786440 | tf_op jit(solution)/shard_map/ppermute | solution.py:262
  46.9 21.0 %collective-permute-start.2 = (bf16[128,1024]{1,0:T(8,128)(2,1)S(1)}, bf16[128,1024]{1,0:T(8,128)(2,1)S(1)}, u32[]{:S(2)}, u32[]{:S(2)}) collective-permute-start(bf16[128,1024]{1,0:T(8,128)(2,1)S(1)} %get-tuple-element.71), channel_id=1, source_target_pairs={{0,3},{1,0},{2,1},{3,2},{4,7},{5,4},{6,5},{7,6},{8,11},{9,8},{10,9... | collective-permute-start | bytes 786440 | tf_op jit(solution)/shard_map/ppermute | solution.py:262
  49.4 21.6 %collective-permute-start = (bf16[128,1024]{1,0:T(8,128)(2,1)S(1)}, bf16[128,1024]{1,0:T(8,128)(2,1)S(1)}, u32[]{:S(2)}, u32[]{:S(2)}) collective-permute-start(bf16[128,1024]{1,0:T(8,128)(2,1)S(1)} %get-tuple-element.72), channel_id=1, source_target_pairs={{0,1},{1,2},{2,3},{3,0},{4,5},{5,6},{6,7},{7,4},{8,9},{9,10},{10,1... | collective-permute-start | bytes 786440 | tf_op jit(solution)/shard_map/ppermute | solution.py:262
  56.7 20.0 %copy-start.7 = (bf16[256,1024]{1,0:T(8,128)(2,1)}, bf16[256,1024]{1,0:T(8,128)(2,1)S(1)}, u32[]{:S(2)}) copy-start(bf16[256,1024]{1,0:T(8,128)(2,1)S(1)} %collective-permute-done.7.n0) | copy-start | bytes 1572868
  56.7 14.4 %collective-permute-start.5 = (bf16[128,1024]{1,0:T(8,128)(2,1)S(1)}, bf16[128,1024]{1,0:T(8,128)(2,1)S(1)}, u32[]{:S(2)}, u32[]{:S(2)}) collective-permute-start(bf16[128,1024]{1,0:T(8,128)(2,1)S(1)} %get-tuple-element.72), channel_id=1, source_target_pairs={{0,3},{1,0},{2,1},{3,2},{4,7},{5,4},{6,5},{7,6},{8,11},{9,8},{10,9... | collective-permute-start | bytes 786440 | tf_op jit(solution)/shard_map/ppermute | solution.py:262
  60.1 16.5 %copy-start.8 = (bf16[256,1024]{1,0:T(8,128)(2,1)}, bf16[256,1024]{1,0:T(8,128)(2,1)S(1)}, u32[]{:S(2)}) copy-start(bf16[256,1024]{1,0:T(8,128)(2,1)S(1)} %collective-permute-done.6.p0) | copy-start | bytes 1572868
  60.1 13.4 %collective-permute-start.9 = (bf16[128,1024]{1,0:T(8,128)(2,1)S(1)}, bf16[128,1024]{1,0:T(8,128)(2,1)S(1)}, u32[]{:S(2)}, u32[]{:S(2)}) collective-permute-start(bf16[128,1024]{1,0:T(8,128)(2,1)S(1)} %slice.63), channel_id=1, source_target_pairs={{0,3},{1,0},{2,1},{3,2},{4,7},{5,4},{6,5},{7,6},{8,11},{9,8},{10,9... | collective-permute-start | bytes 786440 | tf_op jit(solution)/shard_map/ppermute | solution.py:262
  65.4 11.2 %collective-permute-start.8 = (bf16[128,1024]{1,0:T(8,128)(2,1)S(1)}, bf16[128,1024]{1,0:T(8,128)(2,1)S(1)}, u32[]{:S(2)}, u32[]{:S(2)}) collective-permute-start(bf16[128,1024]{1,0:T(8,128)(2,1)S(1)} %slice.62), channel_id=1, source_target_pairs={{0,1},{1,2},{2,3},{3,0},{4,5},{5,6},{6,7},{7,4},{8,9},{9,10},{10,1... | collective-permute-start | bytes 786440 | tf_op jit(solution)/shard_map/ppermute | solution.py:262
  67.9 12.1 %collective-permute-start.3 = (bf16[128,1024]{1,0:T(8,128)(2,1)S(1)}, bf16[128,1024]{1,0:T(8,128)(2,1)S(1)}, u32[]{:S(2)}, u32[]{:S(2)}) collective-permute-start(bf16[128,1024]{1,0:T(8,128)(2,1)S(1)} %collective-permute-done.2.n1a), channel_id=1, source_target_pairs={{0,3},{1,0},{2,1},{3,2},{4,7},{5,4},{6,5},{7,6},{8,11},{9,8},{10,9... | collective-permute-start | bytes 786440 | tf_op jit(solution)/shard_map/ppermute | solution.py:262
  71.0 11.2 %collective-permute-start.1 = (bf16[128,1024]{1,0:T(8,128)(2,1)S(1)}, bf16[128,1024]{1,0:T(8,128)(2,1)S(1)}, u32[]{:S(2)}, u32[]{:S(2)}) collective-permute-start(bf16[128,1024]{1,0:T(8,128)(2,1)S(1)} %collective-permute-done.p1a), channel_id=1, source_target_pairs={{0,1},{1,2},{2,3},{3,0},{4,5},{5,6},{6,7},{7,4},{8,9},{9,10},{10,1... | collective-permute-start | bytes 786440 | tf_op jit(solution)/shard_map/ppermute | solution.py:262
  84.4 6.9 %collective-permute-start.17 = (bf16[256,512]{1,0:T(8,128)(2,1)S(1)}, bf16[256,512]{1,0:T(8,128)(2,1)S(1)}, u32[]{:S(2)}, u32[]{:S(2)}) collective-permute-start(bf16[256,512]{1,0:T(8,128)(2,1)S(1)} %get-tuple-element.54), channel_id=1, source_target_pairs={{0,1},{1,2},{2,3},{3,0},{4,5},{5,6},{6,7},{7,4},{8,9},{9,10},{10,1... | collective-permute-start | bytes 786440 | tf_op jit(solution)/shard_map/ppermute | solution.py:262
  84.5 6.8 %collective-permute-start.18 = (bf16[256,512]{1,0:T(8,128)(2,1)S(1)}, bf16[256,512]{1,0:T(8,128)(2,1)S(1)}, u32[]{:S(2)}, u32[]{:S(2)}) collective-permute-start(bf16[256,512]{1,0:T(8,128)(2,1)S(1)} %get-tuple-element.55), channel_id=1, source_target_pairs={{0,3},{1,0},{2,1},{3,2},{4,7},{5,4},{6,5},{7,6},{8,11},{9,8},{10,9... | collective-permute-start | bytes 786440 | tf_op jit(solution)/shard_map/ppermute | solution.py:262
  87.1 13.8 %collective-permute-start.12 = (f32[64,128]{1,0:T(8,128)S(1)}, f32[64,128]{1,0:T(8,128)S(1)}, u32[]{:S(2)}, u32[]{:S(2)}) collective-permute-start(f32[64,128]{1,0:T(8,128)S(1)} %get-tuple-element.43), channel_id=1, source_target_pairs={{0,2},{1,3},{2,0},{3,1},{4,6},{5,7},{6,4},{7,5},{8,10},{9,11},{10,... | collective-permute-start | bytes 98312 | tf_op jit(solution)/shard_map/ppermute | solution.py:262
  87.1 14.1 %collective-permute-start.11 = (f32[64,128]{1,0:T(8,128)S(1)}, f32[64,128]{1,0:T(8,128)S(1)}, u32[]{:S(2)}, u32[]{:S(2)}) collective-permute-start(f32[64,128]{1,0:T(8,128)S(1)} %get-tuple-element.43), channel_id=1, source_target_pairs={{0,3},{1,0},{2,1},{3,2},{4,7},{5,4},{6,5},{7,6},{8,11},{9,8},{10,9... | collective-permute-start | bytes 98312 | tf_op jit(solution)/shard_map/ppermute | solution.py:262
  88.4 15.5 %collective-permute-start.10 = (f32[64,128]{1,0:T(8,128)S(1)}, f32[64,128]{1,0:T(8,128)S(1)}, u32[]{:S(2)}, u32[]{:S(2)}) collective-permute-start(f32[64,128]{1,0:T(8,128)S(1)} %get-tuple-element.43), channel_id=1, source_target_pairs={{0,1},{1,2},{2,3},{3,0},{4,5},{5,6},{6,7},{7,4},{8,9},{9,10},{10,1... | collective-permute-start | bytes 98312 | tf_op jit(solution)/shard_map/ppermute | solution.py:262
  91.2 6.9 %collective-permute-start.13 = (bf16[256,512]{1,0:T(8,128)(2,1)S(1)}, bf16[256,512]{1,0:T(8,128)(2,1)S(1)}, u32[]{:S(2)}, u32[]{:S(2)}) collective-permute-start(bf16[256,512]{1,0:T(8,128)(2,1)S(1)} %get-tuple-element.48), channel_id=1, source_target_pairs={{0,1},{1,2},{2,3},{3,0},{4,5},{5,6},{6,7},{7,4},{8,9},{9,10},{10,1... | collective-permute-start | bytes 786440 | tf_op jit(solution)/shard_map/ppermute | solution.py:262
  91.3 6.9 %collective-permute-start.14 = (bf16[256,512]{1,0:T(8,128)(2,1)S(1)}, bf16[256,512]{1,0:T(8,128)(2,1)S(1)}, u32[]{:S(2)}, u32[]{:S(2)}) collective-permute-start(bf16[256,512]{1,0:T(8,128)(2,1)S(1)} %get-tuple-element.49), channel_id=1, source_target_pairs={{0,3},{1,0},{2,1},{3,2},{4,7},{5,4},{6,5},{7,6},{8,11},{9,8},{10,9... | collective-permute-start | bytes 786440 | tf_op jit(solution)/shard_map/ppermute | solution.py:262
  98.1 27.4 %collective-permute-start.19 = (bf16[128,512]{1,0:T(8,128)(2,1)S(1)}, bf16[128,512]{1,0:T(8,128)(2,1)S(1)}, u32[]{:S(2)}, u32[]{:S(2)}) collective-permute-start(bf16[128,512]{1,0:T(8,128)(2,1)S(1)} %add_convert_fusion.1), channel_id=1, source_target_pairs={{0,1},{1,2},{2,3},{3,0},{4,5},{5,6},{6,7},{7,4},{8,9},{9,10},{10,1... | collective-permute-start | bytes 393224 | tf_op jit(solution)/shard_map/ppermute | solution.py:262
  98.2 27.4 %collective-permute-start.20 = (bf16[128,512]{1,0:T(8,128)(2,1)S(1)}, bf16[128,512]{1,0:T(8,128)(2,1)S(1)}, u32[]{:S(2)}, u32[]{:S(2)}) collective-permute-start(bf16[128,512]{1,0:T(8,128)(2,1)S(1)} %add_convert_fusion), channel_id=1, source_target_pairs={{0,3},{1,0},{2,1},{3,2},{4,7},{5,4},{6,5},{7,6},{8,11},{9,8},{10,9... | collective-permute-start | bytes 393224 | tf_op jit(solution)/shard_map/ppermute | solution.py:262
  101.0 24.6 %collective-permute-start.15 = (bf16[128,512]{1,0:T(8,128)(2,1)S(1)}, bf16[128,512]{1,0:T(8,128)(2,1)S(1)}, u32[]{:S(2)}, u32[]{:S(2)}) collective-permute-start(bf16[128,512]{1,0:T(8,128)(2,1)S(1)} %add_convert_fusion.3), channel_id=1, source_target_pairs={{0,1},{1,2},{2,3},{3,0},{4,5},{5,6},{6,7},{7,4},{8,9},{9,10},{10,1... | collective-permute-start | bytes 393224 | tf_op jit(solution)/shard_map/ppermute | solution.py:262
  101.3 24.3 %collective-permute-start.16 = (bf16[128,512]{1,0:T(8,128)(2,1)S(1)}, bf16[128,512]{1,0:T(8,128)(2,1)S(1)}, u32[]{:S(2)}, u32[]{:S(2)}) collective-permute-start(bf16[128,512]{1,0:T(8,128)(2,1)S(1)} %add_convert_fusion.2), channel_id=1, source_target_pairs={{0,3},{1,0},{2,1},{3,2},{4,7},{5,4},{6,5},{7,6},{8,11},{9,8},{10,9... | collective-permute-start | bytes 393224 | tf_op jit(solution)/shard_map/ppermute | solution.py:262
  128.0 25.2 %all-to-all-start.2 = ((bf16[64,8,640]{2,1,0:T(8,128)(2,1)}), bf16[64,8,640]{2,1,0:T(8,128)(2,1)S(1)}, u32[]{:S(2)}, u32[]{:S(2)}) async-start(bf16[64,8,640]{2,1,0:T(8,128)(2,1)} %get-tuple-element.58), calls=%async_computation.2 | async-start | bytes 1310720 | tf_op jit(solution)/shard_map/all_to_all | solution.py:265
  (14 other events, 38.5 us)
